TPU v7x, 256 devices: a 4x2x16 block of a 4x16x16 slice. The times are simulated.
256 devices in a mesh: grp: 2 (over y), st: 32 (over z, core), tp: 4 (over x).
Axes of the slice: x: 4, y: 2, z: 16, core: 2. Of those that a mesh axis runs over, the one named last changes fastest.
The devices are a block of a 4x16x16 slice.
Arguments:
- pass_ids: int32 [512, 4], P(('grp', 'st')), parts along dimension 0, may hold values from 0 to 511, as said below
- store: bfloat16 [512, 64, 2048], P('st', None, 'tp'), may hold values from -6 to 6
- queries: bfloat16 [65536, 1024], P(('grp', 'st'), 'tp'), parts along dimension 0, may hold values from -40 to 40
- gate_pre: bfloat16 [65536, 1024], P(('grp', 'st'), 'tp'), parts along dimension 0, may hold values from -6 to 6
- w_query: bfloat16 [2048, 1024], P(None, 'tp'), may hold values from -0.125 to 0.125
- w_gate: bfloat16 [2048, 1024], P(None, 'tp'), may hold values from -0.125 to 0.125
- w_key: bfloat16 [2048, 1024], P(None, 'tp'), may hold values from -0.125 to 0.125
- w_value: bfloat16 [2048, 1024], P(None, 'tp'), may hold values from -0.125 to 0.125
- d_mem: bfloat16 [65536, 1024], P(('grp', 'st'), 'tp'), parts along dimension 0, may hold values from -6 to 6
Outputs:
- d_tokens: bfloat16 [65536, 2048], P(('grp', 'st', 'tp')), parts along dimension 0
- d_store: bfloat16 [1024, 64, 2048], P(('grp', 'st', 'tp')), parts along dimension 0
- d_wkey: float32 [4096, 1024], P(('grp', 'st'), 'tp'), parts along dimension 0
There are 2 independent parts, one for each index of `grp`. A program takes and returns all parts, laid end to end along the dimension named above; an argument that names none is the same for every part. Nothing has to cross between parts.
Inputs may be any that keep to these rules, and one draw needn't show every extreme that they name: `pass_ids`: the 8 blocks of one index of st name at most 2 passages (counted with repetition) held by any one index of st o, that is passages o * 16 to o * 16 + 15. Every index of st takes exactly 2 passages from each of 16 indices of st and none from the others, so the bound 2 is reached by every index.
All inputs are finite; a program needn't handle non-finite values.
Results may differ from a plain program's by a relative error of at most 0.02.
Values may be sent and summed in bfloat16 or wider, within the bound.
A program may use at most 128 MiB of HBM per device.

v0:
```python
import jax
import jax.numpy as jnp
from jax import lax
from jax.sharding import Mesh
from jax.sharding import PartitionSpec as P

HD = 256
BLK = 128
PB = 4
ST = ("st_0", "st_1")
GRP_ST = ("grp", "st_0", "st_1")
GRP_ST_TP = ("grp", "st_0", "st_1", "tp")


def sum_in_order(tiles, axes, order):
    dims = [lax.axis_size(a) for a in axes]
    tiles = tiles.reshape(*dims, *tiles.shape[1:])
    tiles = tiles.transpose(*order, *range(len(axes), tiles.ndim))
    tiles = tiles.reshape(-1, *tiles.shape[len(axes) :])
    for k in order:
        tiles = lax.psum_scatter(tiles, axes[k], scatter_dimension=0, tiled=True)
    return tiles[0]


def in_blocks(array, dim, devices):
    before, after = (array.shape[:dim], array.shape[dim + 1 :])
    return jnp.moveaxis(array.reshape(*before, devices, -1, *after), dim, 0)


def summed_rows_2(array, axes, order, dim):
    devices = lax.axis_size(axes)
    return sum_in_order(in_blocks(array, dim, devices), axes, order)


def summed_on_arrival(array, axis, dim):
    devices = lax.axis_size(axis)
    tiles = lax.all_to_all(in_blocks(array, dim, devices), axis, 0, 0, tiled=True)
    return jnp.sum(tiles.astype(jnp.float32), axis=0)


def local(pass_ids, store, queries, gate_pre, w_query, w_gate, w_key, w_value, d_mem):
    st_count = lax.axis_size(ST)
    tp_count = lax.axis_size("tp")
    tok_rows, head_cols = queries.shape
    head_count = head_cols // HD
    blocks = tok_rows // BLK
    passages = store.shape[0]
    pass_len = store.shape[1]
    model_width = w_key.shape[0]
    requests = blocks * PB
    slot_depth = max(2, requests // st_count)
    slot_total = st_count * slot_depth
    pair_cols = 2 * head_cols
    request_ids = pass_ids.reshape(-1)
    owners = request_ids // passages
    within = request_ids % passages
    owner_hot = (owners[:, None] == jnp.arange(st_count, dtype=jnp.int32)[None, :]).astype(
        jnp.int32
    )
    ranking = jnp.sum(jnp.cumsum(owner_hot, axis=0) * owner_hot, axis=1) - 1
    slot_index = owners * slot_depth + ranking
    slot_hot = slot_index[:, None] == jnp.arange(slot_total, dtype=jnp.int32)[None, :]
    wanted = jnp.max(jnp.where(slot_hot, within[:, None], -1), axis=0).reshape(st_count, slot_depth)
    asked_rows = lax.all_to_all(wanted, ST, split_axis=0, concat_axis=0, tiled=True).reshape(-1)
    weight_kv = jnp.concatenate([w_key, w_value], axis=1)
    gathered = lax.all_gather(store, "tp", axis=2, tiled=True)
    flat_rows = gathered.reshape(passages * pass_len, model_width)
    kv_pass = jnp.dot(flat_rows, weight_kv, preferred_element_type=jnp.float32)
    kv_low = kv_pass.astype(jnp.bfloat16).reshape(passages, pass_len * pair_cols)
    pick_rows = (asked_rows[:, None] == jnp.arange(passages, dtype=jnp.int32)[None, :]).astype(
        jnp.bfloat16
    )
    outgoing = jnp.dot(pick_rows, kv_low, preferred_element_type=jnp.float32).astype(jnp.bfloat16)
    incoming = lax.all_to_all(
        outgoing.reshape(st_count, slot_depth, pass_len, pair_cols),
        ST,
        split_axis=0,
        concat_axis=0,
        tiled=True,
    )
    request_kv = incoming.reshape(slot_total, pass_len, pair_cols)[slot_index]
    block_kv = request_kv.reshape(blocks, PB * pass_len, pair_cols)
    key_rows = block_kv[:, :, :head_cols].reshape(blocks, PB * pass_len, head_count, HD)
    value_rows = block_kv[:, :, head_cols:].reshape(blocks, PB * pass_len, head_count, HD)
    query_rows = queries.reshape(blocks, BLK, head_count, HD)
    score_scale = HD ** (-0.5)
    scores = (
        jnp.einsum("nqhd,nkhd->nhqk", query_rows, key_rows, preferred_element_type=jnp.float32)
        * score_scale
    )
    shifted = jnp.exp(scores - jnp.max(scores, axis=-1, keepdims=True))
    prob_rows = shifted / jnp.sum(shifted, axis=-1, keepdims=True)
    probs_low = prob_rows.astype(jnp.bfloat16)
    attended = jnp.einsum(
        "nhqk,nkhd->nqhd", probs_low, value_rows, preferred_element_type=jnp.float32
    ).reshape(tok_rows, head_cols)
    gate_vals = gate_pre.astype(jnp.float32)
    sigmoid_vals = jax.nn.sigmoid(gate_vals)
    mem_grad = d_mem.astype(jnp.float32)
    attended_grad = (gate_vals * sigmoid_vals * mem_grad).astype(jnp.bfloat16)
    gate_grad = (
        mem_grad * attended * sigmoid_vals * (1.0 + gate_vals * (1.0 - sigmoid_vals))
    ).astype(jnp.bfloat16)
    attended_four = attended_grad.reshape(blocks, BLK, head_count, HD)
    prob_grad = jnp.einsum(
        "nqhd,nkhd->nhqk", attended_four, value_rows, preferred_element_type=jnp.float32
    )
    score_grad = (
        score_scale
        * prob_rows
        * (prob_grad - jnp.sum(prob_rows * prob_grad, axis=-1, keepdims=True))
    ).astype(jnp.bfloat16)
    query_grad = (
        jnp.einsum("nhqk,nkhd->nqhd", score_grad, key_rows, preferred_element_type=jnp.float32)
        .astype(jnp.bfloat16)
        .reshape(tok_rows, head_cols)
    )
    key_grad = jnp.einsum(
        "nhqk,nqhd->nkhd", score_grad, query_rows, preferred_element_type=jnp.float32
    )
    value_grad = jnp.einsum(
        "nhqk,nqhd->nkhd", probs_low, attended_four, preferred_element_type=jnp.float32
    )
    request_grads = jnp.concatenate(
        [
            key_grad.reshape(blocks, PB * pass_len, head_cols),
            value_grad.reshape(blocks, PB * pass_len, head_cols),
        ],
        axis=2,
    )
    request_grads = request_grads.astype(jnp.bfloat16).reshape(requests, pass_len * pair_cols)
    returning = jnp.dot(
        slot_hot.T.astype(jnp.bfloat16), request_grads, preferred_element_type=jnp.float32
    ).astype(jnp.bfloat16)
    arrived = lax.all_to_all(
        returning.reshape(st_count, slot_depth, pass_len, pair_cols),
        ST,
        split_axis=0,
        concat_axis=0,
        tiled=True,
    )
    pass_grad = jnp.dot(
        pick_rows.T,
        arrived.reshape(slot_total, pass_len * pair_cols),
        preferred_element_type=jnp.float32,
    )
    pass_low = pass_grad.astype(jnp.bfloat16).reshape(passages, pass_len, pair_cols)
    key_sums = pass_low[:, :, :head_cols].reshape(passages * pass_len, head_cols)
    d_wkey = summed_rows_2(
        jnp.einsum("rc,rh->ch", flat_rows, key_sums, preferred_element_type=jnp.float32),
        ST,
        (1, 0),
        0,
    )
    partial_value = pass_low.reshape(
        passages // tp_count * lax.axis_size("tp") * pass_len, pair_cols
    )
    d_store = summed_on_arrival(
        jnp.einsum("rc,dc->rd", partial_value, weight_kv, preferred_element_type=jnp.float32)
        .reshape(passages // tp_count * lax.axis_size("tp"), pass_len, model_width)
        .astype(jnp.bfloat16),
        "tp",
        0,
    ).astype(jnp.bfloat16)
    grad_both = jnp.concatenate([query_grad, gate_grad], axis=1)
    weight_both = jnp.concatenate([w_query, w_gate], axis=1)
    partial_value = grad_both
    d_tokens = summed_on_arrival(
        jnp.einsum(
            "rc,dc->rd", partial_value, weight_both, preferred_element_type=jnp.float32
        ).astype(jnp.bfloat16),
        "tp",
        0,
    ).astype(jnp.bfloat16)
    return (d_tokens, d_store, d_wkey)


def solution(mesh):
    finer = Mesh(
        mesh.devices.reshape(mesh.shape["grp"], 16, 2, mesh.shape["tp"]),
        ("grp", "st_0", "st_1", "tp"),
    )
    in_specs = (
        P(GRP_ST, None),
        P(ST, None, "tp"),
        P(GRP_ST, "tp"),
        P(GRP_ST, "tp"),
        P(None, "tp"),
        P(None, "tp"),
        P(None, "tp"),
        P(None, "tp"),
        P(GRP_ST, "tp"),
    )
    out_specs = (P(GRP_ST_TP, None), P(GRP_ST_TP, None, None), P(GRP_ST, "tp"))
    return jax.shard_map(local, mesh=finer, in_specs=in_specs, out_specs=out_specs, check_vma=False)
```

profile of v0, /device:TPU:33, one launch (start us, length us, event | category | flops | bytes accessed | tf_op | source)
XLA Modules:
  0.0 637.7 jit_solution(13220018644907863382)
XLA Ops:
  10.0 25.5 %all-to-all-start = ((s32[32,1,2]{2,1,0:T(1,128)}), s32[32,1,2]{2,1,0:T(1,128)S(1)}, u32[]{:S(2)}, u32[]{:S(2)}) async-start(s32[32,1,2]{2,1,0:T(1,128)} %bitcast), calls=%async_computation | async-start | bytes 32768 | tf_op jit(solution)/shard_map/all_to_all | solution.py:64
  38.8 8.1 %all-to-all-done = s32[32,1,2]{2,1,0:T(1,128)S(1)} async-done(((s32[32,1,2]{2,1,0:T(1,128)}), s32[32,1,2]{2,1,0:T(1,128)S(1)}, u32[]{:S(2)}, u32[]{:S(2)}) %all-to-all-start) | async-done | bytes 288 | tf_op jit(solution)/shard_map/all_to_all | solution.py:64
  48.3 30.3 %all-gather.2.cloned.1.call-done = bf16[16,64,2048]{2,1,0:T(8,128)(2,1)} async-done(((bf16[16,64,512]{2,1,0:T(8,128)(2,1)}), bf16[16,64,2048]{2,1,0:T(8,128)(2,1)}) %all-gather.2.cloned.1.call-update) | async-done | bytes 4194320 | tf_op jit(solution)/shard_map/all_gather | solution.py:66
  78.6 5.2 fusion.6
  86.2 3.6 copy.87
  89.7 13.3 %all-to-all-start.1 = ((bf16[32,2,64,512]{3,2,1,0:T(8,128)(2,1)}), bf16[32,2,64,512]{3,2,1,0:T(8,128)(2,1)}, u32[]{:S(2)}, u32[]{:S(2)}) async-start(bf16[32,2,64,512]{3,2,1,0:T(8,128)(2,1)} %bitcast.76), calls=%async_computation.1 | async-start | bytes 8388608 | tf_op jit(solution)/shard_map/all_to_all | solution.py:74
  103.1 183.1 %all-to-all-done.1 = bf16[32,2,64,512]{3,2,1,0:T(8,128)(2,1)} async-done(((bf16[32,2,64,512]{3,2,1,0:T(8,128)(2,1)}), bf16[32,2,64,512]{3,2,1,0:T(8,128)(2,1)}, u32[]{:S(2)}, u32[]{:S(2)}) %all-to-all-start.1) | async-done | bytes 4194336 | tf_op jit(solution)/shard_map/all_to_all | solution.py:74
  291.9 3.1 fusion.21
  295.0 2.9 fusion.10
  298.0 3.3 fusion.7
  306.8 2.9 convert_element_type.78
  311.1 3.5 copy.88
  314.6 10.8 %all-to-all-start.3 = ((bf16[32,2,64,512]{3,2,1,0:T(8,128)(2,1)}), bf16[32,2,64,512]{3,2,1,0:T(8,128)(2,1)}, u32[]{:S(2)}, u32[]{:S(2)}) async-start(bf16[32,2,64,512]{3,2,1,0:T(8,128)(2,1)} %bitcast.77), calls=%async_computation.3 | async-start | bytes 8388608 | tf_op jit(solution)/shard_map/all_to_all | solution.py:135
  326.8 5.6 convolution_convert_fusion.4
  332.4 176.2 %all-to-all-done.3 = bf16[32,2,64,512]{3,2,1,0:T(8,128)(2,1)} async-done(((bf16[32,2,64,512]{3,2,1,0:T(8,128)(2,1)}), bf16[32,2,64,512]{3,2,1,0:T(8,128)(2,1)}, u32[]{:S(2)}, u32[]{:S(2)}) %all-to-all-start.3) | async-done | bytes 4194336 | tf_op jit(solution)/shard_map/all_to_all | solution.py:135
  508.5 4.9 all-to-all-start.2
  513.8 4.7 copy.89
  528.3 5.9 convolution_convert_fusion.3
  534.2 27.2 %all-to-all-done.2 = bf16[4,256,2048]{2,1,0:T(8,128)(2,1)} async-done(((bf16[4,256,2048]{2,1,0:T(8,128)(2,1)}), bf16[4,256,2048]{2,1,0:T(8,128)(2,1)}, u32[]{:S(2)}, u32[]{:S(2)}) %all-to-all-start.2) | async-done | bytes 4194336 | tf_op jit(solution)/shard_map/all_to_all | solution.py:37
  561.3 5.0 all-to-all-start.4
  567.2 4.3 reduce_sum.54
  571.5 41.9 %all-to-all-done.4 = bf16[4,4,64,2048]{3,2,1,0:T(8,128)(2,1)} async-done(((bf16[4,4,64,2048]{3,2,1,0:T(8,128)(2,1)}), bf16[4,4,64,2048]{3,2,1,0:T(8,128)(2,1)}, u32[]{:S(2)}, u32[]{:S(2)}) %all-to-all-start.4) | async-done | bytes 4194336 | tf_op jit(solution)/shard_map/all_to_all | solution.py:37
  613.4 4.3 reduce_sum.55
  617.7 13.5 %reduce-scatter.5.cloned.1.call-done = f32[1,64,256]{2,1,0:T(8,128)} async-done(((f32[16,64,256]{2,1,0:T(8,128)}), f32[1,64,256]{2,1,0:T(8,128)}) %reduce-scatter.5.cloned.1.call-update) | async-done | bytes 65552 | tf_op jit(solution)/shard_map/reduce_scatter | solution.py:21
  (72 shorter events, 34.6 us)
Async XLA Ops:
  7.2 281.9 %copy-start = (bf16[1024,256]{1,0:T(8,128)(2,1)S(1)}, bf16[1024,256]{1,0:T(8,128)(2,1)}, u32[]{:S(2)}) copy-start(bf16[1024,256]{1,0:T(8,128)(2,1)} %param.11) | copy-start | bytes 1572868
  7.2 30.6 %copy-start.6 = (bf16[2048,256]{1,0:T(8,128)(2,1)S(1)}, bf16[2048,256]{1,0:T(8,128)(2,1)}, u32[]{:S(2)}) copy-start(bf16[2048,256]{1,0:T(8,128)(2,1)} %param.16) | copy-start | bytes 3145732
  7.2 71.4 %all-gather.2.cloned.1.call-start = ((), (), s32[]{:S(2)}) async-start(), calls=%async_computation.7 | async-start | bytes 5242880 | tf_op jit(solution)/shard_map/all_gather | solution.py:66
  10.0 37.0 %all-to-all-start = ((s32[32,1,2]{2,1,0:T(1,128)}), s32[32,1,2]{2,1,0:T(1,128)S(1)}, u32[]{:S(2)}, u32[]{:S(2)}) async-start(s32[32,1,2]{2,1,0:T(1,128)} %bitcast), calls=%async_computation | async-start | bytes 32768 | tf_op jit(solution)/shard_map/all_to_all | solution.py:64
  89.7 196.5 %all-to-all-start.1 = ((bf16[32,2,64,512]{3,2,1,0:T(8,128)(2,1)}), bf16[32,2,64,512]{3,2,1,0:T(8,128)(2,1)}, u32[]{:S(2)}, u32[]{:S(2)}) async-start(bf16[32,2,64,512]{3,2,1,0:T(8,128)(2,1)} %bitcast.76), calls=%async_computation.1 | async-start | bytes 8388608 | tf_op jit(solution)/shard_map/all_to_all | solution.py:74
  289.1 12.2 %copy-start.2 = (bf16[32,64,512]{2,1,0:T(8,128)(2,1)}, bf16[32,64,512]{2,1,0:T(8,128)(2,1)S(1)}, u32[]{:S(2)}) copy-start(bf16[32,64,512]{2,1,0:T(8,128)(2,1)S(1)} %gather_fusion) | copy-start | bytes 6291460
  289.5 1.2 copy-start.5
  291.9 3.1 copy-start.10
  298.0 3.3 copy-start.12
  301.2 1.8 copy-start.4
  303.0 1.2 copy-start.9
  314.6 10.8 %copy-start.3 = (bf16[32,64,512]{2,1,0:T(8,128)(2,1)S(1)}, bf16[32,64,512]{2,1,0:T(8,128)(2,1)}, u32[]{:S(2)}) copy-start(bf16[32,64,512]{2,1,0:T(8,128)(2,1)} %copy-done.2) | copy-start | bytes 6291460
  314.6 193.9 %all-to-all-start.3 = ((bf16[32,2,64,512]{3,2,1,0:T(8,128)(2,1)}), bf16[32,2,64,512]{3,2,1,0:T(8,128)(2,1)}, u32[]{:S(2)}, u32[]{:S(2)}) async-start(bf16[32,2,64,512]{3,2,1,0:T(8,128)(2,1)} %bitcast.77), calls=%async_computation.3 | async-start | bytes 8388608 | tf_op jit(solution)/shard_map/all_to_all | solution.py:135
  325.4 1.0 copy-start.11
  325.4 1.4 copy-start.14
  508.5 52.8 %all-to-all-start.2 = ((bf16[4,256,2048]{2,1,0:T(8,128)(2,1)}), bf16[4,256,2048]{2,1,0:T(8,128)(2,1)}, u32[]{:S(2)}, u32[]{:S(2)}) async-start(bf16[4,256,2048]{2,1,0:T(8,128)(2,1)} %bitcast.87), calls=%async_computation.2 | async-start | bytes 8388608 | tf_op jit(solution)/shard_map/all_to_all | solution.py:37
  513.5 53.0 %reduce-scatter.3.cloned.1.call-start = ((), (), s32[]{:S(2)}) async-start(), calls=%async_computation.8 | async-start | bytes 3145728 | tf_op jit(solution)/shard_map/reduce_scatter | solution.py:21
  518.5 2.5 copy-start.13
  519.6 1.0 copy-start.7
  527.1 1.2 copy-start.8
  561.3 52.0 %all-to-all-start.4 = ((bf16[4,4,64,2048]{3,2,1,0:T(8,128)(2,1)}), bf16[4,4,64,2048]{3,2,1,0:T(8,128)(2,1)}, u32[]{:S(2)}, u32[]{:S(2)}) async-start(bf16[4,4,64,2048]{3,2,1,0:T(8,128)(2,1)} %bitcast.88), calls=%async_computation.4 | async-start | bytes 8388608 | tf_op jit(solution)/shard_map/all_to_all | solution.py:37
  566.4 64.8 %reduce-scatter.5.cloned.1.call-start = ((), (), s32[]{:S(2)}) async-start(), calls=%async_computation.9 | async-start | bytes 1114112 | tf_op jit(solution)/shard_map/reduce_scatter | solution.py:21
  567.2 64.0 %copy-start.1 = (bf16[1024,256]{1,0:T(8,128)(2,1)S(1)}, bf16[1024,256]{1,0:T(8,128)(2,1)}, u32[]{:S(2)}) copy-start(bf16[1024,256]{1,0:T(8,128)(2,1)} %param.11) | copy-start | bytes 1572868
Sparse Core Ops, SparseCore 0:
  9.9 68.6 all-gather.1
  527.2 18.3 reduce-scatter.2
  570.3 60.7 reduce-scatter.4
where the time goes:
time: 647 us; the launch traced here: 638 us
  waiting for transfers between devices  482 us (74%)
  starting transfers between devices  59.9 us (9%)
  local copies, waits for them, and re-layouts  35.7 us (6%)
  matrix products  32.1 us (5%)
  other arithmetic  14.1 us (2%)
  between operations  14.1 us (2%)
    all_to_all x1, waiting for transfers between devices, local(): lax.all_to_all(outgoing.reshape(st_count, slot_depth, pass_len, pair_cols...  183 us
    all_to_all x1, waiting for transfers between devices, local(): lax.all_to_all(returning.reshape(st_count, slot_depth, pass_len, pair_col...  176 us
    all_to_all x2, waiting for transfers between devices, summed_on_arrival(): lax.all_to_all(in_blocks(array, dim, devices), axis, 0, 0, tiled=True)  69.1 us
    all_gather x1, waiting for transfers between devices, local(): gathered = lax.all_gather(store, 'tp', axis=2, tiled=True)  30.3 us
    all_to_all x1, starting transfers between devices, local(): lax.all_to_all(wanted, ST, split_axis=0, concat_axis=0, tiled=True)  25.5 us
    unnamed x36, local copies, waits for them, and re-layouts  20.5 us
    reduce_scatter x2, waiting for transfers between devices, sum_in_order(): tiles = lax.psum_scatter(tiles, axes[k], scatter_dimension=0, tiled=True)  13.5 us
    all_to_all x1, starting transfers between devices, local(): lax.all_to_all(outgoing.reshape(st_count, slot_depth, pass_len, pair_cols...  13.3 us
  transfers between devices with their start and end apart: 8, of which 7 were waited for; matrix products, arithmetic and copies ran while one was open for 6% of the time, Pallas kernels for 0%

commit v1 on v0

--- a/solution.py
+++ b/solution.py
@@ -1,15 +1,359 @@
+import functools
+
 import jax
 import jax.numpy as jnp
 from jax import lax
+from jax.experimental import pallas as pl
+from jax.experimental.pallas import tpu as pltpu
 from jax.sharding import Mesh
 from jax.sharding import PartitionSpec as P
 
 HD = 256
 BLK = 128
 PB = 4
+MOST = 2
+CHUNK = 4
 ST = ("st_0", "st_1")
 GRP_ST = ("grp", "st_0", "st_1")
 GRP_ST_TP = ("grp", "st_0", "st_1", "tp")
+MESH_ID = pl.DeviceIdType.MESH
+VMEM_SPEC = pl.BlockSpec(memory_space=pltpu.VMEM)
+SMEM_SPEC = pl.BlockSpec(memory_space=pltpu.SMEM)
+ANY_SPEC = pl.BlockSpec(memory_space=pl.ANY)
+
+
+class Plan:
+    def __init__(self, ring, passages):
+        self.ring = ring
+        self.passages = passages
+        self.reach = (ring // 2, (ring - 1) // 2)
+        self.sizes = [
+            {t: min(passages, 2 * MOST * (reach - t + 1)) for t in range(1, reach + 1)}
+            for reach in self.reach
+        ]
+        self.base = [{}, {}]
+        at = passages
+        for d in range(2):
+            for t in range(1, self.reach[d] + 1):
+                self.base[d][t] = at
+                at += self.sizes[d][t]
+        self.slots = at
+
+    def steps(self, down=False):
+        order = range(1, max(self.reach) + 1)
+        for t in reversed(order) if down else order:
+            for first in range(0, self.passages, CHUNK):
+                for d in range(2):
+                    if t <= self.reach[d] and first < self.sizes[d][t]:
+                        yield d, t, first, min(CHUNK, self.sizes[d][t] - first)
+
+
+def places():
+    z, k = lax.axis_index("st_0"), lax.axis_index("st_1")
+    ring = lax.axis_size("st_0")
+    g, x = lax.axis_index("grp"), lax.axis_index("tp")
+    turn = 1 - 2 * k
+    ahead = lax.rem(z + turn + ring, ring)
+    behind = lax.rem(z - turn + ring, ring)
+    return (g, ahead, k, x), (g, behind, k, x), (g, z, 1 - k, x)
+
+
+def greet(*devices):
+    barrier = pltpu.get_barrier_semaphore()
+    for device in devices:
+        pl.semaphore_signal(barrier, inc=1, device_id=device, device_id_type=MESH_ID)
+    pl.semaphore_wait(barrier, len(devices))
+
+
+def cast_kernel(
+    plan, order_ref, where_ref, kv_ref, out_ref, buf, first_buf, send_sem, recv_sem, give_sem, take_sem
+):
+    ahead, behind, twin = places()
+    count = plan.passages
+
+    @pl.loop(0, count)
+    def _(j):
+        buf[j] = kv_ref[j]
+        first_buf[j] = kv_ref[order_ref[j]]
+        first_buf[count + j] = kv_ref[order_ref[count + j]]
+
+    greet(ahead, behind, twin)
+    copies = {}
+    gifts = []
+
+    def give(n, src, at, size):
+        gift = pltpu.make_async_remote_copy(
+            src_ref=src,
+            dst_ref=buf.at[pl.ds(plan.slots + at, size)],
+            send_sem=give_sem.at[n],
+            recv_sem=take_sem.at[n],
+            device_id=twin,
+            device_id_type=MESH_ID,
+        )
+        gift.start()
+        gifts.append(gift)
+
+    def send(n, d, t, first, size):
+        if t == 1:
+            src = first_buf.at[pl.ds(d * count + first, size)]
+        else:
+            src = buf.at[pl.ds(plan.base[d][t - 1] + first, size)]
+        copy = pltpu.make_async_remote_copy(
+            src_ref=src,
+            dst_ref=buf.at[pl.ds(plan.base[d][t] + first, size)],
+            send_sem=send_sem.at[n],
+            recv_sem=recv_sem.at[n],
+            device_id=(ahead, behind)[d],
+            device_id_type=MESH_ID,
+        )
+        copy.start()
+        copies[d, t, first] = copy
+
+    steps = list(plan.steps())
+    number = {(d, t, first): n for n, (d, t, first, _) in enumerate(steps)}
+    extent = {(d, t, first): size for d, t, first, size in steps}
+    for d, t, first, size in steps:
+        if t == 1:
+            send(number[d, t, first], d, t, first, size)
+    give(len(steps), kv_ref, 0, count)
+    for n, (d, t, first, size) in enumerate(steps):
+        copies[d, t, first].wait_recv()
+        if (d, t + 1, first) in number:
+            send(number[d, t + 1, first], d, t + 1, first, extent[d, t + 1, first])
+        at = plan.base[d][t] + first
+        give(n, buf.at[pl.ds(at, size)], at, size)
+    for gift in gifts:
+        gift.wait_recv()
+
+    @pl.loop(0, out_ref.shape[0])
+    def _(r):
+        out_ref[r] = buf[where_ref[r]]
+
+    for gift in gifts:
+        gift.wait_send()
+    for copy in copies.values():
+        copy.wait_send()
+
+
+def cast_rows(plan, order, where, kv):
+    count, rows, cols = kv.shape
+    steps = len(list(plan.steps()))
+    return pl.pallas_call(
+        functools.partial(cast_kernel, plan),
+        out_shape=jax.ShapeDtypeStruct((where.shape[0], rows, cols), kv.dtype),
+        in_specs=[SMEM_SPEC, SMEM_SPEC, VMEM_SPEC],
+        out_specs=VMEM_SPEC,
+        scratch_shapes=[
+            pltpu.VMEM((2 * plan.slots, rows, cols), kv.dtype),
+            pltpu.VMEM((2 * count, rows, cols), kv.dtype),
+            pltpu.SemaphoreType.DMA((steps,)),
+            pltpu.SemaphoreType.DMA((steps,)),
+            pltpu.SemaphoreType.DMA((steps + 1,)),
+            pltpu.SemaphoreType.DMA((steps + 1,)),
+        ],
+        compiler_params=pltpu.CompilerParams(
+            collective_id=0, has_side_effects=True, vmem_limit_bytes=60 * 1024 * 1024
+        ),
+        name="cast_rows",
+    )(order, where, kv)
+
+
+def fold_kernel(
+    plan,
+    table_ref,
+    rank_ref,
+    grads_ref,
+    out_ref,
+    held,
+    here,
+    sums,
+    send_sem,
+    recv_sem,
+    give_sem,
+    take_sem,
+    load_sem,
+):
+    ahead, behind, twin = places()
+    count = plan.passages
+    own = grads_ref.shape[0]
+    readers = 2 * MOST
+
+    load = pltpu.make_async_copy(grads_ref, held.at[pl.ds(0, own)], load_sem)
+    load.start()
+    held[2 * own] = jnp.zeros_like(held[2 * own])
+    greet(ahead, behind, twin)
+    gift = pltpu.make_async_remote_copy(
+        src_ref=grads_ref,
+        dst_ref=held.at[pl.ds(own, own)],
+        send_sem=give_sem,
+        recv_sem=take_sem,
+        device_id=twin,
+        device_id_type=MESH_ID,
+    )
+    gift.start()
+    load.wait()
+    gift.wait_recv()
+
+    def readers_sum(slot):
+        total = held[table_ref[slot * readers]].astype(jnp.float32)
+        for q in range(1, readers):
+            total += held[table_ref[slot * readers + q]].astype(jnp.float32)
+        return total
+
+    copies = {}
+    steps = list(plan.steps(down=True))
+    number = {(d, t, first): n for n, (d, t, first, _) in enumerate(steps)}
+    for n, (d, t, first, size) in enumerate(steps):
+        more = (d, t + 1, first) in number
+        at = plan.base[d][t] + first
+        if more:
+            copies[d, t + 1, first].wait_recv()
+            far_at = plan.base[d][t + 1] + first
+            far_size = plan.sizes[d][t + 1] - first
+
+            @pl.loop(0, min(far_size, size))
+            def _(j):
+                total = readers_sum(at + j) + here[far_at - count + j].astype(jnp.float32)
+                sums[at - count + j] = total.astype(sums.dtype)
+
+            begin = min(far_size, size)
+        else:
+            begin = 0
+        if begin < size:
+
+            @pl.loop(begin, size)
+            def _(j):
+                sums[at - count + j] = readers_sum(at + j).astype(sums.dtype)
+
+        copy = pltpu.make_async_remote_copy(
+            src_ref=sums.at[pl.ds(at - count, size)],
+            dst_ref=here.at[pl.ds(at - count, size)],
+            send_sem=send_sem.at[n],
+            recv_sem=recv_sem.at[n],
+            device_id=(behind, ahead)[d],
+            device_id_type=MESH_ID,
+        )
+        copy.start()
+        copies[d, t, first] = copy
+    for (d, t, first), copy in copies.items():
+        if t == 1:
+            copy.wait_recv()
+
+    @pl.loop(0, count)
+    def _(p):
+        total = readers_sum(p)
+        for d in range(2):
+            total += here[plan.base[d][1] - count + rank_ref[d * count + p]].astype(jnp.float32)
+        out_ref[p] = total.astype(out_ref.dtype)
+
+    gift.wait_send()
+    for copy in copies.values():
+        copy.wait_send()
+
+
+def fold_rows(plan, table, rank, grads):
+    own, rows, cols = grads.shape
+    steps = len(list(plan.steps()))
+    count = plan.passages
+    return pl.pallas_call(
+        functools.partial(fold_kernel, plan),
+        out_shape=jax.ShapeDtypeStruct((count, rows, cols), grads.dtype),
+        in_specs=[SMEM_SPEC, SMEM_SPEC, ANY_SPEC],
+        out_specs=VMEM_SPEC,
+        scratch_shapes=[
+            pltpu.VMEM((2 * own + 1, rows, cols), grads.dtype),
+            pltpu.VMEM((plan.slots - count, rows, cols), grads.dtype),
+            pltpu.VMEM((plan.slots - count, rows, cols), grads.dtype),
+            pltpu.SemaphoreType.DMA((steps,)),
+            pltpu.SemaphoreType.DMA((steps,)),
+            pltpu.SemaphoreType.DMA,
+            pltpu.SemaphoreType.DMA,
+            pltpu.SemaphoreType.DMA,
+        ],
+        compiler_params=pltpu.CompilerParams(
+            collective_id=1, has_side_effects=True, vmem_limit_bytes=60 * 1024 * 1024
+        ),
+        name="fold_rows",
+    )(table, rank, grads)
+
+
+def by_value(plan, d, step):
+    total = jnp.zeros_like(step)
+    for t, at in plan.base[d].items():
+        total = total + jnp.where(step == t, at, 0)
+    return total
+
+
+def routes(plan, pass_ids):
+    count, ring = plan.passages, plan.ring
+    me_z, me_k = lax.axis_index("st_0"), lax.axis_index("st_1")
+    ids = lax.all_gather(pass_ids.reshape(-1), ST, axis=0, tiled=False)
+    devices, requests = ids.shape
+    total = devices * count
+    every = jnp.arange(total, dtype=jnp.int32)
+    owner = ids // count
+    owner_z, owner_k = owner // 2, owner % 2
+    reader_z = (jnp.arange(devices, dtype=jnp.int32) // 2)[:, None]
+    away = jnp.mod((1 - 2 * owner_k) * (reader_z - owner_z), ring)
+    reach = plan.reach[0]
+    steps = (
+        jnp.where((away >= 1) & (away <= reach), away, 0),
+        jnp.where(away > reach, ring - away, 0),
+    )
+    hot = ids.reshape(-1)[:, None] == every[None, :]
+    ranks = []
+    slots = (every % count,)
+    for d in range(2):
+        far = jnp.max(jnp.where(hot, steps[d].reshape(-1)[:, None], 0), axis=0)
+        far = far.reshape(devices, count)
+        place = jnp.arange(count, dtype=jnp.int32)
+        before = (far[:, None, :] > far[:, :, None]) | (
+            (far[:, None, :] == far[:, :, None]) & (place[None, None, :] < place[None, :, None])
+        )
+        ranks.append(jnp.sum(before.astype(jnp.int32), axis=2))
+
+    def of_chip(array):
+        return lax.dynamic_slice_in_dim(array, me_z * 2, 2, axis=0)
+
+    mine = lax.dynamic_slice_in_dim
+    me = me_z * 2 + me_k
+    rank_me = jnp.concatenate([mine(r, me, 1, axis=0).reshape(-1) for r in ranks])
+    order = jnp.concatenate(
+        [
+            jnp.sum(
+                jnp.where(
+                    mine(r, me, 1, axis=0).reshape(-1)[None, :] == jnp.arange(count, dtype=jnp.int32)[:, None],
+                    jnp.arange(count, dtype=jnp.int32)[None, :],
+                    0,
+                ),
+                axis=1,
+            )
+            for r in ranks
+        ]
+    ).astype(jnp.int32)
+    chip_ids = of_chip(ids).reshape(-1)
+    chip_steps = [of_chip(s).reshape(-1) for s in steps]
+    chip_k = of_chip(owner_k).reshape(-1)
+    chip_hot = chip_ids[:, None] == every[None, :]
+    slot = chip_ids % count
+    for d in range(2):
+        rank = jnp.sum(jnp.where(chip_hot, ranks[d].reshape(-1)[None, :], 0), axis=1)
+        slot = jnp.where(chip_steps[d] > 0, by_value(plan, d, chip_steps[d]) + rank, slot)
+    where = slot + jnp.where(chip_k == me_k, 0, plan.slots)
+    where = mine(where, me_k * requests, requests, axis=0)
+    first = jnp.where(chip_k == me_k, slot, -1).reshape(2, requests)
+    first = jnp.where(me_k == 0, first, first[::-1]).reshape(-1)
+    at_slot = first[:, None] == jnp.arange(plan.slots, dtype=jnp.int32)[None, :]
+    turn = jnp.cumsum(at_slot.astype(jnp.int32), axis=0)
+    number = jnp.arange(2 * requests, dtype=jnp.int32)[:, None]
+    table = jnp.stack(
+        [
+            jnp.min(jnp.where(at_slot & (turn == q + 1), number, 2 * requests), axis=0)
+            for q in range(2 * MOST)
+        ],
+        axis=1,
+    ).reshape(-1)
+    return order, rank_me.astype(jnp.int32), where.astype(jnp.int32), table.astype(jnp.int32)
 
 
 def sum_in_order(tiles, axes, order):
@@ -39,7 +383,6 @@
 
 
 def local(pass_ids, store, queries, gate_pre, w_query, w_gate, w_key, w_value, d_mem):
-    st_count = lax.axis_size(ST)
     tp_count = lax.axis_size("tp")
     tok_rows, head_cols = queries.shape
     head_count = head_cols // HD
@@ -48,37 +391,15 @@
     pass_len = store.shape[1]
     model_width = w_key.shape[0]
     requests = blocks * PB
-    slot_depth = max(2, requests // st_count)
-    slot_total = st_count * slot_depth
     pair_cols = 2 * head_cols
-    request_ids = pass_ids.reshape(-1)
-    owners = request_ids // passages
-    within = request_ids % passages
-    owner_hot = (owners[:, None] == jnp.arange(st_count, dtype=jnp.int32)[None, :]).astype(
-        jnp.int32
-    )
-    ranking = jnp.sum(jnp.cumsum(owner_hot, axis=0) * owner_hot, axis=1) - 1
-    slot_index = owners * slot_depth + ranking
-    slot_hot = slot_index[:, None] == jnp.arange(slot_total, dtype=jnp.int32)[None, :]
-    wanted = jnp.max(jnp.where(slot_hot, within[:, None], -1), axis=0).reshape(st_count, slot_depth)
-    asked_rows = lax.all_to_all(wanted, ST, split_axis=0, concat_axis=0, tiled=True).reshape(-1)
+    plan = Plan(lax.axis_size("st_0"), passages)
+    order, rank_me, where, table = routes(plan, pass_ids)
     weight_kv = jnp.concatenate([w_key, w_value], axis=1)
     gathered = lax.all_gather(store, "tp", axis=2, tiled=True)
     flat_rows = gathered.reshape(passages * pass_len, model_width)
     kv_pass = jnp.dot(flat_rows, weight_kv, preferred_element_type=jnp.float32)
-    kv_low = kv_pass.astype(jnp.bfloat16).reshape(passages, pass_len * pair_cols)
-    pick_rows = (asked_rows[:, None] == jnp.arange(passages, dtype=jnp.int32)[None, :]).astype(
-        jnp.bfloat16
-    )
-    outgoing = jnp.dot(pick_rows, kv_low, preferred_element_type=jnp.float32).astype(jnp.bfloat16)
-    incoming = lax.all_to_all(
-        outgoing.reshape(st_count, slot_depth, pass_len, pair_cols),
-        ST,
-        split_axis=0,
-        concat_axis=0,
-        tiled=True,
-    )
-    request_kv = incoming.reshape(slot_total, pass_len, pair_cols)[slot_index]
+    kv_low = kv_pass.astype(jnp.bfloat16).reshape(passages, pass_len, pair_cols)
+    request_kv = cast_rows(plan, order, where, kv_low)
     block_kv = request_kv.reshape(blocks, PB * pass_len, pair_cols)
     key_rows = block_kv[:, :, :head_cols].reshape(blocks, PB * pass_len, head_count, HD)
     value_rows = block_kv[:, :, head_cols:].reshape(blocks, PB * pass_len, head_count, HD)
@@ -128,23 +449,8 @@
         ],
         axis=2,
     )
-    request_grads = request_grads.astype(jnp.bfloat16).reshape(requests, pass_len * pair_cols)
-    returning = jnp.dot(
-        slot_hot.T.astype(jnp.bfloat16), request_grads, preferred_element_type=jnp.float32
-    ).astype(jnp.bfloat16)
-    arrived = lax.all_to_all(
-        returning.reshape(st_count, slot_depth, pass_len, pair_cols),
-        ST,
-        split_axis=0,
-        concat_axis=0,
-        tiled=True,
-    )
-    pass_grad = jnp.dot(
-        pick_rows.T,
-        arrived.reshape(slot_total, pass_len * pair_cols),
-        preferred_element_type=jnp.float32,
-    )
-    pass_low = pass_grad.astype(jnp.bfloat16).reshape(passages, pass_len, pair_cols)
+    request_grads = request_grads.astype(jnp.bfloat16).reshape(requests, pass_len, pair_cols)
+    pass_low = fold_rows(plan, table, rank_me, request_grads)
     key_sums = pass_low[:, :, :head_cols].reshape(passages * pass_len, head_cols)
     d_wkey = summed_rows_2(
         jnp.einsum("rc,rh->ch", flat_rows, key_sums, preferred_element_type=jnp.float32),
@@ -177,7 +483,7 @@
 
 def solution(mesh):
     finer = Mesh(
-        mesh.devices.reshape(mesh.shape["grp"], 16, 2, mesh.shape["tp"]),
+        mesh.devices.reshape(mesh.shape["grp"], -1, 2, mesh.shape["tp"]),
         ("grp", "st_0", "st_1", "tp"),
     )
     in_specs = (

time: 647 us -> 548 us (0.85)
  waiting for transfers between devices: 482 us -> 103 us
  Pallas kernels: 0 us -> 297 us
  blocking collectives: 0 us -> 50.4 us
  starting transfers between devices: 59.9 us -> 10.1 us
  local copies, waits for them, and re-layouts: 35.7 us -> 17.6 us
    all_to_all x3 -> x0, waiting for transfers between devices: 367 us -> none  [the longest x1 183 us: local(): lax.all_to_all(outgoing.reshape(st_count, slot_depth, pass_len, pair_cols...]
    pallas_call x0 -> x2, Pallas kernels: none -> 297 us  [the longest x1 149 us: fold_rows(): pl.pallas_call(functools.partial(fold_kernel, plan), out_shape=jax.ShapeD...]
    all_gather x0 -> x1, blocking collectives: none -> 50.4 us  [routes(): ids = lax.all_gather(pass_ids.reshape(-1), ST, axis=0, tiled=False)]
    all_to_all x3 -> x0, starting transfers between devices: 49.6 us -> none  [the longest x1 25.5 us: local(): lax.all_to_all(wanted, ST, split_axis=0, concat_axis=0, tiled=True)]
    all_gather x1, waiting for transfers between devices: 30.3 us -> 8.89 us  [local(): gathered = lax.all_gather(store, 'tp', axis=2, tiled=True)]
    unnamed x36 -> x29, local copies, waits for them, and re-layouts: 20.5 us -> 4.6 us
    all_to_all x2, waiting for transfers between devices: 69.1 us -> 82 us  [summed_on_arrival(): lax.all_to_all(in_blocks(array, dim, devices), axis, 0, 0, tiled=True)]
  transfers between devices with their start and end apart: 8 -> 5, of which waited for: 7 -> 4; matrix products, arithmetic and copies ran while one was open for 6% -> 5% of each run, Pallas kernels for 0% -> 0%
where the time goes in v1:
time: 548 us; the launch traced here: 540 us
  Pallas kernels  297 us (54%)
  waiting for transfers between devices  103 us (19%)
  blocking collectives  50.4 us (9%)
  matrix products  30.4 us (6%)
  other arithmetic  17.9 us (3%)
  local copies, waits for them, and re-layouts  17.6 us (3%)
  between operations  14 us (3%)
  starting transfers between devices  10.1 us (2%)
    pallas_call x1, Pallas kernels, fold_rows(): pl.pallas_call(functools.partial(fold_kernel, plan), out_shape=jax.ShapeD...  149 us
    pallas_call x1, Pallas kernels, cast_rows(): pl.pallas_call(functools.partial(cast_kernel, plan), out_shape=jax.ShapeD...  147 us
    all_to_all x2, waiting for transfers between devices, summed_on_arrival(): lax.all_to_all(in_blocks(array, dim, devices), axis, 0, 0, tiled=True)  82 us
    all_gather x1, blocking collectives, routes(): ids = lax.all_gather(pass_ids.reshape(-1), ST, axis=0, tiled=False)  50.4 us
  transfers between devices with their start and end apart: 5, of which 4 were waited for; matrix products, arithmetic and copies ran while one was open for 5% of the time, Pallas kernels for 0%

profile of v1, /device:TPU:33, one launch (start us, length us, event | category | flops | bytes accessed | tf_op | source)
XLA Modules:
  0.0 539.5 jit_solution(20936963277678232)
XLA Ops:
  8.9 50.4 %all-gather = s32[32,1,32]{2,1,0:T(1,128)S(1)} all-gather(s32[1,1,32]{2,1,0:T(1,128)S(1)} %reshape.267), channel_id=1, replica_groups=mesh['grp'=2,'st_0'=16,'st_1'=2,'tp'=4] {'st_0','st_1'}, dimensions={0}, use_global_device_ids=true | all-gather | bytes 4224 | tf_op jit(solution)/shard_map/all_gather | solution.py:290
  69.7 8.9 %all-gather.3.cloned.1.call-done = bf16[16,64,2048]{2,1,0:T(8,128)(2,1)} async-done(((bf16[16,64,512]{2,1,0:T(8,128)(2,1)}), bf16[16,64,2048]{2,1,0:T(8,128)(2,1)}) %all-gather.3.cloned.1.call-update) | async-done | bytes 4194320 | tf_op jit(solution)/shard_map/all_gather | solution.py:398
  78.6 5.2 fusion.6
  83.8 1.3 copy.67
  85.1 147.2 %cast_rows.1 = bf16[32,64,512]{2,1,0:T(8,128)(2,1)} custom-call(s32[32]{0:T(128)} %pad_add_fusion.1.order_ref, s32[32]{0:T(128)} %dynamic_slice.29.where_ref, bf16[16,64,512]{2,1,0:T(8,128)(2,1)} %bitcast.69), custom_call_target="tpu_custom_call" | custom-call | tf_op jit(solution)/shard_map/cast_rows/pallas_call | solution.py:141
  232.4 1.8 fusion.8
  236.3 3.1 fusion.20
  239.4 2.9 fusion.9
  242.3 3.2 convolution_convert_fusion.2
  245.5 1.8 multiply_reduce_fusion
  248.5 1.5 pad_maximum_fusion.grads_ref
  250.0 149.3 %fold_rows.1 = bf16[16,64,512]{2,1,0:T(8,128)(2,1)} custom-call(s32[832]{0:T(1024)} %reshape.255.table_ref, s32[32]{0:T(128)} %pad_add_fusion.2.rank_ref, bf16[32,64,512]{2,1,0:T(8,128)(2,1)} %pad_maximum_fusion.grads_ref), custom_call_target="tpu_custom_call" | custom-call | tf_op jit(solution)/shard_map/fold_rows/pallas_call | solution.py:258
  399.4 6.4 %convolution_convert_fusion = bf16[16,64,2048]{2,1,0:T(8,128)(2,1)} fusion(bf16[16,64,512]{2,1,0:T(8,128)(2,1)} %fold_rows.1, bf16[2048,512]{1,0:T(8,128)(2,1)} %constant_dynamic-update-slice_fusion), kind=kOutput, calls=%fused_computation.1 | convolution fusion | flops 2149580800 | bytes 7340032 | tf_op jit(solution)/shard_map/rc,dc->rd/dot_general | solution.py:465
  405.8 2.6 convolution_bitcast_fusion
  408.4 3.0 copy.73
  411.4 4.9 all-to-all-start.1
  416.4 3.2 copy.74
  421.0 5.6 %convolution_convert_fusion.1 = bf16[1024,2048]{1,0:T(8,128)(2,1)} fusion(bf16[2048,256]{1,0:T(8,128)(2,1)S(1)} %copy-done.12, bf16[2048,256]{1,0:T(8,128)(2,1)} %param.13, bf16[1024,256]{1,0:T(8,128)(2,1)S(1)} %copy-done.9, bf16[1024,256]{1,0:T(8,128)(2,1)S(1)} %bitcast.74), kind=kOutput, calls=%fused_computation.2 | convolution fusion | flops 2155872256 | bytes 7340032 | tf_op jit(solution)/shard_map/rc,dc->rd/dot_general | solution.py:475
  426.6 38.4 %all-to-all-done.1 = bf16[4,4,64,2048]{3,2,1,0:T(8,128)(2,1)} async-done(((bf16[4,4,64,2048]{3,2,1,0:T(8,128)(2,1)}), bf16[4,4,64,2048]{3,2,1,0:T(8,128)(2,1)}, u32[]{:S(2)}, u32[]{:S(2)}) %all-to-all-start.1) | async-done | bytes 4194336 | tf_op jit(solution)/shard_map/all_to_all | solution.py:381
  464.9 4.9 all-to-all-start
  470.7 4.3 reduce_sum.111
  474.9 43.6 %all-to-all-done = bf16[4,256,2048]{2,1,0:T(8,128)(2,1)} async-done(((bf16[4,256,2048]{2,1,0:T(8,128)(2,1)}), bf16[4,256,2048]{2,1,0:T(8,128)(2,1)}, u32[]{:S(2)}, u32[]{:S(2)}) %all-to-all-start) | async-done | bytes 4194336 | tf_op jit(solution)/shard_map/all_to_all | solution.py:381
  518.5 4.3 reduce_sum.108
  522.8 10.2 %reduce-scatter.5.cloned.1.call-done = f32[1,64,256]{2,1,0:T(8,128)} async-done(((f32[16,64,256]{2,1,0:T(8,128)}), f32[1,64,256]{2,1,0:T(8,128)}) %reduce-scatter.5.cloned.1.call-update) | async-done | bytes 65552 | tf_op jit(solution)/shard_map/reduce_scatter | solution.py:365
  (87 shorter events, 17.6 us)
Async XLA Ops:
  7.2 225.2 %copy-start = (bf16[1024,256]{1,0:T(8,128)(2,1)S(1)}, bf16[1024,256]{1,0:T(8,128)(2,1)}, u32[]{:S(2)}) copy-start(bf16[1024,256]{1,0:T(8,128)(2,1)} %param.11) | copy-start | bytes 1572868
  7.2 60.2 %copy-start.4 = (bf16[2048,256]{1,0:T(8,128)(2,1)S(1)}, bf16[2048,256]{1,0:T(8,128)(2,1)}, u32[]{:S(2)}) copy-start(bf16[2048,256]{1,0:T(8,128)(2,1)} %param.15) | copy-start | bytes 3145732
  7.2 61.4 %copy-start.5 = (bf16[2048,256]{1,0:T(8,128)(2,1)S(1)}, bf16[2048,256]{1,0:T(8,128)(2,1)}, u32[]{:S(2)}) copy-start(bf16[2048,256]{1,0:T(8,128)(2,1)} %param.16) | copy-start | bytes 3145732
  7.2 71.4 %all-gather.3.cloned.1.call-start = ((), (), s32[]{:S(2)}) async-start(), calls=%async_computation.4 | async-start | bytes 5242880 | tf_op jit(solution)/shard_map/all_gather | solution.py:398
  232.4 4.0 copy-start.1
  234.2 1.0 copy-start.3
  236.3 3.1 copy-start.8
  242.3 3.2 copy-start.10
  245.5 1.8 copy-start.2
  247.3 1.2 copy-start.6
  399.4 6.4 %copy-start.7 = (bf16[16,64,512]{2,1,0:T(8,128)(2,1)S(1)}, bf16[16,64,512]{2,1,0:T(8,128)(2,1)}, u32[]{:S(2)}) copy-start(bf16[16,64,512]{2,1,0:T(8,128)(2,1)} %fold_rows.1) | copy-start | bytes 3145732
  399.4 6.4 %copy-start.11 = (bf16[16,64,2048]{2,1,0:T(8,128)(2,1)S(1)}, bf16[16,64,2048]{2,1,0:T(8,128)(2,1)}, u32[]{:S(2)}) copy-start(bf16[16,64,2048]{2,1,0:T(8,128)(2,1)} %all-gather.3.cloned.1.call-done) | copy-start | bytes 12582916
  411.4 53.6 %all-to-all-start.1 = ((bf16[4,4,64,2048]{3,2,1,0:T(8,128)(2,1)}), bf16[4,4,64,2048]{3,2,1,0:T(8,128)(2,1)}, u32[]{:S(2)}, u32[]{:S(2)}) async-start(bf16[4,4,64,2048]{3,2,1,0:T(8,128)(2,1)} %bitcast.67), calls=%async_computation.1 | async-start | bytes 8388608 | tf_op jit(solution)/shard_map/all_to_all | solution.py:381
  416.3 53.6 %reduce-scatter.3.cloned.1.call-start = ((), (), s32[]{:S(2)}) async-start(), calls=%async_computation.5 | async-start | bytes 3145728 | tf_op jit(solution)/shard_map/reduce_scatter | solution.py:365
  419.6 1.0 copy-start.9
  419.6 1.4 copy-start.12
  464.9 53.6 %all-to-all-start = ((bf16[4,256,2048]{2,1,0:T(8,128)(2,1)}), bf16[4,256,2048]{2,1,0:T(8,128)(2,1)}, u32[]{:S(2)}, u32[]{:S(2)}) async-start(bf16[4,256,2048]{2,1,0:T(8,128)(2,1)} %bitcast.68), calls=%async_computation | async-start | bytes 8388608 | tf_op jit(solution)/shard_map/all_to_all | solution.py:381
  469.9 63.1 %reduce-scatter.5.cloned.1.call-start = ((), (), s32[]{:S(2)}) async-start(), calls=%async_computation.6 | async-start | bytes 1114112 | tf_op jit(solution)/shard_map/reduce_scatter | solution.py:365
Sparse Core Ops, SparseCore 0:
  9.9 68.6 all-gather.2
  419.7 17.3 reduce-scatter.2
  473.8 59.1 reduce-scatter.4

commit v2 on v0

v2 whole, which is shorter than its diff:
```python
import functools

import jax
import jax.numpy as jnp
from jax import lax
from jax.experimental import pallas as pl
from jax.experimental.pallas import tpu as pltpu
from jax.sharding import Mesh
from jax.sharding import PartitionSpec as P

HD = 256
BLK = 128
PB = 4
MOST = 2
CHUNK = 4
LIGHT = (24, 22, 22, 20, 18, 16, 12, 4)
VMEM_LIMIT = 62 * 1024 * 1024
ST = ("st_0", "st_1")
GRP_ST = ("grp", "st_0", "st_1")
GRP_ST_TP = ("grp", "st_0", "st_1", "tp")
MESH_ID = pl.DeviceIdType.MESH
VMEM_SPEC = pl.BlockSpec(memory_space=pltpu.VMEM)
SMEM_SPEC = pl.BlockSpec(memory_space=pltpu.SMEM)
ANY_SPEC = pl.BlockSpec(memory_space=pl.ANY)
F32 = jnp.float32


class Plan:
    def __init__(self, ring, passages, light=False):
        self.ring = ring
        self.passages = passages
        self.reach = ring // 2
        self.steps_of = range(1, self.reach + 1)
        per_owner = 2 * MOST
        self.layout = {
            t: min(passages, per_owner * (self.reach - t + 1))
            + min(passages, per_owner * (self.reach - t))
            for t in self.steps_of
        }
        self.sizes = dict(self.layout)
        if light:
            self.sizes = {t: min(n, LIGHT[t - 1]) for t, n in self.layout.items()}
        self.base = [{}, {}]
        at = passages
        for d in range(2):
            for t in self.steps_of:
                self.base[d][t] = at
                at += -(-self.layout[t] // 2)
        self.slots = at

    def half(self, t):
        return -(-self.sizes[t] // 2) if t <= self.reach else 0

    def steps(self, down=False):
        for t in reversed(self.steps_of) if down else self.steps_of:
            for first in range(0, self.half(t), CHUNK):
                for d in range(2):
                    yield d, t, first, min(CHUNK, self.half(t) - first)


class Place:
    def __init__(self):
        self.g, self.z, self.k, self.x = (lax.axis_index(a) for a in GRP_ST_TP)
        self.ring = lax.axis_size("st_0")
        self.tp = lax.axis_size("tp")
        self.twin = (self.g, self.z, 1 - self.k, self.x)

    def along_z(self, step):
        return (self.g, lax.rem(self.z + step + self.ring, self.ring), self.k, self.x)

    def along_x(self, step):
        return (self.g, self.z, self.k, lax.rem(self.x + step + self.tp, self.tp))


def greet(*devices):
    barrier = pltpu.get_barrier_semaphore()
    for device in devices:
        pl.semaphore_signal(barrier, inc=1, device_id=device, device_id_type=MESH_ID)
    pl.semaphore_wait(barrier, len(devices))


class Copies:
    def __init__(self, send_sem, recv_sem):
        self.send_sem, self.recv_sem = send_sem, recv_sem
        self.all = []

    def start(self, src, dst, device):
        n = len(self.all)
        copy = pltpu.make_async_remote_copy(
            src_ref=src,
            dst_ref=dst,
            send_sem=self.send_sem.at[n],
            recv_sem=self.recv_sem.at[n],
            device_id=device,
            device_id_type=MESH_ID,
        )
        copy.start()
        self.all.append(copy)
        return copy

    def wait_sends(self):
        for copy in self.all:
            copy.wait_send()


def copy_sems(count):
    return [pltpu.SemaphoreType.DMA((count,)), pltpu.SemaphoreType.DMA((count,))]


def cast_kernel(plan, weights, order_ref, where_ref, kv_ref, *refs):
    w_refs, refs = refs[:weights], refs[weights:]
    out_ref, w_outs, refs = refs[0], refs[1 : 1 + weights], refs[1 + weights :]
    buf, first_buf, home, *sems = refs
    ring_copies, gifts, w_copies = (Copies(*sems[2 * i : 2 * i + 2]) for i in range(3))
    place = Place()
    count, slots = plan.passages, plan.slots
    top = plan.half(1)

    greet(place.along_z(1), place.along_z(-1), place.along_x(1), place.along_x(-1), place.twin)
    own_gift = gifts.start(kv_ref, home.at[pl.ds(count, count)], place.twin)

    @pl.loop(0, count)
    def _(j):
        home[j] = kv_ref[j]
        buf[j] = kv_ref[j]

    own_gift.wait_recv()

    @pl.loop(0, top)
    def _(j):
        for d in range(2):
            first_buf[d * top + j] = home[order_ref[d * count + j]]

    copies = {}
    steps = list(plan.steps())
    extent = {(d, t, first): size for d, t, first, size in steps}

    def send(d, t, first):
        size = extent[d, t, first]
        if t == 1:
            src = first_buf.at[pl.ds(d * top + first, size)]
        else:
            src = buf.at[pl.ds(plan.base[d][t - 1] + first, size)]
        dst = buf.at[pl.ds(plan.base[d][t] + first, size)]
        copies[d, t, first] = ring_copies.start(src, dst, place.along_z(1 - 2 * d))

    for d, t, first, _ in steps:
        if t == 1:
            send(d, t, first)
    rows = w_refs[0].shape[0] // 2
    half = pl.ds(place.k * rows, rows)
    arrive = [[], []]
    for w_ref, w_out in zip(w_refs, w_outs):
        arrive[0].append(
            w_copies.start(w_ref.at[half], w_out.at[2, half], place.along_x(1))
        )
        arrive[1].append(
            w_copies.start(w_ref.at[half], w_out.at[0, half], place.along_x(-1))
        )
    w_gifts = []
    middle = []

    def forward_weights():
        for copy in arrive[0] + arrive[1]:
            copy.wait_recv()
        for w_out in w_outs:
            middle.append(
                w_copies.start(
                    w_out.at[2 * place.k, half],
                    w_out.at[1, half],
                    place.along_x(2 * place.k - 1),
                )
            )
            for rel in (0, 2):
                part = w_out.at[rel, half]
                w_gifts.append(w_copies.start(part, part, place.twin))

    last = None
    for d, t, first, size in steps:
        if t != last and t == plan.reach // 2 + 1:
            forward_weights()
        last = t
        copies[d, t, first].wait_recv()
        if (d, t + 1, first) in extent:
            send(d, t + 1, first)
        at = plan.base[d][t] + first
        gifts.start(buf.at[pl.ds(at, size)], buf.at[pl.ds(slots + at, size)], place.twin)
    for copy, w_out in zip(middle, w_outs):
        copy.wait_recv()
        part = w_out.at[1, half]
        w_gifts.append(w_copies.start(part, part, place.twin))
    for gift in gifts.all[1:]:
        gift.wait_recv()

    @pl.loop(0, count)
    def _(j):
        buf[slots + j] = home[count + j]

    @pl.loop(0, out_ref.shape[0])
    def _(r):
        out_ref[r] = buf[where_ref[r]]

    for gift in w_gifts:
        gift.wait_recv()
    for group in (gifts, ring_copies, w_copies):
        group.wait_sends()


def cast_rows(plan, ident, order, where, kv, weights):
    count, rows, cols = kv.shape
    steps = len(list(plan.steps()))
    others = lax.axis_size("tp") - 1
    return pl.pallas_call(
        functools.partial(cast_kernel, plan, len(weights)),
        out_shape=[jax.ShapeDtypeStruct((where.shape[0], rows, cols), kv.dtype)]
        + [jax.ShapeDtypeStruct((others, *w.shape), w.dtype) for w in weights],
        in_specs=[SMEM_SPEC, SMEM_SPEC, VMEM_SPEC] + [ANY_SPEC] * len(weights),
        out_specs=[VMEM_SPEC] + [ANY_SPEC] * len(weights),
        scratch_shapes=[
            pltpu.VMEM((2 * plan.slots, rows, cols), kv.dtype),
            pltpu.VMEM((2 * plan.half(1), rows, cols), kv.dtype),
            pltpu.VMEM((2 * count, rows, cols), kv.dtype),
        ]
        + copy_sems(steps)
        + copy_sems(steps + 1)
        + copy_sems(6 * len(weights)),
        compiler_params=pltpu.CompilerParams(
            collective_id=ident, has_side_effects=True, vmem_limit_bytes=VMEM_LIMIT
        ),
        name="cast_rows",
    )(order, where, kv, *weights)


def fold_kernel(
    plan,
    table_ref,
    final_ref,
    grads_ref,
    tokens_ref,
    out_ref,
    tokens_out,
    held,
    here,
    sums,
    load_sem,
    *sems,
):
    ring_copies, gifts, exchange = (Copies(*sems[2 * i : 2 * i + 2]) for i in range(3))
    place = Place()
    count, top = plan.passages, plan.half(1)
    own = grads_ref.shape[0]
    readers = 2 * MOST
    twin_at = plan.slots - count
    zero_at = twin_at + plan.layout[1]
    peers = [place.along_x(rel) for rel in range(1, place.tp)]

    load = pltpu.make_async_copy(grads_ref, held.at[pl.ds(0, own)], load_sem)
    load.start()
    held[2 * own] = jnp.zeros_like(held[2 * own])
    here[zero_at] = jnp.zeros_like(here[zero_at])
    greet(place.along_z(1), place.along_z(-1), place.twin, *peers)
    own_gift = gifts.start(grads_ref, held.at[pl.ds(own, own)], place.twin)
    block = tokens_out.shape[1]
    for rel, peer in enumerate(peers, 1):
        exchange.start(
            tokens_ref.at[pl.ds(peer[3] * block, block)],
            tokens_out.at[place.tp - 1 - rel],
            peer,
        )
    load.wait()
    own_gift.wait_recv()

    def readers_sum(slot):
        total = held[table_ref[slot * readers]].astype(F32)
        for q in range(1, readers):
            total += held[table_ref[slot * readers + q]].astype(F32)
        return total

    copies = {}
    steps = list(plan.steps(down=True))
    extent = {(d, t, first): size for d, t, first, size in steps}
    for d, t, first, size in steps:
        at = plan.base[d][t] + first
        begin = extent.get((d, t + 1, first), 0)
        if begin:
            copies[d, t + 1, first].wait_recv()
            far_at = plan.base[d][t + 1] + first

            @pl.loop(0, begin)
            def _(j):
                total = readers_sum(at + j) + here[far_at - count + j].astype(F32)
                sums[at - count + j] = total.astype(sums.dtype)

        if begin < size:

            @pl.loop(begin, size)
            def _(j):
                sums[at - count + j] = readers_sum(at + j).astype(sums.dtype)

        part = pl.ds(at - count, size)
        copies[d, t, first] = ring_copies.start(
            sums.at[part], here.at[part], place.along_z(2 * d - 1)
        )
    for d, t, first, size in steps:
        if t == 1:
            copies[d, t, first].wait_recv()
            src = here.at[pl.ds(plan.base[d][1] - count + first, size)]
            dst = here.at[pl.ds(twin_at + d * (plan.layout[1] // 2) + first, size)]
            gifts.start(src, dst, place.twin)
    for gift in gifts.all[1:]:
        gift.wait_recv()

    @pl.loop(0, count)
    def _(p):
        total = readers_sum(p)
        for d in range(2):
            total += here[final_ref[d * count + p]].astype(F32)
        out_ref[p] = total.astype(out_ref.dtype)

    for copy in exchange.all:
        copy.wait_recv()
    for group in (gifts, ring_copies, exchange):
        group.wait_sends()


def fold_rows(plan, ident, table, final, grads, tokens):
    own, rows, cols = grads.shape
    steps = list(plan.steps())
    ends = sum(1 for _, t, _, _ in steps if t == 1)
    count = plan.passages
    tp = lax.axis_size("tp")
    return pl.pallas_call(
        functools.partial(fold_kernel, plan),
        out_shape=[
            jax.ShapeDtypeStruct((count, rows, cols), grads.dtype),
            jax.ShapeDtypeStruct((tp - 1, tokens.shape[0] // tp, tokens.shape[1]), tokens.dtype),
        ],
        in_specs=[SMEM_SPEC, SMEM_SPEC, ANY_SPEC, ANY_SPEC],
        out_specs=[VMEM_SPEC, ANY_SPEC],
        scratch_shapes=[
            pltpu.VMEM((2 * own + 1, rows, cols), grads.dtype),
            pltpu.VMEM((plan.slots - count + plan.layout[1] + 1, rows, cols), grads.dtype),
            pltpu.VMEM((plan.slots - count, rows, cols), grads.dtype),
            pltpu.SemaphoreType.DMA,
        ]
        + copy_sems(len(steps))
        + copy_sems(1 + ends)
        + copy_sems(tp - 1),
        compiler_params=pltpu.CompilerParams(
            collective_id=ident, has_side_effects=True, vmem_limit_bytes=VMEM_LIMIT
        ),
        name="fold_rows",
    )(table, final, grads, tokens)


def project(rows_list, weight_list, out_ref, tile):
    @pl.loop(0, out_ref.shape[1] // tile)
    def _(n):
        cols = pl.ds(pl.multiple_of(n * tile, tile), tile)
        total = None
        for rows, weight in zip(rows_list, weight_list):
            term = lax.dot_general(
                rows[...], weight[cols, :], (((1,), (1,)), ((), ())), preferred_element_type=F32
            )
            total = term if total is None else total + term
        out_ref[:, cols] = total.astype(out_ref.dtype)


def tail_kernel(
    sums_ref,
    partial_ref,
    tokens_ref,
    tokens_in,
    *refs,
):
    weights, refs = refs[:8], refs[8:]
    d_tokens_ref, d_store_ref, d_wkey_ref = refs[:3]
    wbuf_t, wbuf_s, own_t, in_t, own_s, in_s, twin_buf, chip_buf, ring_buf = refs[3:12]
    load_sem, *sems = refs[12:]
    exchange, gifts, ring_copies = (Copies(*sems[2 * i : 2 * i + 2]) for i in range(3))
    place = Place()
    tp, ring = place.tp, place.ring
    peers = [place.along_x(rel) for rel in range(1, tp)]
    far = [place.along_z(rel) for rel in range(1, ring)]
    loads = []

    def load(src, dst):
        copy = pltpu.make_async_copy(src, dst, load_sem.at[len(loads)])
        copy.start()
        loads.append(copy)

    greet(place.twin, *peers, *far)
    gift = gifts.start(partial_ref.at[:, pl.ds(1 - place.k, 1)], twin_buf, place.twin)
    share = sums_ref.shape[0] // tp
    for rel, peer in enumerate(peers, 1):
        exchange.start(
            sums_ref.at[pl.ds(peer[3] * share, share)], in_s.at[tp - 1 - rel], peer
        )
    block = own_t.shape[0]
    load(tokens_ref.at[pl.ds(place.x * block, block)], own_t)
    load(tokens_in, in_t)
    load(sums_ref.at[pl.ds(place.x * share, share)], own_s)
    for wbuf, (wa, wb, wa_far, wb_far) in ((wbuf_t, weights[:4]), (wbuf_s, weights[4:])):
        load(wa, wbuf.at[0])
        load(wb, wbuf.at[1])
        load(wa_far, wbuf.at[pl.ds(2, tp - 1)])
        load(wb_far, wbuf.at[pl.ds(2 + tp - 1, tp - 1)])
    gift.wait_recv()

    @pl.loop(0, ring)
    def _(i):
        total = partial_ref[i, place.k] + twin_buf[i, 0]
        chip_buf[i] = total.astype(chip_buf.dtype)

    for rel, device in enumerate(far, 1):
        ring_copies.start(chip_buf.at[device[1]], ring_buf.at[ring - rel], device)
    for copy in loads:
        copy.wait()

    def operands(own, far_rows, wbuf):
        cols = own.shape[-1] // 2
        rows_list, weight_list = [], []
        for c in range(2):
            rows_list.append(own.at[:, pl.ds(c * cols, cols)])
            weight_list.append(wbuf.at[c])
        for rel in range(tp - 1):
            for c in range(2):
                rows_list.append(far_rows.at[rel, :, pl.ds(c * cols, cols)])
                weight_list.append(wbuf.at[2 + c * (tp - 1) + rel])
        return rows_list, weight_list

    project(*operands(own_t, in_t, wbuf_t), d_tokens_ref, 512)
    for copy in exchange.all:
        copy.wait_recv()
    rows = share * sums_ref.shape[1]
    cols = sums_ref.shape[2]
    project(
        *operands(own_s.reshape(rows, cols), in_s.reshape(tp - 1, rows, cols), wbuf_s),
        d_store_ref,
        512,
    )
    ring_copies_done = [copy.wait_recv() for copy in ring_copies.all]
    del ring_copies_done
    total = partial_ref[place.z, place.k] + twin_buf[place.z, 0]
    for rel in range(1, ring):
        total += ring_buf[rel].astype(F32)
    d_wkey_ref[...] = total
    for group in (exchange, gifts, ring_copies):
        group.wait_sends()


def tail(ident, sums, partial, tokens, tokens_in, weights):
    tp = lax.axis_size("tp")
    ring, cores, rows, cols = partial.shape
    model = weights[0].shape[0]
    head_cols = weights[0].shape[1]
    share = sums.shape[0] // tp
    low = sums.dtype
    return pl.pallas_call(
        tail_kernel,
        out_shape=[
            jax.ShapeDtypeStruct((tokens.shape[0] // tp, model), low),
            jax.ShapeDtypeStruct((share * sums.shape[1], model), low),
            jax.ShapeDtypeStruct((rows, cols), F32),
        ],
        in_specs=[ANY_SPEC, VMEM_SPEC] + [ANY_SPEC] * (2 + len(weights)),
        out_specs=[VMEM_SPEC] * 3,
        scratch_shapes=[
            pltpu.VMEM((2 * tp, model, head_cols), low),
            pltpu.VMEM((2 * tp, model, head_cols), low),
            pltpu.VMEM((tokens.shape[0] // tp, tokens.shape[1]), low),
            pltpu.VMEM(tokens_in.shape, low),
            pltpu.VMEM((share, *sums.shape[1:]), low),
            pltpu.VMEM((tp - 1, share, *sums.shape[1:]), low),
            pltpu.VMEM((ring, 1, rows, cols), F32),
            pltpu.VMEM((ring, rows, cols), low),
            pltpu.VMEM((ring, rows, cols), low),
            pltpu.SemaphoreType.DMA((3 + len(weights),)),
        ]
        + copy_sems(tp - 1)
        + copy_sems(1)
        + copy_sems(ring - 1),
        compiler_params=pltpu.CompilerParams(
            collective_id=ident, has_side_effects=True, vmem_limit_bytes=VMEM_LIMIT
        ),
        name="tail",
    )(sums, partial, tokens, tokens_in, *weights)


def first_slot(plan, d, step):
    total = jnp.zeros_like(step)
    for t, at in plan.base[d].items():
        total = total + jnp.where(step == t, at, 0)
    return total


def routes(plan, light, pass_ids):
    count, ring, slots = plan.passages, plan.ring, plan.slots
    me_z, me_k = lax.axis_index("st_0"), lax.axis_index("st_1")
    ids = lax.all_gather(pass_ids.reshape(-1), ST, axis=0, tiled=False)
    devices, requests = ids.shape
    pair = 2 * count
    every = jnp.arange(devices * count, dtype=jnp.int32)
    owner = ids // count
    owner_z, owner_k = owner // 2, owner % 2
    reader_z = (jnp.arange(devices, dtype=jnp.int32) // 2)[:, None]
    away = jnp.mod(reader_z - owner_z, ring)
    up = (2 * away < ring) | ((2 * away == ring) & (owner_k == 0))
    steps = (jnp.where(up, away, 0), jnp.where(up, 0, ring - away))
    hot = ids.reshape(-1)[:, None] == every[None, :]
    place = jnp.arange(pair, dtype=jnp.int32)
    ranks, fars = [], []
    fits = jnp.bool_(True)
    for d in range(2):
        far = jnp.max(jnp.where(hot, steps[d].reshape(-1)[:, None], 0), axis=0)
        far = far.reshape(ring, pair)
        before = (far[:, None, :] > far[:, :, None]) | (
            (far[:, None, :] == far[:, :, None]) & (place[None, None, :] < place[None, :, None])
        )
        ranks.append(jnp.sum(before.astype(jnp.int32), axis=2))
        fars.append(far)
        bounds = jnp.array([light.sizes[t] for t in light.steps_of], jnp.int32)
        dist = jnp.arange(1, plan.reach + 1, dtype=jnp.int32)
        sent = jnp.sum((far[:, None, :] >= dist[None, :, None]).astype(jnp.int32), axis=2)
        fits &= jnp.all(sent <= bounds[None, :])

    def chip(array):
        return lax.dynamic_slice_in_dim(array, me_z, 1, axis=0)[0]

    def readers(array):
        return lax.dynamic_slice_in_dim(array, me_z * 2, 2, axis=0).reshape(-1)

    at_home = place % count + jnp.where(place // count == me_k, 0, count)
    want = 2 * jnp.arange(count, dtype=jnp.int32) + me_k
    order, final = [], []
    for d in range(2):
        rank, far = chip(ranks[d]), chip(fars[d])
        order.append(jnp.sum(jnp.where(rank[None, :] == want[:, None], at_home[None, :], 0), axis=1))
        twin_at = plan.slots - count
        near = plan.base[d][1] - count
        aside = twin_at + d * (plan.layout[1] // 2)
        index = jnp.where(rank % 2 == me_k, near, aside) + rank // 2
        index = jnp.where(far > 0, index, twin_at + plan.layout[1])
        final.append(lax.dynamic_slice_in_dim(index, me_k * count, count, axis=0))
    chip_ids = readers(ids)
    chip_hot = chip_ids[:, None] == every[None, :]
    slot, core = chip_ids % count, readers(owner_k)
    for d in range(2):
        rank = jnp.sum(jnp.where(chip_hot, ranks[d].reshape(-1)[None, :], 0), axis=1)
        step = readers(steps[d] * (away > 0))
        slot = jnp.where(step > 0, first_slot(plan, d, step) + rank // 2, slot)
        core = jnp.where(step > 0, rank % 2, core)
    where = slot + jnp.where(core == me_k, 0, slots)
    where = lax.dynamic_slice_in_dim(where, me_k * requests, requests, axis=0)
    mine = jnp.where(core == me_k, slot, -1).reshape(2, requests)
    mine = jnp.where(me_k == 0, mine, mine[::-1]).reshape(-1)
    at_slot = mine[:, None] == jnp.arange(slots, dtype=jnp.int32)[None, :]
    turn = jnp.cumsum(at_slot.astype(jnp.int32), axis=0)
    number = jnp.arange(2 * requests, dtype=jnp.int32)[:, None]
    table = jnp.stack(
        [
            jnp.min(jnp.where(at_slot & (turn == q + 1), number, 2 * requests), axis=0)
            for q in range(2 * MOST)
        ],
        axis=1,
    ).reshape(-1)
    tables = (jnp.concatenate(order), where, table, jnp.concatenate(final))
    return fits, *(t.astype(jnp.int32) for t in tables)


def local(pass_ids, store, queries, gate_pre, w_query, w_gate, w_key, w_value, d_mem):
    tp_count = lax.axis_size("tp")
    ring = lax.axis_size("st_0")
    tok_rows, head_cols = queries.shape
    head_count = head_cols // HD
    blocks = tok_rows // BLK
    passages = store.shape[0]
    pass_len = store.shape[1]
    model_width = w_key.shape[0]
    requests = blocks * PB
    pair_cols = 2 * head_cols
    plan = Plan(ring, passages)
    light = Plan(ring, passages, light=True)
    fits, order, where, table, final = routes(plan, light, pass_ids)
    weight_kv = jnp.concatenate([w_key, w_value], axis=1)
    gathered = lax.all_gather(store, "tp", axis=2, tiled=True)
    flat_rows = gathered.reshape(passages * pass_len, model_width)
    kv_pass = jnp.dot(flat_rows, weight_kv, preferred_element_type=jnp.float32)
    kv_low = kv_pass.astype(jnp.bfloat16).reshape(passages, pass_len, pair_cols)
    weights = (w_query, w_gate, w_key, w_value)
    request_kv, wq_far, wg_far, wk_far, wv_far = lax.cond(
        fits,
        functools.partial(cast_rows, light, 0),
        functools.partial(cast_rows, plan, 1),
        order,
        where,
        kv_low,
        weights,
    )
    block_kv = request_kv.reshape(blocks, PB * pass_len, pair_cols)
    key_rows = block_kv[:, :, :head_cols].reshape(blocks, PB * pass_len, head_count, HD)
    value_rows = block_kv[:, :, head_cols:].reshape(blocks, PB * pass_len, head_count, HD)
    query_rows = queries.reshape(blocks, BLK, head_count, HD)
    score_scale = HD ** (-0.5)
    scores = (
        jnp.einsum("nqhd,nkhd->nhqk", query_rows, key_rows, preferred_element_type=jnp.float32)
        * score_scale
    )
    shifted = jnp.exp(scores - jnp.max(scores, axis=-1, keepdims=True))
    prob_rows = shifted / jnp.sum(shifted, axis=-1, keepdims=True)
    probs_low = prob_rows.astype(jnp.bfloat16)
    attended = jnp.einsum(
        "nhqk,nkhd->nqhd", probs_low, value_rows, preferred_element_type=jnp.float32
    ).reshape(tok_rows, head_cols)
    gate_vals = gate_pre.astype(jnp.float32)
    sigmoid_vals = jax.nn.sigmoid(gate_vals)
    mem_grad = d_mem.astype(jnp.float32)
    attended_grad = (gate_vals * sigmoid_vals * mem_grad).astype(jnp.bfloat16)
    gate_grad = (
        mem_grad * attended * sigmoid_vals * (1.0 + gate_vals * (1.0 - sigmoid_vals))
    ).astype(jnp.bfloat16)
    attended_four = attended_grad.reshape(blocks, BLK, head_count, HD)
    prob_grad = jnp.einsum(
        "nqhd,nkhd->nhqk", attended_four, value_rows, preferred_element_type=jnp.float32
    )
    score_grad = (
        score_scale
        * prob_rows
        * (prob_grad - jnp.sum(prob_rows * prob_grad, axis=-1, keepdims=True))
    ).astype(jnp.bfloat16)
    query_grad = (
        jnp.einsum("nhqk,nkhd->nqhd", score_grad, key_rows, preferred_element_type=jnp.float32)
        .astype(jnp.bfloat16)
        .reshape(tok_rows, head_cols)
    )
    key_grad = jnp.einsum(
        "nhqk,nqhd->nkhd", score_grad, query_rows, preferred_element_type=jnp.float32
    )
    value_grad = jnp.einsum(
        "nhqk,nqhd->nkhd", probs_low, attended_four, preferred_element_type=jnp.float32
    )
    request_grads = jnp.concatenate(
        [
            key_grad.reshape(blocks, PB * pass_len, head_cols),
            value_grad.reshape(blocks, PB * pass_len, head_cols),
        ],
        axis=2,
    )
    request_grads = request_grads.astype(jnp.bfloat16).reshape(requests, pass_len, pair_cols)
    token_grads = jnp.concatenate([query_grad, gate_grad], axis=1)
    pass_low, tokens_in = lax.cond(
        fits,
        functools.partial(fold_rows, light, 2),
        functools.partial(fold_rows, plan, 3),
        table,
        final,
        request_grads,
        token_grads,
    )
    key_sums = pass_low[:, :, :head_cols].reshape(passages * pass_len, head_cols)
    partial = jnp.einsum("rc,rh->ch", flat_rows, key_sums, preferred_element_type=jnp.float32)
    partial = partial.reshape(ring, 2, model_width // (2 * ring), head_cols)
    d_tokens, d_store, d_wkey = tail(
        4,
        pass_low,
        partial,
        token_grads,
        tokens_in,
        (w_query, w_gate, wq_far, wg_far, w_key, w_value, wk_far, wv_far),
    )
    return d_tokens, d_store.reshape(passages // tp_count, pass_len, model_width), d_wkey


def solution(mesh):
    finer = Mesh(
        mesh.devices.reshape(mesh.shape["grp"], -1, 2, mesh.shape["tp"]),
        ("grp", "st_0", "st_1", "tp"),
    )
    in_specs = (
        P(GRP_ST, None),
        P(ST, None, "tp"),
        P(GRP_ST, "tp"),
        P(GRP_ST, "tp"),
        P(None, "tp"),
        P(None, "tp"),
        P(None, "tp"),
        P(None, "tp"),
        P(GRP_ST, "tp"),
    )
    out_specs = (P(GRP_ST_TP, None), P(GRP_ST_TP, None, None), P(GRP_ST, "tp"))
    return jax.shard_map(local, mesh=finer, in_specs=in_specs, out_specs=out_specs, check_vma=False)
```

time: 647 us -> 395 us (0.61); the launches traced: 638 us -> 394 us
  waiting for transfers between devices: 482 us -> 10.7 us
  Pallas kernels: 0 us -> 266 us
  starting transfers between devices: 59.9 us -> 0.06 us
  blocking collectives: 0 us -> 50.4 us
  local copies, waits for them, and re-layouts: 35.7 us -> 18.3 us
  matrix products: 32.1 us -> 21 us
    all_to_all x5 -> x0, waiting for transfers between devices: 436 us -> none  [the longest x1 183 us: local(): lax.all_to_all(outgoing.reshape(st_count, slot_depth, pass_len, pair_cols...]
    pallas_call x0 -> x3, Pallas kernels: none -> 266 us  [the longest x1 115 us: cast_rows(): pl.pallas_call(functools.partial(cast_kernel, plan, len(weights)), out_sh...]
    all_to_all x5 -> x0, starting transfers between devices: 59.5 us -> none  [the longest x1 25.5 us: local(): lax.all_to_all(wanted, ST, split_axis=0, concat_axis=0, tiled=True)]
    all_gather x0 -> x1, blocking collectives: none -> 50.4 us  [routes(): ids = lax.all_gather(pass_ids.reshape(-1), ST, axis=0, tiled=False)]
    all_gather x1, waiting for transfers between devices: 30.3 us -> 10 us  [local(): gathered = lax.all_gather(store, 'tp', axis=2, tiled=True)]
    dot_general x5 -> x0, matrix products: 14.9 us -> none  [the longest x1 5.89 us: local(): jnp.einsum('rc,dc->rd', partial_value, weight_kv, preferred_element_type=...]
    unnamed x36 -> x27, local copies, waits for them, and re-layouts: 20.5 us -> 6.58 us
    reduce_scatter x2 -> x0, waiting for transfers between devices: 13.5 us -> none  [sum_in_order(): tiles = lax.psum_scatter(tiles, axes[k], scatter_dimension=0, tiled=True)]
  transfers between devices with their start and end apart: 8 -> 1, of which waited for: 7 -> 1; matrix products, arithmetic and copies ran while one was open for 6% -> 2% of each run, Pallas kernels for 0% -> 0%
where the time goes in v2:
time: 395 us; the launch traced here: 394 us
  Pallas kernels  266 us (67%)
  blocking collectives  50.4 us (13%)
  matrix products  21 us (5%)
  local copies, waits for them, and re-layouts  18.3 us (5%)
  between operations  15.6 us (4%)
  other arithmetic  11.3 us (3%)
  waiting for transfers between devices  10.7 us (3%)
    pallas_call x1, Pallas kernels, cast_rows(): pl.pallas_call(functools.partial(cast_kernel, plan, len(weights)), out_sh...  115 us
    pallas_call x1, Pallas kernels, fold_rows(): pl.pallas_call(functools.partial(fold_kernel, plan), out_shape=[jax.Shape...  114 us
    all_gather x1, blocking collectives, routes(): ids = lax.all_gather(pass_ids.reshape(-1), ST, axis=0, tiled=False)  50.4 us
    pallas_call x1, Pallas kernels, tail(): pl.pallas_call(tail_kernel, out_shape=[jax.ShapeDtypeStruct((tokens.shape...  37.9 us
    all_gather x1, waiting for transfers between devices, local(): gathered = lax.all_gather(store, 'tp', axis=2, tiled=True)  10 us
  transfers between devices with their start and end apart: 1, of which 1 were waited for; matrix products, arithmetic and copies ran while one was open for 2% of the time, Pallas kernels for 0%

profile of v2, /device:TPU:33, one launch (start us, length us, event | category | flops | bytes accessed | tf_op | source)
XLA Modules:
  0.0 394.2 jit_solution(14895125532421991912)
XLA Ops:
  8.8 50.4 %all-gather = s32[32,1,32]{2,1,0:T(1,128)S(1)} all-gather(s32[1,1,32]{2,1,0:T(1,128)S(1)} %reshape.268), channel_id=1, replica_groups=mesh['grp'=2,'st_0'=16,'st_1'=2,'tp'=4] {'st_0','st_1'}, dimensions={0}, use_global_device_ids=true | all-gather | bytes 4224 | tf_op jit(solution)/shard_map/all_gather | solution.py:500
  65.1 1.4 compare_reduce_fusion
  68.5 10.0 %all-gather.3.cloned.1.call-done = bf16[16,64,2048]{2,1,0:T(8,128)(2,1)} async-done(((bf16[16,64,512]{2,1,0:T(8,128)(2,1)}), bf16[16,64,2048]{2,1,0:T(8,128)(2,1)}) %all-gather.3.cloned.1.call-update) | async-done | bytes 4194320 | tf_op jit(solution)/shard_map/all_gather | solution.py:586
  78.6 5.3 %fusion.44 = bf16[1024,512]{0,1:T(8,128)(2,1)S(1)} fusion(bf16[1024,2048]{1,0:T(8,128)(2,1)} %bitcast.85, bf16[2048,256]{1,0:T(8,128)(2,1)} %refs_5_.1, bf16[2048,256]{1,0:T(8,128)(2,1)} %refs_4_.1), kind=kOutput, calls=%fused_computation.114 | convolution fusion | flops 2152202240 | bytes 7340032 | tf_op jit(solution)/shard_map/dot_general | solution.py:588
  83.9 118.5 %conditional.2 = (bf16[32,64,512]{2,1,0:T(8,128)(2,1)}, (bf16[32,64,512]{2,1,0:T(8,128)(2,1)S(1)}, bf16[3,2048,256]{2,1,0:T(8,128)(2,1)}, bf16[3,2048,256]{2,1,0...) conditional(s32[]{:T(128)} %convert_element_type.60, (s32[64]{0:T(128)S(1)}, ...), branch_computations={%region_17.18_spmd.clone, %region_18.19_spmd.clone} | conditional | flops 5892 | bytes 6295598 | solution.py:591
  84.8 1.3 copy.66
  86.1 114.6 %cast_rows.15 = (bf16[32,64,512]{2,1,0:T(8,128)(2,1)}, bf16[3,2048,256]{2,1,0:T(8,128)(2,1)}, bf16[3,2048,256]{2,1,0:T(8,128)(2,1)}, bf16[3,2048,256]{2,1,0:T(8,128)(2,1)}, bf16[3,2048,256]{2,1,0:T(8,128)(2,1)}) custom-call(s32[32]{0:T(128)S(1)} %get-tuple-element.2230.order_ref, s32[32]{0:T(128)} %dynamic_slice.60.where_ref, bf16[16,64,512]{2,1,0:T(8,128)(2,1)} %bitcast.71, ...), custom_call_target="tpu_custom_call" | custom-call | tf_op jit(solution)/shard_map/cond/branch_1_fun/cast_rows/pallas_call | solution.py:213
  200.7 1.6 copy.101
  202.3 1.8 fusion.47
  204.2 1.0 copy-done.4
  205.1 1.2 fusion.108
  206.3 3.1 fusion.56
  209.4 2.9 fusion.51
  212.4 3.3 convolution_convert_fusion
  215.7 1.8 multiply_reduce_fusion
  219.3 1.5 pad_maximum_fusion
  220.8 116.6 %conditional.3 = (bf16[16,64,512]{2,1,0:T(8,128)(2,1)}, bf16[3,256,512]{2,1,0:T(8,128)(2,1)}, bf16[16,64,256]{2,1,0:T(8,128)(2,1)}) conditional(s32[]{:T(128)} %convert_element_type.60, (s32[208,4]{0,1:T(4,128)S(1)}, s32[32]{0:T(128)S(1)}, bf16[32,64,512]{2,1,0:T(8,128)(2,1)}, bf16[1024,512]{1,0:T(8,128)(2,1)S(1)}) %tuple.78, ...), branch_computations={%region_22.23_spmd.clone, %region_23.24_spmd.clone} | conditional | bytes 1061912 | solution.py:651
  221.6 113.9 %fold_rows.5 = (bf16[16,64,512]{2,1,0:T(8,128)(2,1)}, bf16[3,256,512]{2,1,0:T(8,128)(2,1)}) custom-call(s32[832]{0:T(1024)} %reshape.267.table_ref, s32[32]{0:T(128)S(1)} %get-tuple-element.2263.final_ref, bf16[32,64,512]{2,1,0:T(8,128)(2,1)} %get-tuple-element.2264.grads_ref, bf16[1024,512]{1,0:T(8,128)(2,1)S(1)} %get-tuple-element.2265.tokens_ref), custom_call_target="tpu_custom_call" | custom-call | tf_op jit(solution)/shard_map/cond/branch_1_fun/fold_rows/pallas_call | solution.py:332
  335.5 1.9 slice.44
  337.4 5.0 %convolution_bitcast_fusion = f32[2048,256]{0,1:T(8,128)} fusion(bf16[16,64,256]{2,1,0:T(8,128)(2,1)} %get-tuple-element.2558, bf16[16,64,2048]{2,1,0:T(8,128)(2,1)} %all-gather.3.cloned.1.call-done), kind=kOutput, calls=%fused_computation.97 | convolution fusion | flops 1073741824 | bytes 6815744 | tf_op jit(solution)/shard_map/rc,rh->ch/dot_general | solution.py:661
  342.4 2.9 copy.73
  345.3 37.9 %tail.1 = (bf16[256,2048]{1,0:T(8,128)(2,1)}, bf16[256,2048]{1,0:T(8,128)(2,1)}, f32[64,256]{1,0:T(8,128)}) custom-call(bf16[16,64,512]{2,1,0:T(8,128)(2,1)} %get-tuple-element.2190.sums_ref, f32[16,2,64,256]{3,2,1,0:T(8,128)} %bitcast.69, bf16[1024,512]{1,0:T(8,128)(2,1)S(1)} %pad_maximum_fusion.1.tokens_ref, ...), custom_call_target="tpu_custom_call" | custom-call | tf_op jit(solution)/shard_map/tail/pallas_call | solution.py:459
  383.3 2.4 copy.102
  385.7 1.0 copy.103
  (84 shorter events, 12.1 us)
Async XLA Ops:
  7.2 195.2 %copy-start = (bf16[1024,256]{1,0:T(8,128)(2,1)S(1)}, bf16[1024,256]{1,0:T(8,128)(2,1)}, u32[]{:S(2)}) copy-start(bf16[1024,256]{1,0:T(8,128)(2,1)} %param.17) | copy-start | bytes 1572868
  7.2 71.4 %all-gather.3.cloned.1.call-start = ((), (), s32[]{:S(2)}) async-start(), calls=%async_computation | async-start | bytes 5242880 | tf_op jit(solution)/shard_map/all_gather | solution.py:586
  78.6 5.3 %copy-start.2 = (bf16[2048,256]{1,0:T(8,128)(2,1)S(1)}, bf16[2048,256]{1,0:T(8,128)(2,1)}, u32[]{:S(2)}) copy-start(bf16[2048,256]{1,0:T(8,128)(2,1)} %refs_5_.1) | copy-start | bytes 3145732
  202.3 4.0 %copy-start.1 = (bf16[32,64,512]{2,1,0:T(8,128)(2,1)S(1)}, bf16[32,64,512]{2,1,0:T(8,128)(2,1)}, u32[]{:S(2)}) copy-start(bf16[32,64,512]{2,1,0:T(8,128)(2,1)} %get-tuple-element.2200) | copy-start | bytes 6291460
  204.2 1.0 copy-start.4
  206.3 3.1 copy-start.8
  212.4 3.3 copy-start.9
  215.7 1.8 copy-start.3
  217.6 1.0 copy-start.5
  218.0 1.3 copy-start.7
  383.3 2.4 copy-start.6
  383.3 3.4 copy-start.10
Sparse Core Ops, SparseCore 0:
  9.8 68.6 all-gather.2

commit v3 on v2

--- a/solution.py
+++ b/solution.py
@@ -105,6 +105,155 @@
 
 def copy_sems(count):
     return [pltpu.SemaphoreType.DMA((count,)), pltpu.SemaphoreType.DMA((count,))]
+
+
+def front_kernel(ids_ref, store_ref, wk_ref, wv_ref, ids_out, all_out, kv_out, total, *sems):
+    gifts, ring_copies, x_copies = (Copies(*sems[2 * i : 2 * i + 2]) for i in range(3))
+    place = Place()
+    count = store_ref.shape[0]
+    half = count // 2
+    reach = place.ring // 2
+    greet(place.along_z(1), place.along_z(-1), place.along_x(1), place.along_x(-1), place.twin)
+    halves = (pl.ds(0, half), pl.ds(half, half))
+    near = {}
+    for d, step in ((0, 1), (1, -1)):
+        for h in (d, 1 - d):
+            near[d, h] = x_copies.start(
+                store_ref.at[halves[h]], all_out.at[place.x, halves[h]], place.along_x(step)
+            )
+    gift = gifts.start(ids_ref, ids_out.at[place.z, place.k], place.twin)
+    ids_out[place.z, place.k] = ids_ref[...]
+    all_out[place.x] = store_ref[...]
+    gift.wait_recv()
+    hops = {}
+
+    def hop(d, t):
+        source = lax.rem(place.z + (t - 1) * (2 * d - 1) + place.ring, place.ring)
+        part = ids_out.at[source]
+        hops[d, t] = ring_copies.start(part, part, place.along_z(1 - 2 * d))
+
+    def hops_until(first, last):
+        for t in range(first, last):
+            for d in range(2):
+                if t > 1 and t <= reach - d:
+                    hops[d, t - 1].wait_recv()
+                if t <= reach - d:
+                    hop(d, t)
+
+    def add(source, start):
+        rows = total.shape[0]
+        depth = store_ref.shape[2]
+        cols = wk_ref.shape[1]
+        part = all_out[source].reshape(rows, depth)
+        w_rows = pl.ds(pl.multiple_of(source * depth, depth), depth)
+        for c, w_ref in enumerate((wk_ref, wv_ref)):
+            at = slice(c * cols, (c + 1) * cols)
+            term = jnp.dot(part, w_ref[w_rows, :], preferred_element_type=F32)
+            total[:, at] = term if start else total[:, at] + term
+
+    hops_until(1, 4)
+    add(place.x, True)
+    hops_until(4, 6)
+    far = []
+    for d, step in ((0, 1), (1, -1)):
+        near[d, d].wait_recv()
+        source = lax.rem(place.x - step + place.tp, place.tp)
+        part = all_out.at[source, halves[d]]
+        far.append(x_copies.start(part, part, place.along_x(step)))
+    hops_until(6, reach + 1)
+    for d, step in ((0, 1), (1, -1)):
+        near[d, 1 - d].wait_recv()
+        add(lax.rem(place.x - step + place.tp, place.tp), False)
+    for d in range(2):
+        hops[d, reach - d].wait_recv()
+    for copy in far:
+        copy.wait_recv()
+    add(lax.rem(place.x + 2, place.tp), False)
+    kv_out[...] = total[...].reshape(kv_out.shape).astype(kv_out.dtype)
+    for group in (gifts, ring_copies, x_copies):
+        group.wait_sends()
+
+
+def front(ident, ids, store, w_key, w_value):
+    count, rows, cols = store.shape
+    ring, tp = lax.axis_size("st_0"), lax.axis_size("tp")
+    pair = 2 * w_key.shape[1]
+    return pl.pallas_call(
+        front_kernel,
+        out_shape=[
+            jax.ShapeDtypeStruct((ring, 2, *ids.shape), ids.dtype),
+            jax.ShapeDtypeStruct((tp, *store.shape), store.dtype),
+            jax.ShapeDtypeStruct((count, rows, pair), store.dtype),
+        ],
+        in_specs=[VMEM_SPEC] * 4,
+        out_specs=[VMEM_SPEC] * 3,
+        scratch_shapes=[pltpu.VMEM((count * rows, pair), F32)]
+        + copy_sems(1)
+        + copy_sems(ring - 1)
+        + copy_sems(6),
+        compiler_params=pltpu.CompilerParams(
+            collective_id=ident, has_side_effects=True, vmem_limit_bytes=VMEM_LIMIT
+        ),
+        name="front",
+    )(ids, store, w_key, w_value)
+
+
+def attend_kernel(scale, q_ref, gate_ref, mem_ref, kv_ref, grads_ref, tokens_ref):
+    blocks = q_ref.shape[0] // BLK
+    cols = q_ref.shape[1]
+    pass_len = kv_ref.shape[1]
+    low = q_ref.dtype
+
+    def dot(a, b, ca, cb):
+        return lax.dot_general(a, b, (((ca,), (cb,)), ((), ())), preferred_element_type=F32)
+
+    for b in range(blocks):
+        toks = pl.ds(b * BLK, BLK)
+        kv = kv_ref[pl.ds(b * PB, PB)].reshape(PB * pass_len, 2 * cols)
+        for h in range(cols // HD):
+            k_at = slice(h * HD, (h + 1) * HD)
+            v_at = slice(cols + h * HD, cols + (h + 1) * HD)
+            q, keys, values = q_ref[toks, k_at], kv[:, k_at], kv[:, v_at]
+            scores = dot(q, keys, 1, 1) * scale
+            shifted = jnp.exp(scores - jnp.max(scores, axis=-1, keepdims=True))
+            probs = shifted / jnp.sum(shifted, axis=-1, keepdims=True)
+            probs_low = probs.astype(low)
+            attended = dot(probs_low, values, 1, 0)
+            gate = gate_ref[toks, k_at].astype(F32)
+            mem = mem_ref[toks, k_at].astype(F32)
+            sig = jax.nn.sigmoid(gate)
+            attended_grad = (gate * sig * mem).astype(low)
+            gate_grad = mem * attended * sig * (1.0 + gate * (1.0 - sig))
+            prob_grad = dot(attended_grad, values, 1, 1)
+            inner = jnp.sum(probs * prob_grad, axis=-1, keepdims=True)
+            score_grad = (scale * probs * (prob_grad - inner)).astype(low)
+            tokens_ref[toks, k_at] = dot(score_grad, keys, 1, 0).astype(low)
+            tokens_ref[toks, v_at] = gate_grad.astype(low)
+            key_grad = dot(score_grad, q, 0, 0).astype(low)
+            value_grad = dot(probs_low, attended_grad, 0, 0).astype(low)
+            passes = pl.ds(b * PB, PB)
+            grads_ref[passes, :, k_at] = key_grad.reshape(PB, pass_len, HD)
+            grads_ref[passes, :, v_at] = value_grad.reshape(PB, pass_len, HD)
+
+
+def attend(queries, gate_pre, d_mem, request_kv):
+    toks, cols = queries.shape
+    _, pass_len, pair = request_kv.shape
+    step = 2
+    grid = toks // BLK // step
+    tok_spec = pl.BlockSpec((step * BLK, cols), lambda i: (i, 0))
+    kv_spec = pl.BlockSpec((step * PB, pass_len, pair), lambda i: (i, 0, 0))
+    return pl.pallas_call(
+        functools.partial(attend_kernel, HD**-0.5),
+        grid=(grid,),
+        out_shape=[
+            jax.ShapeDtypeStruct(request_kv.shape, request_kv.dtype),
+            jax.ShapeDtypeStruct((toks, pair), queries.dtype),
+        ],
+        in_specs=[tok_spec, tok_spec, tok_spec, kv_spec],
+        out_specs=[kv_spec, pl.BlockSpec((step * BLK, pair), lambda i: (i, 0))],
+        name="attend",
+    )(queries, gate_pre, d_mem, request_kv)
 
 
 def cast_kernel(plan, weights, order_ref, where_ref, kv_ref, *refs):
@@ -353,35 +502,28 @@
     )(table, final, grads, tokens)
 
 
-def project(rows_list, weight_list, out_ref, tile):
-    @pl.loop(0, out_ref.shape[1] // tile)
-    def _(n):
-        cols = pl.ds(pl.multiple_of(n * tile, tile), tile)
-        total = None
-        for rows, weight in zip(rows_list, weight_list):
-            term = lax.dot_general(
-                rows[...], weight[cols, :], (((1,), (1,)), ((), ())), preferred_element_type=F32
-            )
-            total = term if total is None else total + term
-        out_ref[:, cols] = total.astype(out_ref.dtype)
-
-
-def tail_kernel(
-    sums_ref,
-    partial_ref,
-    tokens_ref,
-    tokens_in,
-    *refs,
-):
+def project(rows_list, weight_list, out_ref, n, tile):
+    cols = pl.ds(n * tile, tile)
+    total = None
+    for rows, weight in zip(rows_list, weight_list):
+        term = lax.dot_general(
+            rows[...], weight[cols, :], (((1,), (1,)), ((), ())), preferred_element_type=F32
+        )
+        total = term if total is None else total + term
+    out_ref[:, cols] = total.astype(out_ref.dtype)
+
+
+def tail_kernel(sums_ref, all_ref, tokens_ref, tokens_in, *refs):
     weights, refs = refs[:8], refs[8:]
     d_tokens_ref, d_store_ref, d_wkey_ref = refs[:3]
-    wbuf_t, wbuf_s, own_t, in_t, own_s, in_s, twin_buf, chip_buf, ring_buf = refs[3:12]
-    load_sem, *sems = refs[12:]
+    wbuf_t, wbuf_s, own_t, in_t, own_s, in_s, refs = *refs[3:9], refs[9:]
+    keys, keys_turned, all_buf, terms, twin_terms, sent, come, last, last_in, refs = *refs[:9], refs[9:]
+    load_sem, *sems = refs
     exchange, gifts, ring_copies = (Copies(*sems[2 * i : 2 * i + 2]) for i in range(3))
     place = Place()
     tp, ring = place.tp, place.ring
+    reach = ring // 2
     peers = [place.along_x(rel) for rel in range(1, tp)]
-    far = [place.along_z(rel) for rel in range(1, ring)]
     loads = []
 
     def load(src, dst):
@@ -389,8 +531,10 @@
         copy.start()
         loads.append(copy)
 
-    greet(place.twin, *peers, *far)
-    gift = gifts.start(partial_ref.at[:, pl.ds(1 - place.k, 1)], twin_buf, place.twin)
+    load(sums_ref, keys)
+    for n in range(tp):
+        load(all_ref.at[n], all_buf.at[n])
+    greet(place.twin, place.along_z(1), place.along_z(-1), *peers)
     share = sums_ref.shape[0] // tp
     for rel, peer in enumerate(peers, 1):
         exchange.start(
@@ -405,86 +549,137 @@
         load(wb, wbuf.at[1])
         load(wa_far, wbuf.at[pl.ds(2, tp - 1)])
         load(wb_far, wbuf.at[pl.ds(2 + tp - 1, tp - 1)])
-    gift.wait_recv()
-
-    @pl.loop(0, ring)
-    def _(i):
-        total = partial_ref[i, place.k] + twin_buf[i, 0]
-        chip_buf[i] = total.astype(chip_buf.dtype)
-
-    for rel, device in enumerate(far, 1):
-        ring_copies.start(chip_buf.at[device[1]], ring_buf.at[ring - rel], device)
-    for copy in loads:
+    count, pass_len, pair = sums_ref.shape
+    rows, cols = count * pass_len, pair // 2
+    depth = all_ref.shape[3]
+    width = terms.shape[3]
+    loads[0].wait()
+    keys_turned[...] = keys[:, :, :cols].reshape(rows, cols).T
+    for n in range(tp):
+        loads[1 + n].wait()
+        term = jnp.dot(
+            keys_turned[...], all_buf[n].reshape(rows, depth), preferred_element_type=F32
+        )
+        for c in range(depth // width):
+            for h in range(2):
+                terms[h, n * (depth // width) + c] = term[
+                    h * (cols // 2) : (h + 1) * (cols // 2), c * width : (c + 1) * width
+                ]
+    gift = gifts.start(terms.at[1 - place.k], twin_terms, place.twin)
+    for copy in loads[1 + tp :]:
         copy.wait()
 
     def operands(own, far_rows, wbuf):
-        cols = own.shape[-1] // 2
+        n_cols = own.shape[-1] // 2
         rows_list, weight_list = [], []
         for c in range(2):
-            rows_list.append(own.at[:, pl.ds(c * cols, cols)])
+            rows_list.append(own.at[:, pl.ds(c * n_cols, n_cols)])
             weight_list.append(wbuf.at[c])
         for rel in range(tp - 1):
             for c in range(2):
-                rows_list.append(far_rows.at[rel, :, pl.ds(c * cols, cols)])
+                rows_list.append(far_rows.at[rel, :, pl.ds(c * n_cols, n_cols)])
                 weight_list.append(wbuf.at[2 + c * (tp - 1) + rel])
         return rows_list, weight_list
 
-    project(*operands(own_t, in_t, wbuf_t), d_tokens_ref, 512)
-    for copy in exchange.all:
-        copy.wait_recv()
-    rows = share * sums_ref.shape[1]
-    cols = sums_ref.shape[2]
-    project(
-        *operands(own_s.reshape(rows, cols), in_s.reshape(tp - 1, rows, cols), wbuf_s),
-        d_store_ref,
-        512,
+    part_rows = share * pass_len
+    tile = 512
+    tiles = d_tokens_ref.shape[1] // tile
+    for_tokens = operands(own_t, in_t, wbuf_t)
+    for_store = operands(
+        own_s.reshape(part_rows, pair), in_s.reshape(tp - 1, part_rows, pair), wbuf_s
     )
-    ring_copies_done = [copy.wait_recv() for copy in ring_copies.all]
-    del ring_copies_done
-    total = partial_ref[place.z, place.k] + twin_buf[place.z, 0]
-    for rel in range(1, ring):
-        total += ring_buf[rel].astype(F32)
-    d_wkey_ref[...] = total
+    gift.wait_recv()
+    hops = {}
+
+    def mine(dest):
+        return terms[place.k, dest] + twin_terms[dest]
+
+    done = 0
+    for s in range(1, reach + 1):
+        for d in range(2):
+            to_go = reach - d + 1 - s
+            if to_go < 1:
+                continue
+            turn = 1 - 2 * d
+            total = mine(lax.rem(place.z + turn * to_go + ring, ring))
+            n = d * reach + s - 1
+            if s > 1:
+                hops[d, s - 1].wait_recv()
+                total += come[n - 1].astype(F32)
+            sent[n] = total.astype(sent.dtype)
+            hops[d, s] = ring_copies.start(sent.at[n], come.at[n], place.along_z(turn))
+        if s == reach // 2:
+            for copy in exchange.all:
+                copy.wait_recv()
+        if s <= reach // 2:
+            for _ in range(-(-tiles // (reach // 2))):
+                if done < tiles:
+                    project(*for_tokens, d_tokens_ref, done, tile)
+                    done += 1
+        elif s < reach:
+            for _ in range(-(-tiles // (reach // 2 - 1))):
+                if done < 2 * tiles:
+                    project(*for_store, d_store_ref, done - tiles, tile)
+                    done += 1
+    total = mine(place.z)
+    for d in range(2):
+        hops[d, reach - d].wait_recv()
+        total += come[d * reach + reach - d - 1].astype(F32)
+    turned = total.T
+    out_rows = turned.shape[0] // 2
+    for c in range(2):
+        last[c] = turned[c * out_rows : (c + 1) * out_rows]
+    end = gifts.start(last.at[1 - place.k], last_in, place.twin)
+    half = cols // 2
+    d_wkey_ref[:, pl.ds(pl.multiple_of(place.k * half, half), half)] = last[place.k]
+    end.wait_recv()
+    d_wkey_ref[:, pl.ds(pl.multiple_of((1 - place.k) * half, half), half)] = last_in[...]
     for group in (exchange, gifts, ring_copies):
         group.wait_sends()
 
 
-def tail(ident, sums, partial, tokens, tokens_in, weights):
-    tp = lax.axis_size("tp")
-    ring, cores, rows, cols = partial.shape
-    model = weights[0].shape[0]
-    head_cols = weights[0].shape[1]
-    share = sums.shape[0] // tp
+def tail(ident, sums, all_rows, tokens, tokens_in, weights):
+    tp, ring = lax.axis_size("tp"), lax.axis_size("st_0")
+    model, head_cols = weights[0].shape
+    count, pass_len, pair = sums.shape
+    share = count // tp
+    width = model // ring
     low = sums.dtype
     return pl.pallas_call(
         tail_kernel,
         out_shape=[
             jax.ShapeDtypeStruct((tokens.shape[0] // tp, model), low),
-            jax.ShapeDtypeStruct((share * sums.shape[1], model), low),
-            jax.ShapeDtypeStruct((rows, cols), F32),
+            jax.ShapeDtypeStruct((share * pass_len, model), low),
+            jax.ShapeDtypeStruct((width // 2, head_cols), F32),
         ],
-        in_specs=[ANY_SPEC, VMEM_SPEC] + [ANY_SPEC] * (2 + len(weights)),
+        in_specs=[ANY_SPEC] * (4 + len(weights)),
         out_specs=[VMEM_SPEC] * 3,
         scratch_shapes=[
             pltpu.VMEM((2 * tp, model, head_cols), low),
             pltpu.VMEM((2 * tp, model, head_cols), low),
             pltpu.VMEM((tokens.shape[0] // tp, tokens.shape[1]), low),
             pltpu.VMEM(tokens_in.shape, low),
-            pltpu.VMEM((share, *sums.shape[1:]), low),
-            pltpu.VMEM((tp - 1, share, *sums.shape[1:]), low),
-            pltpu.VMEM((ring, 1, rows, cols), F32),
-            pltpu.VMEM((ring, rows, cols), low),
-            pltpu.VMEM((ring, rows, cols), low),
-            pltpu.SemaphoreType.DMA((3 + len(weights),)),
+            pltpu.VMEM((share, pass_len, pair), low),
+            pltpu.VMEM((tp - 1, share, pass_len, pair), low),
+            pltpu.VMEM(sums.shape, low),
+            pltpu.VMEM((head_cols, count * pass_len), low),
+            pltpu.VMEM(all_rows.shape, low),
+            pltpu.VMEM((2, ring, head_cols // 2, width), F32),
+            pltpu.VMEM((ring, head_cols // 2, width), F32),
+            pltpu.VMEM((ring, head_cols // 2, width), low),
+            pltpu.VMEM((ring, head_cols // 2, width), low),
+            pltpu.VMEM((2, width // 2, head_cols // 2), F32),
+            pltpu.VMEM((width // 2, head_cols // 2), F32),
+            pltpu.SemaphoreType.DMA((4 + tp + len(weights),)),
         ]
         + copy_sems(tp - 1)
-        + copy_sems(1)
+        + copy_sems(2)
         + copy_sems(ring - 1),
         compiler_params=pltpu.CompilerParams(
             collective_id=ident, has_side_effects=True, vmem_limit_bytes=VMEM_LIMIT
         ),
         name="tail",
-    )(sums, partial, tokens, tokens_in, *weights)
+    )(sums, all_rows, tokens, tokens_in, *weights)
 
 
 def first_slot(plan, d, step):
@@ -494,10 +689,9 @@
     return total
 
 
-def routes(plan, light, pass_ids):
+def routes(plan, light, ids):
     count, ring, slots = plan.passages, plan.ring, plan.slots
     me_z, me_k = lax.axis_index("st_0"), lax.axis_index("st_1")
-    ids = lax.all_gather(pass_ids.reshape(-1), ST, axis=0, tiled=False)
     devices, requests = ids.shape
     pair = 2 * count
     every = jnp.arange(devices * count, dtype=jnp.int32)
@@ -571,22 +765,16 @@
 def local(pass_ids, store, queries, gate_pre, w_query, w_gate, w_key, w_value, d_mem):
     tp_count = lax.axis_size("tp")
     ring = lax.axis_size("st_0")
-    tok_rows, head_cols = queries.shape
-    head_count = head_cols // HD
-    blocks = tok_rows // BLK
-    passages = store.shape[0]
-    pass_len = store.shape[1]
+    passages, pass_len, _ = store.shape
     model_width = w_key.shape[0]
-    requests = blocks * PB
-    pair_cols = 2 * head_cols
+    requests = pass_ids.size
     plan = Plan(ring, passages)
     light = Plan(ring, passages, light=True)
-    fits, order, where, table, final = routes(plan, light, pass_ids)
-    weight_kv = jnp.concatenate([w_key, w_value], axis=1)
-    gathered = lax.all_gather(store, "tp", axis=2, tiled=True)
-    flat_rows = gathered.reshape(passages * pass_len, model_width)
-    kv_pass = jnp.dot(flat_rows, weight_kv, preferred_element_type=jnp.float32)
-    kv_low = kv_pass.astype(jnp.bfloat16).reshape(passages, pass_len, pair_cols)
+    ids = jnp.zeros((8, 128), jnp.int32).at[0, :requests].set(pass_ids.reshape(-1))
+    ids, all_rows, kv = front(5, ids, store, w_key, w_value)
+    fits, order, where, table, final = routes(
+        plan, light, ids[:, :, 0, :requests].reshape(2 * ring, requests)
+    )
     weights = (w_query, w_gate, w_key, w_value)
     request_kv, wq_far, wg_far, wk_far, wv_far = lax.cond(
         fits,
@@ -594,61 +782,11 @@
         functools.partial(cast_rows, plan, 1),
         order,
         where,
-        kv_low,
+        kv,
         weights,
     )
-    block_kv = request_kv.reshape(blocks, PB * pass_len, pair_cols)
-    key_rows = block_kv[:, :, :head_cols].reshape(blocks, PB * pass_len, head_count, HD)
-    value_rows = block_kv[:, :, head_cols:].reshape(blocks, PB * pass_len, head_count, HD)
-    query_rows = queries.reshape(blocks, BLK, head_count, HD)
-    score_scale = HD ** (-0.5)
-    scores = (
-        jnp.einsum("nqhd,nkhd->nhqk", query_rows, key_rows, preferred_element_type=jnp.float32)
-        * score_scale
-    )
-    shifted = jnp.exp(scores - jnp.max(scores, axis=-1, keepdims=True))
-    prob_rows = shifted / jnp.sum(shifted, axis=-1, keepdims=True)
-    probs_low = prob_rows.astype(jnp.bfloat16)
-    attended = jnp.einsum(
-        "nhqk,nkhd->nqhd", probs_low, value_rows, preferred_element_type=jnp.float32
-    ).reshape(tok_rows, head_cols)
-    gate_vals = gate_pre.astype(jnp.float32)
-    sigmoid_vals = jax.nn.sigmoid(gate_vals)
-    mem_grad = d_mem.astype(jnp.float32)
-    attended_grad = (gate_vals * sigmoid_vals * mem_grad).astype(jnp.bfloat16)
-    gate_grad = (
-        mem_grad * attended * sigmoid_vals * (1.0 + gate_vals * (1.0 - sigmoid_vals))
-    ).astype(jnp.bfloat16)
-    attended_four = attended_grad.reshape(blocks, BLK, head_count, HD)
-    prob_grad = jnp.einsum(
-        "nqhd,nkhd->nhqk", attended_four, value_rows, preferred_element_type=jnp.float32
-    )
-    score_grad = (
-        score_scale
-        * prob_rows
-        * (prob_grad - jnp.sum(prob_rows * prob_grad, axis=-1, keepdims=True))
-    ).astype(jnp.bfloat16)
-    query_grad = (
-        jnp.einsum("nhqk,nkhd->nqhd", score_grad, key_rows, preferred_element_type=jnp.float32)
-        .astype(jnp.bfloat16)
-        .reshape(tok_rows, head_cols)
-    )
-    key_grad = jnp.einsum(
-        "nhqk,nqhd->nkhd", score_grad, query_rows, preferred_element_type=jnp.float32
-    )
-    value_grad = jnp.einsum(
-        "nhqk,nqhd->nkhd", probs_low, attended_four, preferred_element_type=jnp.float32
-    )
-    request_grads = jnp.concatenate(
-        [
-            key_grad.reshape(blocks, PB * pass_len, head_cols),
-            value_grad.reshape(blocks, PB * pass_len, head_cols),
-        ],
-        axis=2,
-    )
-    request_grads = request_grads.astype(jnp.bfloat16).reshape(requests, pass_len, pair_cols)
-    token_grads = jnp.concatenate([query_grad, gate_grad], axis=1)
-    pass_low, tokens_in = lax.cond(
+    request_grads, token_grads = attend(queries, gate_pre, d_mem, request_kv)
+    sums, tokens_in = lax.cond(
         fits,
         functools.partial(fold_rows, light, 2),
         functools.partial(fold_rows, plan, 3),
@@ -657,13 +795,10 @@
         request_grads,
         token_grads,
     )
-    key_sums = pass_low[:, :, :head_cols].reshape(passages * pass_len, head_cols)
-    partial = jnp.einsum("rc,rh->ch", flat_rows, key_sums, preferred_element_type=jnp.float32)
-    partial = partial.reshape(ring, 2, model_width // (2 * ring), head_cols)
     d_tokens, d_store, d_wkey = tail(
         4,
-        pass_low,
-        partial,
+        sums,
+        all_rows,
         token_grads,
         tokens_in,
         (w_query, w_gate, wq_far, wg_far, w_key, w_value, wk_far, wv_far),

time: 395 us -> 349 us (0.88)
  Pallas kernels: 266 us -> 332 us
  blocking collectives: 50.4 us -> 0 us
  matrix products: 21 us -> 0 us
  between operations: 15.6 us -> 2.12 us
  waiting for transfers between devices: 10.7 us -> 0 us
  local copies, waits for them, and re-layouts: 18.3 us -> 9.68 us
  other arithmetic: 11.3 us -> 4.04 us
    pallas_call x0 -> x2, Pallas kernels: none -> 73.1 us  [the longest x1 65.1 us: front(): pl.pallas_call(front_kernel, out_shape=[jax.ShapeDtypeStruct((ring, 2, *i...]
    all_gather x1 -> x0, blocking collectives: 50.4 us -> none  [routes(): ids = lax.all_gather(pass_ids.reshape(-1), ST, axis=0, tiled=False)]
    dot_general x8 -> x0, matrix products: 21 us -> none  [the longest x1 5.29 us: local(): kv_pass = jnp.dot(flat_rows, weight_kv, preferred_element_type=jnp.float32)]
    all_gather x1 -> x0, waiting for transfers between devices: 10 us -> none  [local(): gathered = lax.all_gather(store, 'tp', axis=2, tiled=True)]
    pallas_call x1, Pallas kernels: 37.9 us -> 33.2 us  [tail(): pl.pallas_call(tail_kernel, out_shape=[jax.ShapeDtypeStruct((tokens.shape...]
  transfers between devices with their start and end apart: 1 -> 0, of which waited for: 1 -> 0; matrix products, arithmetic and copies ran while one was open for 2% -> 0% of each run, Pallas kernels for 0% -> 0%
where the time goes in v3:
time: 349 us; the launch traced here: 348 us
  Pallas kernels  332 us (95%)
  local copies, waits for them, and re-layouts  9.68 us (3%)
  other arithmetic  4.04 us (1%)
    pallas_call x1, Pallas kernels, fold_rows(): pl.pallas_call(functools.partial(fold_kernel, plan), out_shape=[jax.Shape...  114 us
    pallas_call x1, Pallas kernels, cast_rows(): pl.pallas_call(functools.partial(cast_kernel, plan, len(weights)), out_sh...  112 us
    pallas_call x1, Pallas kernels, front(): pl.pallas_call(front_kernel, out_shape=[jax.ShapeDtypeStruct((ring, 2, *i...  65.1 us
    pallas_call x1, Pallas kernels, tail(): pl.pallas_call(tail_kernel, out_shape=[jax.ShapeDtypeStruct((tokens.shape...  33.2 us
    pallas_call x1, Pallas kernels, attend(): pl.pallas_call(functools.partial(attend_kernel, HD ** (-0.5)), grid=(grid...  8.03 us

profile of v3, /device:TPU:33, one launch (start us, length us, event | category | flops | bytes accessed | tf_op | source)
XLA Modules:
  0.0 348.4 jit_solution(8122661895540895576)
XLA Ops:
  0.7 0.8 copy.21
  1.6 0.6 scatter.4.ids_ref
  2.4 65.1 %front.1 = (s32[16,2,8,128]{3,2,1,0:T(8,128)}, bf16[4,16,64,512]{3,2,1,0:T(8,128)(2,1)}, bf16[16,64,512]{2,1,0:T(8,128)(2,1)}) custom-call(s32[8,128]{1,0:T(8,128)} %scatter.4.ids_ref, bf16[16,64,512]{2,1,0:T(8,128)(2,1)} %store_ref.1, bf16[2048,256]{1,0:T(8,128)(2,1)} %refs_4_.1, bf16[2048,256]{1,0:T(8,128)(2,1)} %refs_5_.1), custom_call_target="tpu_custom_call" | custom-call | tf_op jit(solution)/shard_map/front/pallas_call | solution.py:181
  67.5 1.0 fusion.55
  68.6 0.7 select_reduce_fusion
  69.5 0.8 convert_reduce_fusion
  70.3 0.7 convert_reduce_fusion.2
  71.4 0.2 select_reduce_fusion.9
  71.8 0.7 compare_reduce_fusion
  73.8 0.1 and_or_fusion
  74.0 0.2 select_reduce_fusion.2
  75.1 0.1 reduce_window_sum.11
  75.2 0.2 select_reduce_fusion.7
  75.4 0.1 copy.24
  75.5 0.1 reshape.317
  75.6 112.5 %conditional.2 = ((bf16[32,64,512]{2,1,0:T(8,128)(2,1)}, bf16[3,2048,256]{2,1,0:T(8,128)(2,1)}, bf16[3,2048,256]{2,1,0:T(8,128)(2,1)}, bf16[3,2048,256]{2,1,0:T(8,128)(2,1)}, bf16[3,2048,256]{2,1,0:T(8,128)(2,1)})) conditional(s32[]{:T(128)} %convert_element_type.23, (s32[32]{0:T(128)S(1)}, s32[32]{0:T(128)S(1)}, bf16[16,64,512]{2,1,0:T(8,128)(2,1)}, ...), branch_computations={%region_17.18_spmd, %region_18.19_spmd} | conditional | bytes 8 | solution.py:779
  75.6 112.5 %cast_rows.3 = (bf16[32,64,512]{2,1,0:T(8,128)(2,1)}, bf16[3,2048,256]{2,1,0:T(8,128)(2,1)}, bf16[3,2048,256]{2,1,0:T(8,128)(2,1)}, bf16[3,2048,256]{2,1,0:T(8,128)(2,1)}, bf16[3,2048,256]{2,1,0:T(8,128)(2,1)}) custom-call(s32[32]{0:T(128)S(1)} %get-tuple-element.63.order_ref, s32[32]{0:T(128)S(1)} %get-tuple-element.64.where_ref, ...), custom_call_target="tpu_custom_call" | custom-call | tf_op jit(solution)/shard_map/cond/branch_1_fun/cast_rows/pallas_call | solution.py:362
  188.1 8.0 %attend.1 = (bf16[32,64,512]{2,1,0:T(8,128)(2,1)}, bf16[1024,512]{1,0:T(8,128)(2,1)}) custom-call(bf16[1024,256]{1,0:T(8,128)(2,1)} %q_ref.1, bf16[1024,256]{1,0:T(8,128)(2,1)} %gate_ref.1, bf16[1024,256]{1,0:T(8,128)(2,1)} %mem_ref.1, bf16[32,64,512]{2,1,0:T(8,128)(2,1)} %get-tuple-element.98.kv_ref), custom_call_target="tpu_custom_call" | custom-call | tf_op jit(solution)/shard_map/attend/pallas_call | solution.py:246
  196.1 113.8 %conditional.3 = ((bf16[16,64,512]{2,1,0:T(8,128)(2,1)}, bf16[3,256,512]{2,1,0:T(8,128)(2,1)S(1)})) conditional(s32[]{:T(128)} %convert_element_type.23, (s32[832]{0:T(1024)S(1)}, s32[32]{0:T(128)S(1)}, bf16[32,64,512]{2,1,0:T(8,128)(2,1)}, bf16[1024,512]{1,0:T(8,128)(2,1)}) %tuple.25, (s32[832]{0:T(1024)S(1)}, s32[32]{0:T(128)S(1)}, ...), branch_computations={%region_19.20_spmd, %region_20.21_spmd} | conditional | bytes 8 | solution.py:789
  196.1 113.6 %fold_rows.3 = (bf16[16,64,512]{2,1,0:T(8,128)(2,1)}, bf16[3,256,512]{2,1,0:T(8,128)(2,1)S(1)}) custom-call(s32[832]{0:T(1024)S(1)} %get-tuple-element.74.table_ref, s32[32]{0:T(128)S(1)} %get-tuple-element.75.final_ref, bf16[32,64,512]{2,1,0:T(8,128)(2,1)} %get-tuple-element.76.grads_ref, bf16[1024,512]{1,0:T(8,128)(2,1)} %get-tuple-element.77.tokens_ref), custom_call_target="tpu_custom_call" | custom-call | tf_op jit(solution)/shard_map/cond/branch_1_fun/fold_rows/pallas_call | solution.py:481
  309.9 33.2 %tail.1 = (bf16[256,2048]{1,0:T(8,128)(2,1)}, bf16[256,2048]{1,0:T(8,128)(2,1)}, f32[64,256]{1,0:T(8,128)}) custom-call(bf16[16,64,512]{2,1,0:T(8,128)(2,1)} %get-tuple-element.101.sums_ref, bf16[4,16,64,512]{3,2,1,0:T(8,128)(2,1)} %get-tuple-element.102.all_ref, bf16[1024,512]{1,0:T(8,128)(2,1)} %get-tuple-element.100.tokens_ref, ...), custom_call_target="tpu_custom_call" | custom-call | tf_op jit(solution)/shard_map/tail/pallas_call | solution.py:648
  343.1 2.3 copy.42
  345.5 2.3 copy.43
  347.8 0.6 copy.44
  (47 shorter events, 2.2 us)
Async XLA Ops:
  0.6 71.1 %copy-start.2 = (s32[8]{0:T(128)S(1)}, s32[8]{0:T(128)}, u32[]{:S(2)}) copy-start(s32[8]{0:T(128)} %constant.258.clone) | copy-start | bytes 100
  0.6 74.9 %copy-start = (bf16[2048,256]{1,0:T(8,128)(2,1)S(1)}, bf16[2048,256]{1,0:T(8,128)(2,1)}, u32[]{:S(2)}) copy-start(bf16[2048,256]{1,0:T(8,128)(2,1)} %refs_4_.1) | copy-start | bytes 3145732
  343.1 4.7 %copy-start.1 = (f32[64,256]{1,0:T(8,128)S(1)}, f32[64,256]{1,0:T(8,128)}, u32[]{:S(2)}) copy-start(f32[64,256]{1,0:T(8,128)} %get-tuple-element.167) | copy-start | bytes 196612

commit v4 on v3

--- a/solution.py
+++ b/solution.py
@@ -13,7 +13,9 @@
 PB = 4
 MOST = 2
 CHUNK = 4
-LIGHT = (24, 22, 22, 20, 18, 16, 12, 4)
+LENGTH = 54
+STAGE = 2
+LAG = 2 * STAGE
 VMEM_LIMIT = 62 * 1024 * 1024
 ST = ("st_0", "st_1")
 GRP_ST = ("grp", "st_0", "st_1")
@@ -26,7 +28,7 @@
 
 
 class Plan:
-    def __init__(self, ring, passages, light=False):
+    def __init__(self, ring, passages):
         self.ring = ring
         self.passages = passages
         self.reach = ring // 2
@@ -37,9 +39,7 @@
             + min(passages, per_owner * (self.reach - t))
             for t in self.steps_of
         }
-        self.sizes = dict(self.layout)
-        if light:
-            self.sizes = {t: min(n, LIGHT[t - 1]) for t, n in self.layout.items()}
+        self.sizes = self.layout
         self.base = [{}, {}]
         at = passages
         for d in range(2):
@@ -500,6 +500,392 @@
         ),
         name="fold_rows",
     )(table, final, grads, tokens)
+
+
+def copy_slots(src, src_at, dst, dst_at, size):
+    @pl.loop(0, size)
+    def _(j):
+        dst[dst_at + j] = src[src_at + j]
+
+
+class WeightShare:
+    def __init__(self, place, copies, w_refs, w_outs):
+        self.place, self.copies, self.outs = place, copies, w_outs
+        rows = w_refs[0].shape[0] // 2
+        self.half = pl.ds(place.k * rows, rows)
+        self.near, self.middle, self.gifts = [], [], []
+        for w_ref, w_out in zip(w_refs, w_outs):
+            for slot, step in ((2, 1), (0, -1)):
+                src, dst = w_ref.at[self.half], w_out.at[slot, self.half]
+                self.near.append(copies.start(src, dst, place.along_x(step)))
+
+    def forward(self):
+        for copy in self.near:
+            copy.wait_recv()
+        for w_out in self.outs:
+            src = w_out.at[2 * self.place.k, self.half]
+            dst = w_out.at[1, self.half]
+            device = self.place.along_x(2 * self.place.k - 1)
+            self.middle.append(self.copies.start(src, dst, device))
+            for slot in (0, 2):
+                self.give(w_out.at[slot, self.half])
+
+    def give(self, part):
+        self.gifts.append(self.copies.start(part, part, self.place.twin))
+
+    def finish(self):
+        for copy, w_out in zip(self.middle, self.outs):
+            copy.wait_recv()
+            self.give(w_out.at[1, self.half])
+
+    def wait(self):
+        for gift in self.gifts:
+            gift.wait_recv()
+
+
+def stream_cast_kernel(weights, source_ref, where_ref, kv_ref, *refs):
+    w_refs, refs = refs[:weights], refs[weights:]
+    out_ref, w_outs, refs = refs[0], refs[1 : 1 + weights], refs[1 + weights :]
+    kept, land, twin_land, leave, *sems = refs
+    ring_copies, gifts, w_copies = (Copies(*sems[2 * i : 2 * i + 2]) for i in range(3))
+    place = Place()
+    count = kv_ref.shape[0]
+    length = land.shape[0] // 2
+    stages = length // STAGE
+    home = 2 * count
+
+    greet(place.along_z(1), place.along_z(-1), place.along_x(1), place.along_x(-1), place.twin)
+    own_gift = gifts.start(kv_ref, kept.at[pl.ds(count, count)], place.twin)
+
+    @pl.loop(0, count)
+    def _(j):
+        kept[j] = kv_ref[j]
+
+    own_gift.wait_recv()
+    sends, given = {}, {}
+    share = None
+    for i in range(stages + 4):
+        for d in range(2):
+            if 0 <= i - 2 < stages:
+                at = d * length + (i - 2) * STAGE
+                sends[d, i - 2].wait_recv()
+                part = pl.ds(at, STAGE)
+                given[d, i - 2] = gifts.start(land.at[part], twin_land.at[part], place.twin)
+                copy_slots(land, at, kept, home + at, STAGE)
+            if i < stages:
+                at = d * length + i * STAGE
+
+                @pl.loop(at, at + STAGE)
+                def _(q):
+                    leave[q] = kept[source_ref[q]]
+
+            if 0 <= i - 4 < stages:
+                at = d * length + (i - 4) * STAGE
+                given[d, i - 4].wait_recv()
+                copy_slots(twin_land, at, kept, home + 2 * length + at, STAGE)
+        if i < stages:
+            for d in range(2):
+                part = pl.ds(d * length + i * STAGE, STAGE)
+                sends[d, i] = ring_copies.start(
+                    leave.at[part], land.at[part], place.along_z(1 - 2 * d)
+                )
+        if i == 1:
+            share = WeightShare(place, w_copies, w_refs, w_outs)
+        if i == 2 * stages // 3:
+            share.forward()
+    share.finish()
+
+    @pl.loop(0, out_ref.shape[0])
+    def _(r):
+        out_ref[r] = kept[where_ref[r]]
+
+    share.wait()
+    for group in (gifts, ring_copies, w_copies):
+        group.wait_sends()
+
+
+def stream_cast(ident, source, where, kv, weights):
+    count, rows, cols = kv.shape
+    stages = LENGTH // STAGE
+    others = lax.axis_size("tp") - 1
+    return pl.pallas_call(
+        functools.partial(stream_cast_kernel, len(weights)),
+        out_shape=[jax.ShapeDtypeStruct((where.shape[0], rows, cols), kv.dtype)]
+        + [jax.ShapeDtypeStruct((others, *w.shape), w.dtype) for w in weights],
+        in_specs=[SMEM_SPEC, SMEM_SPEC, VMEM_SPEC] + [ANY_SPEC] * len(weights),
+        out_specs=[VMEM_SPEC] + [ANY_SPEC] * len(weights),
+        scratch_shapes=[
+            pltpu.VMEM((2 * count + 4 * LENGTH, rows, cols), kv.dtype),
+            pltpu.VMEM((2 * LENGTH, rows, cols), kv.dtype),
+            pltpu.VMEM((2 * LENGTH, rows, cols), kv.dtype),
+            pltpu.VMEM((2 * LENGTH, rows, cols), kv.dtype),
+        ]
+        + copy_sems(2 * stages)
+        + copy_sems(2 * stages + 1)
+        + copy_sems(6 * len(weights)),
+        compiler_params=pltpu.CompilerParams(
+            collective_id=ident, has_side_effects=True, vmem_limit_bytes=VMEM_LIMIT
+        ),
+        name="stream_cast",
+    )(source, where, kv, *weights)
+
+
+def stream_fold_kernel(
+    table_ref, onward_ref, final_ref, grads_ref, tokens_ref, out_ref, tokens_out, held, kept, land,
+    leave, twin_land, load_sem, *sems
+):
+    ring_copies, gifts, exchange = (Copies(*sems[2 * i : 2 * i + 2]) for i in range(3))
+    place = Place()
+    count = out_ref.shape[0]
+    length = land.shape[0] // 2
+    stages = length // STAGE
+    own = grads_ref.shape[0]
+    readers = 2 * MOST
+    zero = 2 * length
+    peers = [place.along_x(rel) for rel in range(1, place.tp)]
+
+    load = pltpu.make_async_copy(grads_ref, held.at[pl.ds(0, own)], load_sem)
+    load.start()
+    blank = jnp.zeros_like(held[0])
+    held[2 * own] = blank
+    kept[zero] = blank
+    twin_land[2 * count] = blank
+    greet(place.along_z(1), place.along_z(-1), place.twin, *peers)
+    own_gift = gifts.start(grads_ref, held.at[pl.ds(own, own)], place.twin)
+    block = tokens_out.shape[1]
+    for rel, peer in enumerate(peers, 1):
+        exchange.start(
+            tokens_ref.at[pl.ds(peer[3] * block, block)],
+            tokens_out.at[place.tp - 1 - rel],
+            peer,
+        )
+    load.wait()
+    own_gift.wait_recv()
+
+    def readers_sum(slot):
+        total = held[table_ref[slot * readers]].astype(F32)
+        for q in range(1, readers):
+            total += held[table_ref[slot * readers + q]].astype(F32)
+        return total
+
+    sends = {}
+
+    def arrive(i):
+        for d in range(2):
+            at = d * length + i * STAGE
+            sends[d, i].wait_recv()
+            if i * STAGE < count:
+                src = land.at[pl.ds(at, STAGE)]
+                dst = twin_land.at[pl.ds(d * count + i * STAGE, STAGE)]
+                gifts.start(src, dst, place.twin)
+            copy_slots(land, at, kept, at, STAGE)
+
+    for i in reversed(range(stages)):
+        if i + 2 < stages:
+            arrive(i + 2)
+        for d in range(2):
+            at = d * length + i * STAGE
+
+            @pl.loop(at, at + STAGE)
+            def _(q):
+                total = readers_sum(count + q) + kept[onward_ref[q]].astype(F32)
+                leave[q] = total.astype(leave.dtype)
+
+        for d in range(2):
+            part = pl.ds(d * length + i * STAGE, STAGE)
+            sends[d, i] = ring_copies.start(
+                leave.at[part], land.at[part], place.along_z(2 * d - 1)
+            )
+    arrive(1)
+    arrive(0)
+    for gift in gifts.all[1:]:
+        gift.wait_recv()
+
+    @pl.loop(0, count)
+    def _(p):
+        total = readers_sum(p)
+        for d in range(2):
+            total += kept[final_ref[d * count + p]].astype(F32)
+            total += twin_land[final_ref[(2 + d) * count + p]].astype(F32)
+        out_ref[p] = total.astype(out_ref.dtype)
+
+    for copy in exchange.all:
+        copy.wait_recv()
+    for group in (gifts, ring_copies, exchange):
+        group.wait_sends()
+
+
+def stream_fold(ident, count, table, onward, final, grads, tokens):
+    own, rows, cols = grads.shape
+    stages = LENGTH // STAGE
+    tp = lax.axis_size("tp")
+    return pl.pallas_call(
+        stream_fold_kernel,
+        out_shape=[
+            jax.ShapeDtypeStruct((count, rows, cols), grads.dtype),
+            jax.ShapeDtypeStruct((tp - 1, tokens.shape[0] // tp, tokens.shape[1]), tokens.dtype),
+        ],
+        in_specs=[SMEM_SPEC, SMEM_SPEC, SMEM_SPEC, ANY_SPEC, ANY_SPEC],
+        out_specs=[VMEM_SPEC, ANY_SPEC],
+        scratch_shapes=[
+            pltpu.VMEM((2 * own + 1, rows, cols), grads.dtype),
+            pltpu.VMEM((2 * LENGTH + 1, rows, cols), grads.dtype),
+            pltpu.VMEM((2 * LENGTH, rows, cols), grads.dtype),
+            pltpu.VMEM((2 * LENGTH, rows, cols), grads.dtype),
+            pltpu.VMEM((2 * count + 1, rows, cols), grads.dtype),
+            pltpu.SemaphoreType.DMA,
+        ]
+        + copy_sems(2 * stages)
+        + copy_sems(1 + 2 * (-(-count // STAGE)))
+        + copy_sems(tp - 1),
+        compiler_params=pltpu.CompilerParams(
+            collective_id=ident, has_side_effects=True, vmem_limit_bytes=VMEM_LIMIT
+        ),
+        name="stream_fold",
+    )(table, onward, final, grads, tokens)
+
+
+def summed(pairs, start):
+    total = start
+    for holds, value in pairs:
+        total = total + jnp.where(holds, value, 0)
+    return total
+
+
+def readers_table(slot, slots, requests):
+    at_slot = slot[:, None] == jnp.arange(slots, dtype=jnp.int32)[None, :]
+    turn = jnp.cumsum(at_slot.astype(jnp.int32), axis=0)
+    number = jnp.arange(requests, dtype=jnp.int32)[:, None]
+    columns = [
+        jnp.min(jnp.where(at_slot & (turn == q + 1), number, requests), axis=0)
+        for q in range(2 * MOST)
+    ]
+    return jnp.stack(columns, axis=1).reshape(-1).astype(jnp.int32)
+
+
+def needs(ring, count, ids):
+    devices = ids.shape[0]
+    pair = 2 * count
+    every = jnp.arange(devices * count, dtype=jnp.int32)
+    owner = ids // count
+    owner_z, owner_k = owner // 2, owner % 2
+    reader_z = (jnp.arange(devices, dtype=jnp.int32) // 2)[:, None]
+    away = jnp.mod(reader_z - owner_z, ring)
+    up = (2 * away < ring) | ((2 * away == ring) & (owner_k == 0))
+    steps = (jnp.where(up, away, 0), jnp.where(up, 0, ring - away))
+    hot = ids.reshape(-1)[:, None] == every[None, :]
+    place = jnp.arange(pair, dtype=jnp.int32)
+    ranks, fars = [], []
+    for d in range(2):
+        far = jnp.max(jnp.where(hot, steps[d].reshape(-1)[:, None], 0), axis=0)
+        far = far.reshape(ring, pair)
+        before = (far[:, None, :] > far[:, :, None]) | (
+            (far[:, None, :] == far[:, :, None]) & (place[None, None, :] < place[None, :, None])
+        )
+        ranks.append(jnp.sum(before.astype(jnp.int32), axis=2))
+        fars.append(far)
+    return owner_k, steps, fars, ranks
+
+
+def own_chip(array):
+    return lax.dynamic_slice_in_dim(array, lax.axis_index("st_0"), 1, axis=0)[0]
+
+
+def chip_requests(array):
+    return lax.dynamic_slice_in_dim(array, 2 * lax.axis_index("st_0"), 2, axis=0).reshape(-1)
+
+
+def stream_routes(ring, count, ids):
+    me_k = lax.axis_index("st_1")
+    requests = ids.shape[1]
+    pair = 2 * count
+    reach = ring // 2
+    owner_k, steps, fars, ranks = needs(ring, count, ids)
+    core = jnp.arange(2, dtype=jnp.int32)
+    spot = jnp.arange(LENGTH, dtype=jnp.int32)
+    place = jnp.arange(pair, dtype=jnp.int32)
+    at_home = place % count + jnp.where(place // count == me_k, 0, count)
+    want = 2 * jnp.arange(count, dtype=jnp.int32) + me_k
+    chip_ids = chip_requests(ids)
+    every = jnp.arange(ids.shape[0] * count, dtype=jnp.int32)
+    chip_hot = chip_ids[:, None] == every[None, :]
+    chip_owner = chip_requests(owner_k)
+    within = chip_ids % count
+    where = within + jnp.where(chip_owner == me_k, 0, count)
+    slot = jnp.where(chip_owner == me_k, within, -1)
+    fits = jnp.bool_(True)
+    source, onward, near, aside = [], [], [], []
+    for d in range(2):
+        turn = 1 - 2 * d
+        sizes, starts = [], []
+        for t in range(1, reach + 1):
+            whole = jnp.sum((fars[d] >= t).astype(jnp.int32), axis=1)[:, None]
+            sizes.append((whole + 1 - core[None, :]) // 2)
+            if t == 1:
+                starts.append(jnp.zeros_like(sizes[0]))
+            else:
+                behind = jnp.roll(starts[-1] + sizes[-2], -turn, axis=0)
+                starts.append(jnp.maximum(behind, starts[-1] + LAG))
+            fits &= jnp.all(starts[-1] + sizes[-1] <= LENGTH)
+        out_size = [own_chip(jnp.roll(a, turn * t, axis=0)) for t, a in enumerate(sizes)]
+        out_at = [own_chip(jnp.roll(a, turn * t, axis=0)) for t, a in enumerate(starts)]
+        in_size = [own_chip(jnp.roll(a, turn * (t + 1), axis=0)) for t, a in enumerate(sizes)]
+        in_at = [own_chip(jnp.roll(a, turn * (t + 1), axis=0)) for t, a in enumerate(starts)]
+        mine = [
+            [jnp.where(me_k == 0, a[0], a[1]) for a in array]
+            for array in (out_size, out_at, in_size, in_at)
+        ]
+        size_o, at_o, size_i, at_i = mine
+        rank, far = own_chip(ranks[d]), own_chip(fars[d])
+        order = jnp.sum(jnp.where(rank[None, :] == want[:, None], at_home[None, :], 0), axis=1)
+        order = jnp.concatenate([order, jnp.zeros((LENGTH - count,), order.dtype)])
+        base = pair + d * LENGTH
+        source.append(
+            summed(
+                [
+                    ((spot >= at_o[t]) & (spot < at_o[t] + size_o[t]), base + at_i[t - 1] + spot - at_o[t])
+                    for t in range(1, reach)
+                ],
+                jnp.where(spot < size_o[0], order, 0),
+            )
+        )
+        onward.append(
+            summed(
+                [
+                    (
+                        (spot >= at_i[t]) & (spot < at_i[t] + jnp.minimum(size_i[t], size_o[t + 1])),
+                        d * LENGTH + at_o[t + 1] + spot - at_i[t] - 2 * LENGTH,
+                    )
+                    for t in range(reach - 1)
+                ],
+                jnp.full((LENGTH,), 2 * LENGTH, jnp.int32),
+            )
+        )
+        index = lax.dynamic_slice_in_dim(rank, me_k * count, count)
+        used = lax.dynamic_slice_in_dim(far, me_k * count, count) > 0
+        same = index % 2 == me_k
+        near.append(jnp.where(used & same, d * LENGTH + index // 2, 2 * LENGTH))
+        aside.append(jnp.where(used & ~same, d * count + index // 2, 2 * count))
+        step = chip_requests(steps[d])
+        ranked = jnp.sum(jnp.where(chip_hot, ranks[d].reshape(-1)[None, :], 0), axis=1)
+        at = summed(
+            [
+                ((step == t + 1) & (ranked % 2 == c), in_at[t][c])
+                for t in range(reach)
+                for c in range(2)
+            ],
+            ranked // 2,
+        )
+        by_me = ranked % 2 == me_k
+        where = jnp.where(step > 0, base + at + jnp.where(by_me, 0, 2 * LENGTH), where)
+        slot = jnp.where(step > 0, jnp.where(by_me, count + d * LENGTH + at, -1), slot)
+    where = lax.dynamic_slice_in_dim(where, me_k * requests, requests)
+    slot = slot.reshape(2, requests)
+    slot = jnp.where(me_k == 0, slot, slot[::-1]).reshape(-1)
+    table = readers_table(slot, count + 2 * LENGTH, 2 * requests)
+    tables = (jnp.concatenate(source), where, jnp.concatenate(onward), jnp.concatenate(near + aside))
+    source, where, onward, final = (t.astype(jnp.int32) for t in tables)
+    return fits, source, where, table, onward, final
 
 
 def project(rows_list, weight_list, out_ref, n, tile):
@@ -689,77 +1075,41 @@
     return total
 
 
-def routes(plan, light, ids):
-    count, ring, slots = plan.passages, plan.ring, plan.slots
-    me_z, me_k = lax.axis_index("st_0"), lax.axis_index("st_1")
-    devices, requests = ids.shape
-    pair = 2 * count
-    every = jnp.arange(devices * count, dtype=jnp.int32)
-    owner = ids // count
-    owner_z, owner_k = owner // 2, owner % 2
-    reader_z = (jnp.arange(devices, dtype=jnp.int32) // 2)[:, None]
-    away = jnp.mod(reader_z - owner_z, ring)
-    up = (2 * away < ring) | ((2 * away == ring) & (owner_k == 0))
-    steps = (jnp.where(up, away, 0), jnp.where(up, 0, ring - away))
-    hot = ids.reshape(-1)[:, None] == every[None, :]
-    place = jnp.arange(pair, dtype=jnp.int32)
-    ranks, fars = [], []
-    fits = jnp.bool_(True)
-    for d in range(2):
-        far = jnp.max(jnp.where(hot, steps[d].reshape(-1)[:, None], 0), axis=0)
-        far = far.reshape(ring, pair)
-        before = (far[:, None, :] > far[:, :, None]) | (
-            (far[:, None, :] == far[:, :, None]) & (place[None, None, :] < place[None, :, None])
-        )
-        ranks.append(jnp.sum(before.astype(jnp.int32), axis=2))
-        fars.append(far)
-        bounds = jnp.array([light.sizes[t] for t in light.steps_of], jnp.int32)
-        dist = jnp.arange(1, plan.reach + 1, dtype=jnp.int32)
-        sent = jnp.sum((far[:, None, :] >= dist[None, :, None]).astype(jnp.int32), axis=2)
-        fits &= jnp.all(sent <= bounds[None, :])
-
-    def chip(array):
-        return lax.dynamic_slice_in_dim(array, me_z, 1, axis=0)[0]
-
-    def readers(array):
-        return lax.dynamic_slice_in_dim(array, me_z * 2, 2, axis=0).reshape(-1)
-
+def routes(plan, ids):
+    count, slots = plan.passages, plan.slots
+    me_k = lax.axis_index("st_1")
+    requests = ids.shape[1]
+    every = jnp.arange(ids.shape[0] * count, dtype=jnp.int32)
+    owner_k, steps, fars, ranks = needs(plan.ring, count, ids)
+    place = jnp.arange(2 * count, dtype=jnp.int32)
     at_home = place % count + jnp.where(place // count == me_k, 0, count)
     want = 2 * jnp.arange(count, dtype=jnp.int32) + me_k
     order, final = [], []
     for d in range(2):
-        rank, far = chip(ranks[d]), chip(fars[d])
+        rank, far = own_chip(ranks[d]), own_chip(fars[d])
         order.append(jnp.sum(jnp.where(rank[None, :] == want[:, None], at_home[None, :], 0), axis=1))
         twin_at = plan.slots - count
         near = plan.base[d][1] - count
         aside = twin_at + d * (plan.layout[1] // 2)
         index = jnp.where(rank % 2 == me_k, near, aside) + rank // 2
         index = jnp.where(far > 0, index, twin_at + plan.layout[1])
-        final.append(lax.dynamic_slice_in_dim(index, me_k * count, count, axis=0))
-    chip_ids = readers(ids)
+        final.append(lax.dynamic_slice_in_dim(index, me_k * count, count))
+    chip_ids = chip_requests(ids)
     chip_hot = chip_ids[:, None] == every[None, :]
-    slot, core = chip_ids % count, readers(owner_k)
+    slot, core = chip_ids % count, chip_requests(owner_k)
     for d in range(2):
         rank = jnp.sum(jnp.where(chip_hot, ranks[d].reshape(-1)[None, :], 0), axis=1)
-        step = readers(steps[d] * (away > 0))
+        step = chip_requests(steps[d])
         slot = jnp.where(step > 0, first_slot(plan, d, step) + rank // 2, slot)
         core = jnp.where(step > 0, rank % 2, core)
     where = slot + jnp.where(core == me_k, 0, slots)
-    where = lax.dynamic_slice_in_dim(where, me_k * requests, requests, axis=0)
+    where = lax.dynamic_slice_in_dim(where, me_k * requests, requests)
     mine = jnp.where(core == me_k, slot, -1).reshape(2, requests)
     mine = jnp.where(me_k == 0, mine, mine[::-1]).reshape(-1)
-    at_slot = mine[:, None] == jnp.arange(slots, dtype=jnp.int32)[None, :]
-    turn = jnp.cumsum(at_slot.astype(jnp.int32), axis=0)
-    number = jnp.arange(2 * requests, dtype=jnp.int32)[:, None]
-    table = jnp.stack(
-        [
-            jnp.min(jnp.where(at_slot & (turn == q + 1), number, 2 * requests), axis=0)
-            for q in range(2 * MOST)
-        ],
-        axis=1,
-    ).reshape(-1)
-    tables = (jnp.concatenate(order), where, table, jnp.concatenate(final))
-    return fits, *(t.astype(jnp.int32) for t in tables)
+    table = readers_table(mine, slots, 2 * requests)
+    tables = (jnp.concatenate(order), where, jnp.concatenate(final))
+    order, where, final = (t.astype(jnp.int32) for t in tables)
+    return order, where, table, final
 
 
 def local(pass_ids, store, queries, gate_pre, w_query, w_gate, w_key, w_value, d_mem):
@@ -769,31 +1119,32 @@
     model_width = w_key.shape[0]
     requests = pass_ids.size
     plan = Plan(ring, passages)
-    light = Plan(ring, passages, light=True)
     ids = jnp.zeros((8, 128), jnp.int32).at[0, :requests].set(pass_ids.reshape(-1))
     ids, all_rows, kv = front(5, ids, store, w_key, w_value)
-    fits, order, where, table, final = routes(
-        plan, light, ids[:, :, 0, :requests].reshape(2 * ring, requests)
-    )
+    ids = ids[:, :, 0, :requests].reshape(2 * ring, requests)
+    fits, source, where, table, onward, final = stream_routes(ring, passages, ids)
+
+    def cast_short(ids, source, where, kv, weights):
+        return stream_cast(0, source, where, kv, weights)
+
+    def cast_any(ids, source, where, kv, weights):
+        order, where, _, _ = routes(plan, ids)
+        return cast_rows(plan, 1, order, where, kv, weights)
+
+    def fold_short(ids, table, onward, final, grads, tokens):
+        return stream_fold(2, passages, table, onward, final, grads, tokens)
+
+    def fold_any(ids, table, onward, final, grads, tokens):
+        _, _, table, final = routes(plan, ids)
+        return fold_rows(plan, 3, table, final, grads, tokens)
+
     weights = (w_query, w_gate, w_key, w_value)
     request_kv, wq_far, wg_far, wk_far, wv_far = lax.cond(
-        fits,
-        functools.partial(cast_rows, light, 0),
-        functools.partial(cast_rows, plan, 1),
-        order,
-        where,
-        kv,
-        weights,
+        fits, cast_short, cast_any, ids, source, where, kv, weights
     )
     request_grads, token_grads = attend(queries, gate_pre, d_mem, request_kv)
     sums, tokens_in = lax.cond(
-        fits,
-        functools.partial(fold_rows, light, 2),
-        functools.partial(fold_rows, plan, 3),
-        table,
-        final,
-        request_grads,
-        token_grads,
+        fits, fold_short, fold_any, ids, table, onward, final, request_grads, token_grads
     )
     d_tokens, d_store, d_wkey = tail(
         4,

time: 349 us -> 494 us (1.42); the launches traced: 348 us -> 486 us
  between operations: 2.12 us -> 85.3 us
  other arithmetic: 4.04 us -> 55.3 us
  local copies, waits for them, and re-layouts: 9.68 us -> 49.9 us
  Pallas kernels: 332 us -> 295 us
    pallas_call x2, Pallas kernels: 226 us -> 188 us  [the longest x1 94.9 us: stream_cast(): pl.pallas_call(functools.partial(stream_cast_kernel, len(weights)), out_s...]
    select_n x6 -> x22, other arithmetic: 0.11 us -> 37.1 us  [the longest x1 18.3 us: stream_routes(): jnp.where(step > 0, jnp.where(by_me, count + d * LENGTH + at, -1), slot)]
    slice x1 -> x130, local copies, waits for them, and re-layouts: 0.96 us -> 37 us  [the longest x44 23 us: stream_routes(): a[1]]
    reduce_and x1 -> x15, other arithmetic: 0.72 us -> 10.7 us  [stream_routes(): fits &= jnp.all(starts[-1] + sizes[-1] <= LENGTH)]
    dynamic_slice x3 -> x59, local copies, waits for them, and re-layouts: 0.23 us -> 5.47 us  [the longest x57 4.85 us: own_chip(): return lax.dynamic_slice_in_dim(array, lax.axis_index('st_0'), 1, axis=0)[0]]
where the time goes in v4:
time: 494 us; the launch traced here: 486 us
  Pallas kernels  295 us (60%)
  between operations  85.3 us (17%)
  other arithmetic  55.3 us (11%)
  local copies, waits for them, and re-layouts  49.9 us (10%)
    pallas_call x1, Pallas kernels, stream_cast(): pl.pallas_call(functools.partial(stream_cast_kernel, len(weights)), out_s...  94.9 us
    pallas_call x1, Pallas kernels, stream_fold(): pl.pallas_call(stream_fold_kernel, out_shape=[jax.ShapeDtypeStruct((count...  92.7 us
    pallas_call x1, Pallas kernels, front(): pl.pallas_call(front_kernel, out_shape=[jax.ShapeDtypeStruct((ring, 2, *i...  65.2 us
    pallas_call x1, Pallas kernels, tail(): pl.pallas_call(tail_kernel, out_shape=[jax.ShapeDtypeStruct((tokens.shape...  34 us
    slice x44, local copies, waits for them, and re-layouts, stream_routes(): a[1]  23 us
    select_n x1, other arithmetic, stream_routes(): jnp.where(step > 0, jnp.where(by_me, count + d * LENGTH + at, -1), slot)  18.3 us
    select_n x1, other arithmetic, stream_routes(): jnp.where(step > 0, base + at + jnp.where(by_me, 0, 2 * LENGTH), where)  18.3 us
    reduce_and x15, other arithmetic, stream_routes(): fits &= jnp.all(starts[-1] + sizes[-1] <= LENGTH)  10.7 us

profile of v4, /device:TPU:33, one launch (start us, length us, event | category | flops | bytes accessed | tf_op | source)
XLA Modules:
  0.0 486.0 jit_solution(16436775788049795289)
XLA Ops:
  2.1 0.8 copy.20
  3.7 65.2 %front.1 = (s32[16,2,8,128]{3,2,1,0:T(8,128)}, bf16[4,16,64,512]{3,2,1,0:T(8,128)(2,1)}, bf16[16,64,512]{2,1,0:T(8,128)(2,1)}) custom-call(s32[8,128]{1,0:T(8,128)} %scatter.4.ids_ref, bf16[16,64,512]{2,1,0:T(8,128)(2,1)} %store_ref.1, bf16[2048,256]{1,0:T(8,128)(2,1)} %refs_4_.1, bf16[2048,256]{1,0:T(8,128)(2,1)} %refs_5_.1), custom_call_target="tpu_custom_call" | custom-call | tf_op jit(solution)/shard_map/front/pallas_call | solution.py:181
  68.9 1.0 fusion.194
  70.0 0.7 select_reduce_fusion.14
  75.6 0.7 compare_reduce_fusion.11
  76.4 0.7 compare_reduce_fusion.10
  77.2 0.8 compare_reduce_fusion.9
  139.6 0.8 convert_reduce_fusion.4
  174.0 0.7 compare_reduce_fusion.5
  175.5 0.7 compare_reduce_fusion.4
  176.9 0.7 compare_reduce_fusion.3
  178.3 0.7 compare_reduce_fusion.2
  179.8 0.7 compare_reduce_fusion.1
  181.2 0.7 compare_reduce_fusion
  212.5 18.3 %compare_select_fusion.66 = (s32[2,32]{1,0:T(2,128)S(1)}, s32[2,32]{1,0:T(2,128)S(1)}, s32[2,32]{1,0:T(2,128)S(1)}, s32[2,32]{1,0:T(2,128)S(1)}) fusion(s32[2,32]{1,0:T(2,128)S(1)} %reduce_sum.319, s32[2,32]{1,0:T(2,128)S(1)} %reduce_sum.318, s32[]{:T(128)} %bitcast.39, s32[]{:T(128)} %bitcast.38, s32[]{:T(128)} %bitcast.37, s32[]{:T(128)} %bitcast.36, ...), kind=kLoop, calls=%fused_computation.526 | loop fusion | flops 11072 | bytes 2492 | tf_op jit(solution)/shard_map/jit(_where)/select_n | solution.py:881
  231.2 114.3 %conditional.2 = ((bf16[32,64,512]{2,1,0:T(8,128)(2,1)}, bf16[3,2048,256]{2,1,0:T(8,128)(2,1)}, bf16[3,2048,256]{2,1,0:T(8,128)(2,1)}, bf16[3,2048,256]{2,1,0:T(8,128)(2,1)}, bf16[3,2048,256]{2,1,0:T(8,128)(2,1)})) conditional(s32[]{:T(128)} %convert_element_type.92, (s32[16,2,1,32]{3,2,1,0:T(1,128)S(1)}, s32[32,32]{1,0:T(8,128)S(1)}, ...), branch_computations={%region_40.49_spmd, %region_49.50_spmd.clone.clone} | conditional | flops 3053777 | bytes 118530 | solution.py:1142
  231.7 18.3 %compare_select_fusion.3 = s32[64]{0:T(128)S(1)} fusion(s32[64]{0:T(128)S(1)} %reshape.817, s32[64]{0:T(128)S(1)} %get-tuple-element.1618, s32[64]{0:T(128)S(1)} %reshape.818, pred[64]{0:T(512)(128)(4,1)S(1)} %eq.1006, s32[64]{0:T(128)S(1)} %get-tuple-element.1654, pred[64]{0:T(512)(128)(4,1)S(1)} %get-tuple-element.1639, ...), kind=kLoop, calls=%fused_computation.38 | loop fusion | flops 11008 | bytes 2748 | tf_op jit(solution)/shard_map/jit(_where)/select_n | solution.py:880
  250.6 94.9 %stream_cast.5 = (bf16[32,64,512]{2,1,0:T(8,128)(2,1)}, bf16[3,2048,256]{2,1,0:T(8,128)(2,1)}, bf16[3,2048,256]{2,1,0:T(8,128)(2,1)}, bf16[3,2048,256]{2,1,0:T(8,128)(2,1)}, bf16[3,2048,256]{2,1,0:T(8,128)(2,1)}) custom-call(s32[108]{0:T(128)S(1)} %get-tuple-element.1616.source_ref, s32[32]{0:T(128)} %dynamic_slice.345.where_ref, ...), custom_call_target="tpu_custom_call" | custom-call | tf_op jit(solution)/shard_map/cond/branch_1_fun/stream_cast/pallas_call | solution.py:611
  345.5 8.0 %attend.1 = (bf16[32,64,512]{2,1,0:T(8,128)(2,1)}, bf16[1024,512]{1,0:T(8,128)(2,1)}) custom-call(bf16[1024,256]{1,0:T(8,128)(2,1)} %q_ref.1, bf16[1024,256]{1,0:T(8,128)(2,1)} %gate_ref.1, bf16[1024,256]{1,0:T(8,128)(2,1)} %mem_ref.1, bf16[32,64,512]{2,1,0:T(8,128)(2,1)} %get-tuple-element.1473.kv_ref), custom_call_target="tpu_custom_call" | custom-call | tf_op jit(solution)/shard_map/attend/pallas_call | solution.py:246
  353.5 93.9 %conditional.3 = ((bf16[16,64,512]{2,1,0:T(8,128)(2,1)}, bf16[3,256,512]{2,1,0:T(8,128)(2,1)S(1)})) conditional(s32[]{:T(128)} %convert_element_type.92, (s32[32,32]{1,0:T(8,128)S(1)}, s32[16,2,1,32]{3,2,1,0:T(1,128)S(1)}, bf16[32,64,512]{2,1,0:T(8,128)(2,1)}, bf16[1024,512]{1,0:T(8,128)(2,1)}) %tuple.239, (s32[124,4]{0,1:T(4,128)S(1)}, ...), branch_computations={%region_55.67_spmd, %region_67.68_spmd} | conditional | flops 4145074 | bytes 353532 | solution.py:1146
  354.6 92.7 %stream_fold.1 = (bf16[16,64,512]{2,1,0:T(8,128)(2,1)}, bf16[3,256,512]{2,1,0:T(8,128)(2,1)S(1)}) custom-call(s32[496]{0:T(512)} %reshape.796.table_ref, s32[108]{0:T(128)S(1)} %get-tuple-element.1449.onward_ref, s32[64]{0:T(128)S(1)} %get-tuple-element.1450.final_ref, bf16[32,64,512]{2,1,0:T(8,128)(2,1)} %get-tuple-element.1451.grads_ref, ...), custom_call_target="tpu_custom_call" | custom-call | tf_op jit(solution)/shard_map/cond/branch_1_fun/stream_fold/pallas_call | solution.py:722
  447.5 34.0 %tail.1 = (bf16[256,2048]{1,0:T(8,128)(2,1)}, bf16[256,2048]{1,0:T(8,128)(2,1)}, f32[64,256]{1,0:T(8,128)}) custom-call(bf16[16,64,512]{2,1,0:T(8,128)(2,1)} %get-tuple-element.1476.sums_ref, bf16[4,16,64,512]{3,2,1,0:T(8,128)(2,1)} %get-tuple-element.1477.all_ref, bf16[1024,512]{1,0:T(8,128)(2,1)} %get-tuple-element.1475.tokens_ref, ...), custom_call_target="tpu_custom_call" | custom-call | tf_op jit(solution)/shard_map/tail/pallas_call | solution.py:1034
  481.5 2.4 copy.39
  483.9 1.0 copy.40
  (328 shorter events, 55.5 us)
Async XLA Ops:
  3.7 227.5 %copy-start = (bf16[2048,256]{1,0:T(8,128)(2,1)S(1)}, bf16[2048,256]{1,0:T(8,128)(2,1)}, u32[]{:S(2)}) copy-start(bf16[2048,256]{1,0:T(8,128)(2,1)} %refs_4_.1) | copy-start | bytes 3145732
  481.5 2.4 copy-start.1
  481.5 3.4 copy-start.2

commit v5 on v4

--- a/solution.py
+++ b/solution.py
@@ -543,7 +543,7 @@
             gift.wait_recv()
 
 
-def stream_cast_kernel(weights, source_ref, where_ref, kv_ref, *refs):
+def stream_cast_kernel(weights, table_ref, kv_ref, *refs):
     w_refs, refs = refs[:weights], refs[weights:]
     out_ref, w_outs, refs = refs[0], refs[1 : 1 + weights], refs[1 + weights :]
     kept, land, twin_land, leave, *sems = refs
@@ -577,7 +577,7 @@
 
                 @pl.loop(at, at + STAGE)
                 def _(q):
-                    leave[q] = kept[source_ref[q]]
+                    leave[q] = kept[table_ref[q]]
 
             if 0 <= i - 4 < stages:
                 at = d * length + (i - 4) * STAGE
@@ -597,22 +597,22 @@
 
     @pl.loop(0, out_ref.shape[0])
     def _(r):
-        out_ref[r] = kept[where_ref[r]]
+        out_ref[r] = kept[table_ref[2 * length + r]]
 
     share.wait()
     for group in (gifts, ring_copies, w_copies):
         group.wait_sends()
 
 
-def stream_cast(ident, source, where, kv, weights):
+def stream_cast(ident, table, kv, weights):
     count, rows, cols = kv.shape
     stages = LENGTH // STAGE
     others = lax.axis_size("tp") - 1
     return pl.pallas_call(
         functools.partial(stream_cast_kernel, len(weights)),
-        out_shape=[jax.ShapeDtypeStruct((where.shape[0], rows, cols), kv.dtype)]
+        out_shape=[jax.ShapeDtypeStruct((table.shape[0] - 2 * LENGTH, rows, cols), kv.dtype)]
         + [jax.ShapeDtypeStruct((others, *w.shape), w.dtype) for w in weights],
-        in_specs=[SMEM_SPEC, SMEM_SPEC, VMEM_SPEC] + [ANY_SPEC] * len(weights),
+        in_specs=[SMEM_SPEC, VMEM_SPEC] + [ANY_SPEC] * len(weights),
         out_specs=[VMEM_SPEC] + [ANY_SPEC] * len(weights),
         scratch_shapes=[
             pltpu.VMEM((2 * count + 4 * LENGTH, rows, cols), kv.dtype),
@@ -627,11 +627,11 @@
             collective_id=ident, has_side_effects=True, vmem_limit_bytes=VMEM_LIMIT
         ),
         name="stream_cast",
-    )(source, where, kv, *weights)
+    )(table, kv, *weights)
 
 
 def stream_fold_kernel(
-    table_ref, onward_ref, final_ref, grads_ref, tokens_ref, out_ref, tokens_out, held, kept, land,
+    table_ref, grads_ref, tokens_ref, out_ref, tokens_out, held, kept, land,
     leave, twin_land, load_sem, *sems
 ):
     ring_copies, gifts, exchange = (Copies(*sems[2 * i : 2 * i + 2]) for i in range(3))
@@ -642,6 +642,8 @@
     own = grads_ref.shape[0]
     readers = 2 * MOST
     zero = 2 * length
+    onward_at = (count + 2 * length + 1) * readers
+    final_at = onward_at + 2 * length
     peers = [place.along_x(rel) for rel in range(1, place.tp)]
 
     load = pltpu.make_async_copy(grads_ref, held.at[pl.ds(0, own)], load_sem)
@@ -688,7 +690,7 @@
 
             @pl.loop(at, at + STAGE)
             def _(q):
-                total = readers_sum(count + q) + kept[onward_ref[q]].astype(F32)
+                total = readers_sum(count + q) + kept[table_ref[onward_at + q]].astype(F32)
                 leave[q] = total.astype(leave.dtype)
 
         for d in range(2):
@@ -705,8 +707,8 @@
     def _(p):
         total = readers_sum(p)
         for d in range(2):
-            total += kept[final_ref[d * count + p]].astype(F32)
-            total += twin_land[final_ref[(2 + d) * count + p]].astype(F32)
+            total += kept[table_ref[final_at + d * count + p]].astype(F32)
+            total += twin_land[table_ref[final_at + (2 + d) * count + p]].astype(F32)
         out_ref[p] = total.astype(out_ref.dtype)
 
     for copy in exchange.all:
@@ -715,7 +717,7 @@
         group.wait_sends()
 
 
-def stream_fold(ident, count, table, onward, final, grads, tokens):
+def stream_fold(ident, count, table, grads, tokens):
     own, rows, cols = grads.shape
     stages = LENGTH // STAGE
     tp = lax.axis_size("tp")
@@ -725,7 +727,7 @@
             jax.ShapeDtypeStruct((count, rows, cols), grads.dtype),
             jax.ShapeDtypeStruct((tp - 1, tokens.shape[0] // tp, tokens.shape[1]), tokens.dtype),
         ],
-        in_specs=[SMEM_SPEC, SMEM_SPEC, SMEM_SPEC, ANY_SPEC, ANY_SPEC],
+        in_specs=[SMEM_SPEC, ANY_SPEC, ANY_SPEC],
         out_specs=[VMEM_SPEC, ANY_SPEC],
         scratch_shapes=[
             pltpu.VMEM((2 * own + 1, rows, cols), grads.dtype),
@@ -742,14 +744,7 @@
             collective_id=ident, has_side_effects=True, vmem_limit_bytes=VMEM_LIMIT
         ),
         name="stream_fold",
-    )(table, onward, final, grads, tokens)
-
-
-def summed(pairs, start):
-    total = start
-    for holds, value in pairs:
-        total = total + jnp.where(holds, value, 0)
-    return total
+    )(table, grads, tokens)
 
 
 def readers_table(slot, slots, requests):
@@ -795,97 +790,165 @@
     return lax.dynamic_slice_in_dim(array, 2 * lax.axis_index("st_0"), 2, axis=0).reshape(-1)
 
 
+def routes_kernel(count, requests, size_ref, info_ref, fits_ref, cast_ref, fold_ref, starts, start, size, used, sem):
+    z, k = lax.axis_index("st_0"), lax.axis_index("st_1")
+    ring = lax.axis_size("st_0")
+    reach = ring // 2
+    pair = 2 * count
+    twin_at = 2 * LENGTH
+    lane = lax.broadcasted_iota(jnp.int32, starts.shape, 1)
+    lanes = starts.shape[1]
+    spot = lane % ring
+    up = lane < 2 * ring
+    now = jnp.zeros(starts.shape, jnp.int32)
+    most = jnp.zeros(starts.shape, jnp.int32)
+    for t in range(reach):
+        if t > 0:
+            ends = now + jnp.broadcast_to(size_ref[t - 1 : t, :], starts.shape)
+            after = jnp.where(
+                spot == ring - 1, pltpu.roll(ends, ring - 1, 1), pltpu.roll(ends, lanes - 1, 1)
+            )
+            before = jnp.where(
+                spot == 0, pltpu.roll(ends, lanes - ring + 1, 1), pltpu.roll(ends, 1, 1)
+            )
+            now = jnp.maximum(jnp.where(up, after, before), now + LAG)
+        starts[t : t + 1, :] = now[0:1, :]
+        here = now + jnp.broadcast_to(size_ref[t : t + 1, :], starts.shape)
+        most = jnp.maximum(most, jnp.where(lane < 4 * ring, here, 0))
+    fits_ref[0] = (jnp.max(most) <= LENGTH).astype(jnp.int32)
+    for n, (src, dst) in enumerate(((starts, start), (size_ref, size))):
+        copy = pltpu.make_async_copy(src, dst, sem.at[n])
+        copy.start()
+        copy.wait()
+
+    slots = count + 2 * LENGTH
+    readers = 2 * MOST
+    onward_at, final_at = (slots + 1) * readers, (slots + 1) * readers + 2 * LENGTH
+
+    @pl.loop(0, onward_at)
+    def _(i):
+        fold_ref[i] = 2 * requests
+
+    @pl.loop(0, slots + 1)
+    def _(i):
+        used[i] = 0
+
+    @pl.loop(0, 2 * LENGTH)
+    def _(i):
+        fold_ref[onward_at + i] = 2 * LENGTH
+        cast_ref[i] = 0
+
+    def info(row, i):
+        return info_ref[row * 2 * requests + i]
+
+    def column(d, core, step):
+        source = lax.rem(z - (1 - 2 * d) * step + 2 * ring, ring)
+        return (2 * d + core) * ring + source
+
+    last = LENGTH - 1
+    for d in range(2):
+
+        @pl.loop(0, pair)
+        def _(p):
+            rank = info(5, d * pair + p)
+            far = info(6, d * pair + p)
+            core = lax.div(p, count)
+            mine = rank % 2 == k
+            home = p % count + jnp.where(core == k, 0, count)
+
+            @pl.when(mine)
+            def _():
+                cast_ref[d * LENGTH + rank // 2] = home
+
+            @pl.when(core == k)
+            def _():
+                i = p % count
+                near = jnp.where((far > 0) & mine, d * LENGTH + rank // 2, 2 * LENGTH)
+                aside = jnp.where((far > 0) & (rank % 2 != k), d * count + rank // 2, 2 * count)
+                fold_ref[final_at + d * count + i] = near
+                fold_ref[final_at + (2 + d) * count + i] = aside
+
+        for t in range(1, reach):
+            lane_of = column(d, k, t)
+            at_out, at_in = start[t, lane_of], start[t - 1, lane_of]
+
+            @pl.loop(0, size[t, lane_of])
+            def _(r):
+                out = d * LENGTH + jnp.minimum(at_out + r, last)
+                come = d * LENGTH + jnp.minimum(at_in + r, last)
+                cast_ref[out] = pair + come
+                fold_ref[onward_at + come] = out
+
+    @pl.loop(0, 2 * requests)
+    def _(i):
+        c = lax.rem(i + k * requests, 2 * requests)
+        step, way, rank, within, owner = (info(row, c) for row in range(5))
+        core = jnp.where(step > 0, rank % 2, owner)
+        lane_of = column(way, core, step)
+        at = start[jnp.maximum(step - 1, 0), lane_of] + lax.div(rank, 2)
+        at = way * LENGTH + jnp.minimum(at, last)
+        where = pair + at + jnp.where(core == k, 0, twin_at)
+        where = jnp.where(step > 0, where, within + jnp.where(core == k, 0, count))
+        slot = jnp.where(core == k, jnp.where(step > 0, count + at, within), slots)
+        turn = jnp.where(slot == slots, 0, jnp.minimum(used[slot], readers - 1))
+        used[slot] = turn + 1
+        fold_ref[slot * readers + turn] = i
+
+        @pl.when(i < requests)
+        def _():
+            cast_ref[2 * LENGTH + i] = where
+
+
 def stream_routes(ring, count, ids):
-    me_k = lax.axis_index("st_1")
-    requests = ids.shape[1]
+    devices, requests = ids.shape
     pair = 2 * count
     reach = ring // 2
     owner_k, steps, fars, ranks = needs(ring, count, ids)
+    dist = jnp.arange(1, reach + 1, dtype=jnp.int32)
     core = jnp.arange(2, dtype=jnp.int32)
-    spot = jnp.arange(LENGTH, dtype=jnp.int32)
-    place = jnp.arange(pair, dtype=jnp.int32)
-    at_home = place % count + jnp.where(place // count == me_k, 0, count)
-    want = 2 * jnp.arange(count, dtype=jnp.int32) + me_k
+    far = jnp.stack(fars)
+    whole = jnp.sum((far[None] >= dist[:, None, None, None]).astype(jnp.int32), axis=3)
+    size = (whole[:, :, None, :] + 1 - core[None, None, :, None]) // 2
+    size = jnp.pad(size.reshape(reach, 4 * ring), ((0, 0), (0, 128 - 4 * ring)))
     chip_ids = chip_requests(ids)
-    every = jnp.arange(ids.shape[0] * count, dtype=jnp.int32)
+    every = jnp.arange(devices * count, dtype=jnp.int32)
     chip_hot = chip_ids[:, None] == every[None, :]
-    chip_owner = chip_requests(owner_k)
-    within = chip_ids % count
-    where = within + jnp.where(chip_owner == me_k, 0, count)
-    slot = jnp.where(chip_owner == me_k, within, -1)
-    fits = jnp.bool_(True)
-    source, onward, near, aside = [], [], [], []
-    for d in range(2):
-        turn = 1 - 2 * d
-        sizes, starts = [], []
-        for t in range(1, reach + 1):
-            whole = jnp.sum((fars[d] >= t).astype(jnp.int32), axis=1)[:, None]
-            sizes.append((whole + 1 - core[None, :]) // 2)
-            if t == 1:
-                starts.append(jnp.zeros_like(sizes[0]))
-            else:
-                behind = jnp.roll(starts[-1] + sizes[-2], -turn, axis=0)
-                starts.append(jnp.maximum(behind, starts[-1] + LAG))
-            fits &= jnp.all(starts[-1] + sizes[-1] <= LENGTH)
-        out_size = [own_chip(jnp.roll(a, turn * t, axis=0)) for t, a in enumerate(sizes)]
-        out_at = [own_chip(jnp.roll(a, turn * t, axis=0)) for t, a in enumerate(starts)]
-        in_size = [own_chip(jnp.roll(a, turn * (t + 1), axis=0)) for t, a in enumerate(sizes)]
-        in_at = [own_chip(jnp.roll(a, turn * (t + 1), axis=0)) for t, a in enumerate(starts)]
-        mine = [
-            [jnp.where(me_k == 0, a[0], a[1]) for a in array]
-            for array in (out_size, out_at, in_size, in_at)
+    step = [chip_requests(s) for s in steps]
+    way = (step[1] > 0).astype(jnp.int32)
+    ranked = [jnp.sum(jnp.where(chip_hot, r.reshape(-1)[None, :], 0), axis=1) for r in ranks]
+    info = jnp.concatenate(
+        [
+            step[0] + step[1],
+            way,
+            jnp.where(way == 0, ranked[0], ranked[1]),
+            chip_ids % count,
+            chip_requests(owner_k),
+            own_chip(ranks[0]),
+            own_chip(ranks[1]),
+            own_chip(fars[0]),
+            own_chip(fars[1]),
         ]
-        size_o, at_o, size_i, at_i = mine
-        rank, far = own_chip(ranks[d]), own_chip(fars[d])
-        order = jnp.sum(jnp.where(rank[None, :] == want[:, None], at_home[None, :], 0), axis=1)
-        order = jnp.concatenate([order, jnp.zeros((LENGTH - count,), order.dtype)])
-        base = pair + d * LENGTH
-        source.append(
-            summed(
-                [
-                    ((spot >= at_o[t]) & (spot < at_o[t] + size_o[t]), base + at_i[t - 1] + spot - at_o[t])
-                    for t in range(1, reach)
-                ],
-                jnp.where(spot < size_o[0], order, 0),
-            )
-        )
-        onward.append(
-            summed(
-                [
-                    (
-                        (spot >= at_i[t]) & (spot < at_i[t] + jnp.minimum(size_i[t], size_o[t + 1])),
-                        d * LENGTH + at_o[t + 1] + spot - at_i[t] - 2 * LENGTH,
-                    )
-                    for t in range(reach - 1)
-                ],
-                jnp.full((LENGTH,), 2 * LENGTH, jnp.int32),
-            )
-        )
-        index = lax.dynamic_slice_in_dim(rank, me_k * count, count)
-        used = lax.dynamic_slice_in_dim(far, me_k * count, count) > 0
-        same = index % 2 == me_k
-        near.append(jnp.where(used & same, d * LENGTH + index // 2, 2 * LENGTH))
-        aside.append(jnp.where(used & ~same, d * count + index // 2, 2 * count))
-        step = chip_requests(steps[d])
-        ranked = jnp.sum(jnp.where(chip_hot, ranks[d].reshape(-1)[None, :], 0), axis=1)
-        at = summed(
-            [
-                ((step == t + 1) & (ranked % 2 == c), in_at[t][c])
-                for t in range(reach)
-                for c in range(2)
-            ],
-            ranked // 2,
-        )
-        by_me = ranked % 2 == me_k
-        where = jnp.where(step > 0, base + at + jnp.where(by_me, 0, 2 * LENGTH), where)
-        slot = jnp.where(step > 0, jnp.where(by_me, count + d * LENGTH + at, -1), slot)
-    where = lax.dynamic_slice_in_dim(where, me_k * requests, requests)
-    slot = slot.reshape(2, requests)
-    slot = jnp.where(me_k == 0, slot, slot[::-1]).reshape(-1)
-    table = readers_table(slot, count + 2 * LENGTH, 2 * requests)
-    tables = (jnp.concatenate(source), where, jnp.concatenate(onward), jnp.concatenate(near + aside))
-    source, where, onward, final = (t.astype(jnp.int32) for t in tables)
-    return fits, source, where, table, onward, final
+    ).astype(jnp.int32)
+    slots = count + 2 * LENGTH
+    fold_size = (slots + 1) * 2 * MOST + 2 * LENGTH + 4 * count
+    return pl.pallas_call(
+        functools.partial(routes_kernel, count, requests),
+        out_shape=[
+            jax.ShapeDtypeStruct((1,), jnp.int32),
+            jax.ShapeDtypeStruct((2 * LENGTH + requests,), jnp.int32),
+            jax.ShapeDtypeStruct((fold_size,), jnp.int32),
+        ],
+        in_specs=[VMEM_SPEC, SMEM_SPEC],
+        out_specs=[SMEM_SPEC] * 3,
+        scratch_shapes=[
+            pltpu.VMEM((reach, 128), jnp.int32),
+            pltpu.SMEM((reach, 128), jnp.int32),
+            pltpu.SMEM((reach, 128), jnp.int32),
+            pltpu.SMEM((slots + 1,), jnp.int32),
+            pltpu.SemaphoreType.DMA((2,)),
+        ],
+        name="routes",
+    )(size, info)
 
 
 def project(rows_list, weight_list, out_ref, n, tile):
@@ -1122,29 +1185,30 @@
     ids = jnp.zeros((8, 128), jnp.int32).at[0, :requests].set(pass_ids.reshape(-1))
     ids, all_rows, kv = front(5, ids, store, w_key, w_value)
     ids = ids[:, :, 0, :requests].reshape(2 * ring, requests)
-    fits, source, where, table, onward, final = stream_routes(ring, passages, ids)
-
-    def cast_short(ids, source, where, kv, weights):
-        return stream_cast(0, source, where, kv, weights)
-
-    def cast_any(ids, source, where, kv, weights):
+    fits, cast_table, fold_table = stream_routes(ring, passages, ids)
+    fits = fits[0] > 0
+
+    def cast_short(ids, table, kv, weights):
+        return stream_cast(0, table, kv, weights)
+
+    def cast_any(ids, table, kv, weights):
         order, where, _, _ = routes(plan, ids)
         return cast_rows(plan, 1, order, where, kv, weights)
 
-    def fold_short(ids, table, onward, final, grads, tokens):
-        return stream_fold(2, passages, table, onward, final, grads, tokens)
-
-    def fold_any(ids, table, onward, final, grads, tokens):
+    def fold_short(ids, table, grads, tokens):
+        return stream_fold(2, passages, table, grads, tokens)
+
+    def fold_any(ids, table, grads, tokens):
         _, _, table, final = routes(plan, ids)
         return fold_rows(plan, 3, table, final, grads, tokens)
 
     weights = (w_query, w_gate, w_key, w_value)
     request_kv, wq_far, wg_far, wk_far, wv_far = lax.cond(
-        fits, cast_short, cast_any, ids, source, where, kv, weights
+        fits, cast_short, cast_any, ids, cast_table, kv, weights
     )
     request_grads, token_grads = attend(queries, gate_pre, d_mem, request_kv)
     sums, tokens_in = lax.cond(
-        fits, fold_short, fold_any, ids, table, onward, final, request_grads, token_grads
+        fits, fold_short, fold_any, ids, fold_table, request_grads, token_grads
     )
     d_tokens, d_store, d_wkey = tail(
         4,

time: 494 us -> 320 us (0.65); the launches traced: 486 us -> 320 us
  between operations: 85.3 us -> 1.45 us
  other arithmetic: 55.3 us -> 2.36 us
  local copies, waits for them, and re-layouts: 49.9 us -> 8.96 us
  Pallas kernels: 295 us -> 307 us
    select_n x19 -> x2, other arithmetic: 37 us -> 0.02 us  [the longest x1 0.01 us: stream_routes(): size = (whole[:, :, None, :] + 1 - core[None, None, :, None]) // 2]
    slice x129 -> x0, local copies, waits for them, and re-layouts: 36 us -> none  [the longest x44 23 us: stream_routes(): a[1]]
    pallas_call x0 -> x1, Pallas kernels: none -> 12.2 us  [stream_routes(): pl.pallas_call(functools.partial(routes_kernel, count, requests), out_sha...]
    reduce_and x15 -> x0, other arithmetic: 10.7 us -> none  [stream_routes(): fits &= jnp.all(starts[-1] + sizes[-1] <= LENGTH)]
    dynamic_slice x58 -> x0, local copies, waits for them, and re-layouts: 5.46 us -> none  [the longest x57 4.85 us: own_chip(): return lax.dynamic_slice_in_dim(array, lax.axis_index('st_0'), 1, axis=0)[0]]
where the time goes in v5:
time: 320 us
  Pallas kernels  307 us (96%)
  local copies, waits for them, and re-layouts  8.96 us (3%)
    pallas_call x1, Pallas kernels, stream_cast(): pl.pallas_call(functools.partial(stream_cast_kernel, len(weights)), out_s...  95.1 us
    pallas_call x1, Pallas kernels, stream_fold(): pl.pallas_call(stream_fold_kernel, out_shape=[jax.ShapeDtypeStruct((count...  92.5 us
    pallas_call x1, Pallas kernels, front(): pl.pallas_call(front_kernel, out_shape=[jax.ShapeDtypeStruct((ring, 2, *i...  65.1 us
    pallas_call x1, Pallas kernels, tail(): pl.pallas_call(tail_kernel, out_shape=[jax.ShapeDtypeStruct((tokens.shape...  33.9 us
    pallas_call x1, Pallas kernels, stream_routes(): pl.pallas_call(functools.partial(routes_kernel, count, requests), out_sha...  12.2 us
    pallas_call x1, Pallas kernels, attend(): pl.pallas_call(functools.partial(attend_kernel, HD ** (-0.5)), grid=(grid...  8.03 us

profile of v5, /device:TPU:33, one launch (start us, length us, event | category | flops | bytes accessed | tf_op | source)
XLA Modules:
  0.0 319.8 jit_solution(1336462856071261041)
XLA Ops:
  0.8 0.8 copy.16
  1.7 0.6 scatter.4.ids_ref
  2.4 65.1 %front.1 = (s32[16,2,8,128]{3,2,1,0:T(8,128)}, bf16[4,16,64,512]{3,2,1,0:T(8,128)(2,1)}, bf16[16,64,512]{2,1,0:T(8,128)(2,1)}) custom-call(s32[8,128]{1,0:T(8,128)} %scatter.4.ids_ref, bf16[16,64,512]{2,1,0:T(8,128)(2,1)} %store_ref.1, bf16[2048,256]{1,0:T(8,128)(2,1)} %refs_4_.1, bf16[2048,256]{1,0:T(8,128)(2,1)} %refs_5_.1), custom_call_target="tpu_custom_call" | custom-call | tf_op jit(solution)/shard_map/front/pallas_call | solution.py:181
  67.5 1.0 fusion.90
  68.5 0.1 eq.421
  68.6 0.1 eq.430
  68.7 0.7 select_reduce_fusion.15
  69.7 0.8 convert_reduce_fusion.4
  70.6 0.2 select_reduce_fusion.16
  70.9 0.4 convert_reduce_fusion.6
  71.4 0.1 sub.162
  71.5 0.6 pad.9.size_ref
  72.1 0.1 and_or_fusion.2
  72.5 0.7 concatenate.11.info_ref
  73.1 12.2 %routes.1 = (s32[1]{0:T(128)}, s32[140]{0:T(256)S(1)}, s32[672]{0:T(1024)S(1)}) custom-call(s32[8,128]{1,0:T(8,128)} %pad.9.size_ref, s32[448]{0:T(512)} %concatenate.11.info_ref), custom_call_target="tpu_custom_call" | custom-call | tf_op jit(solution)/shard_map/routes/pallas_call | solution.py:934
  86.0 95.3 %conditional.2 = ((bf16[32,64,512]{2,1,0:T(8,128)(2,1)}, bf16[3,2048,256]{2,1,0:T(8,128)(2,1)}, bf16[3,2048,256]{2,1,0:T(8,128)(2,1)}, bf16[3,2048,256]{2,1,0:T(8,128)(2,1)}, bf16[3,2048,256]{2,1,0:T(8,128)(2,1)})) conditional(s32[]{:T(128)} %bitcast.15, (s32[16,2,1,32]{3,2,1,0:T(1,128)S(1)}, s32[32,32]{1,0:T(8,128)S(1)}, ...), branch_computations={%region_7.16_spmd, %region_16.17_spmd} | conditional | flops 3053777 | bytes 118530 | solution.py:1206
  86.2 95.1 %stream_cast.1 = (bf16[32,64,512]{2,1,0:T(8,128)(2,1)}, bf16[3,2048,256]{2,1,0:T(8,128)(2,1)}, bf16[3,2048,256]{2,1,0:T(8,128)(2,1)}, bf16[3,2048,256]{2,1,0:T(8,128)(2,1)}, bf16[3,2048,256]{2,1,0:T(8,128)(2,1)}) custom-call(s32[140]{0:T(256)S(1)} %get-tuple-element.59.table_ref, bf16[16,64,512]{2,1,0:T(8,128)(2,1)} %get-tuple-element.60.kv_ref, ...), custom_call_target="tpu_custom_call" | custom-call | tf_op jit(solution)/shard_map/cond/branch_1_fun/stream_cast/pallas_call | solution.py:611
  181.3 8.0 %attend.1 = (bf16[32,64,512]{2,1,0:T(8,128)(2,1)}, bf16[1024,512]{1,0:T(8,128)(2,1)}) custom-call(bf16[1024,256]{1,0:T(8,128)(2,1)} %q_ref.1, bf16[1024,256]{1,0:T(8,128)(2,1)} %gate_ref.1, bf16[1024,256]{1,0:T(8,128)(2,1)} %mem_ref.1, bf16[32,64,512]{2,1,0:T(8,128)(2,1)} %get-tuple-element.97.kv_ref), custom_call_target="tpu_custom_call" | custom-call | tf_op jit(solution)/shard_map/attend/pallas_call | solution.py:246
  189.3 92.5 %conditional.3 = ((bf16[16,64,512]{2,1,0:T(8,128)(2,1)}, bf16[3,256,512]{2,1,0:T(8,128)(2,1)S(1)})) conditional(s32[]{:T(128)} %bitcast.15, (s32[32,32]{1,0:T(8,128)S(1)}, s32[16,2,1,32]{3,2,1,0:T(1,128)S(1)}, bf16[32,64,512]{2,1,0:T(8,128)(2,1)}, bf16[1024,512]{1,0:T(8,128)(2,1)}) %tuple.70, (s32[672]{0:T(1024)S(1)}, ...), branch_computations={%region_17.29_spmd, %region_29.30_spmd} | conditional | flops 4145074 | bytes 353532 | solution.py:1210
  189.3 92.5 %stream_fold.1 = (bf16[16,64,512]{2,1,0:T(8,128)(2,1)}, bf16[3,256,512]{2,1,0:T(8,128)(2,1)S(1)}) custom-call(s32[672]{0:T(1024)S(1)} %get-tuple-element.69.table_ref, bf16[32,64,512]{2,1,0:T(8,128)(2,1)} %get-tuple-element.70.grads_ref, bf16[1024,512]{1,0:T(8,128)(2,1)} %get-tuple-element.71.tokens_ref), custom_call_target="tpu_custom_call" | custom-call | tf_op jit(solution)/shard_map/cond/branch_1_fun/stream_fold/pallas_call | solution.py:724
  281.9 33.9 %tail.1 = (bf16[256,2048]{1,0:T(8,128)(2,1)}, bf16[256,2048]{1,0:T(8,128)(2,1)}, f32[64,256]{1,0:T(8,128)}) custom-call(bf16[16,64,512]{2,1,0:T(8,128)(2,1)} %get-tuple-element.101.sums_ref, bf16[4,16,64,512]{3,2,1,0:T(8,128)(2,1)} %get-tuple-element.102.all_ref, bf16[1024,512]{1,0:T(8,128)(2,1)} %get-tuple-element.99.tokens_ref, ...), custom_call_target="tpu_custom_call" | custom-call | tf_op jit(solution)/shard_map/tail/pallas_call | solution.py:1097
  315.8 2.4 copy.34
  318.2 1.0 copy.35
  319.2 0.6 copy.36
  (35 shorter events, 1.2 us)
Async XLA Ops:
  0.6 85.3 %copy-start = (bf16[2048,256]{1,0:T(8,128)(2,1)S(1)}, bf16[2048,256]{1,0:T(8,128)(2,1)}, u32[]{:S(2)}) copy-start(bf16[2048,256]{1,0:T(8,128)(2,1)} %refs_4_.1) | copy-start | bytes 3145732
  315.8 2.4 copy-start.1
  315.8 3.4 %copy-start.2 = (f32[64,256]{1,0:T(8,128)S(1)}, f32[64,256]{1,0:T(8,128)}, u32[]{:S(2)}) copy-start(f32[64,256]{1,0:T(8,128)} %get-tuple-element.180) | copy-start | bytes 196612

commit v6 on v5

--- a/solution.py
+++ b/solution.py
@@ -107,95 +107,93 @@
     return [pltpu.SemaphoreType.DMA((count,)), pltpu.SemaphoreType.DMA((count,))]
 
 
-def front_kernel(ids_ref, store_ref, wk_ref, wv_ref, ids_out, all_out, kv_out, total, *sems):
-    gifts, ring_copies, x_copies = (Copies(*sems[2 * i : 2 * i + 2]) for i in range(3))
+def ids_kernel(ids_ref, ids_out, *sems):
+    gifts, ring_copies = (Copies(*sems[2 * i : 2 * i + 2]) for i in range(2))
     place = Place()
-    count = store_ref.shape[0]
-    half = count // 2
     reach = place.ring // 2
-    greet(place.along_z(1), place.along_z(-1), place.along_x(1), place.along_x(-1), place.twin)
-    halves = (pl.ds(0, half), pl.ds(half, half))
-    near = {}
-    for d, step in ((0, 1), (1, -1)):
-        for h in (d, 1 - d):
-            near[d, h] = x_copies.start(
-                store_ref.at[halves[h]], all_out.at[place.x, halves[h]], place.along_x(step)
-            )
+    greet(place.along_z(1), place.along_z(-1), place.twin)
     gift = gifts.start(ids_ref, ids_out.at[place.z, place.k], place.twin)
     ids_out[place.z, place.k] = ids_ref[...]
-    all_out[place.x] = store_ref[...]
     gift.wait_recv()
     hops = {}
-
-    def hop(d, t):
-        source = lax.rem(place.z + (t - 1) * (2 * d - 1) + place.ring, place.ring)
-        part = ids_out.at[source]
-        hops[d, t] = ring_copies.start(part, part, place.along_z(1 - 2 * d))
-
-    def hops_until(first, last):
-        for t in range(first, last):
-            for d in range(2):
-                if t > 1 and t <= reach - d:
-                    hops[d, t - 1].wait_recv()
-                if t <= reach - d:
-                    hop(d, t)
-
-    def add(source, start):
-        rows = total.shape[0]
-        depth = store_ref.shape[2]
-        cols = wk_ref.shape[1]
-        part = all_out[source].reshape(rows, depth)
-        w_rows = pl.ds(pl.multiple_of(source * depth, depth), depth)
-        for c, w_ref in enumerate((wk_ref, wv_ref)):
-            at = slice(c * cols, (c + 1) * cols)
-            term = jnp.dot(part, w_ref[w_rows, :], preferred_element_type=F32)
-            total[:, at] = term if start else total[:, at] + term
-
-    hops_until(1, 4)
-    add(place.x, True)
-    hops_until(4, 6)
-    far = []
-    for d, step in ((0, 1), (1, -1)):
-        near[d, d].wait_recv()
-        source = lax.rem(place.x - step + place.tp, place.tp)
-        part = all_out.at[source, halves[d]]
-        far.append(x_copies.start(part, part, place.along_x(step)))
-    hops_until(6, reach + 1)
-    for d, step in ((0, 1), (1, -1)):
-        near[d, 1 - d].wait_recv()
-        add(lax.rem(place.x - step + place.tp, place.tp), False)
+    for t in range(1, reach + 1):
+        for d in range(2):
+            if t > reach - d:
+                continue
+            if t > 1:
+                hops[d, t - 1].wait_recv()
+            source = lax.rem(place.z + (t - 1) * (2 * d - 1) + place.ring, place.ring)
+            part = ids_out.at[source]
+            hops[d, t] = ring_copies.start(part, part, place.along_z(1 - 2 * d))
     for d in range(2):
         hops[d, reach - d].wait_recv()
-    for copy in far:
-        copy.wait_recv()
-    add(lax.rem(place.x + 2, place.tp), False)
-    kv_out[...] = total[...].reshape(kv_out.shape).astype(kv_out.dtype)
-    for group in (gifts, ring_copies, x_copies):
+    for group in (gifts, ring_copies):
         group.wait_sends()
 
 
-def front(ident, ids, store, w_key, w_value):
-    count, rows, cols = store.shape
-    ring, tp = lax.axis_size("st_0"), lax.axis_size("tp")
+def gather_ids(ident, ids):
+    ring = lax.axis_size("st_0")
+    return pl.pallas_call(
+        ids_kernel,
+        out_shape=jax.ShapeDtypeStruct((ring, 2, *ids.shape), ids.dtype),
+        in_specs=[VMEM_SPEC],
+        out_specs=VMEM_SPEC,
+        scratch_shapes=copy_sems(1) + copy_sems(ring - 1),
+        compiler_params=pltpu.CompilerParams(
+            collective_id=ident, has_side_effects=True, vmem_limit_bytes=8 * 1024 * 1024
+        ),
+        cost_estimate=pl.CostEstimate(flops=9 * 10**9, bytes_accessed=10**6, transcendentals=0),
+        name="gather_ids",
+    )(ids)
+
+
+def keys_values_kernel(own_ref, ahead_ref, behind_ref, low_ref, high_ref, wk_ref, wv_ref, kv_ref):
+    x, tp = lax.axis_index("tp"), lax.axis_size("tp")
+    count, pass_len, depth = own_ref.shape
+    rows, cols = count * pass_len, wk_ref.shape[1]
+    early = pl.program_id(0) < pl.num_programs(0) // 2
+    opposite = jnp.where(early, low_ref[...], high_ref[...])
+    parts = (own_ref[...], ahead_ref[...], opposite, behind_ref[...])
+    for c, w_ref in enumerate((wk_ref, wv_ref)):
+        total = None
+        for rel, part in enumerate(parts):
+            at = pl.multiple_of(lax.rem(x + rel, tp) * depth, depth)
+            weight = w_ref[pl.ds(at, depth), :]
+            term = jnp.dot(part.reshape(rows, depth), weight, preferred_element_type=F32)
+            total = term if total is None else total + term
+        at = slice(c * cols, (c + 1) * cols)
+        kv_ref[:, :, at] = total.reshape(count, pass_len, cols).astype(kv_ref.dtype)
+
+
+def keys_values(pieces, w_key, w_value):
+    count, rows, depth = pieces[0].shape
     pair = 2 * w_key.shape[1]
+    steps = 4
+    block = (count // steps, rows, depth)
+    whole = pl.BlockSpec(block, lambda i: (i, 0, 0))
+    low = pl.BlockSpec(block, lambda i: (jnp.minimum(i, steps // 2 - 1), 0, 0))
+    high = pl.BlockSpec(block, lambda i: (jnp.maximum(i - steps // 2, 0), 0, 0))
+    weight = pl.BlockSpec(w_key.shape, lambda i: (0, 0))
     return pl.pallas_call(
-        front_kernel,
-        out_shape=[
-            jax.ShapeDtypeStruct((ring, 2, *ids.shape), ids.dtype),
-            jax.ShapeDtypeStruct((tp, *store.shape), store.dtype),
-            jax.ShapeDtypeStruct((count, rows, pair), store.dtype),
-        ],
-        in_specs=[VMEM_SPEC] * 4,
-        out_specs=[VMEM_SPEC] * 3,
-        scratch_shapes=[pltpu.VMEM((count * rows, pair), F32)]
-        + copy_sems(1)
-        + copy_sems(ring - 1)
-        + copy_sems(6),
-        compiler_params=pltpu.CompilerParams(
-            collective_id=ident, has_side_effects=True, vmem_limit_bytes=VMEM_LIMIT
-        ),
-        name="front",
-    )(ids, store, w_key, w_value)
+        keys_values_kernel,
+        grid=(steps,),
+        out_shape=jax.ShapeDtypeStruct((count, rows, pair), pieces[0].dtype),
+        in_specs=[whole, whole, whole, low, high, weight, weight],
+        out_specs=pl.BlockSpec((count // steps, rows, pair), lambda i: (i, 0, 0)),
+        name="keys_values",
+    )(*pieces, w_key, w_value)
+
+
+def gather_store(store):
+    tp = lax.axis_size("tp")
+    half = store.shape[0] // 2
+    up = [(i, (i + 1) % tp) for i in range(tp)]
+    down = [(i, (i - 1) % tp) for i in range(tp)]
+    behind = lax.ppermute(store, "tp", up)
+    ahead = lax.ppermute(store, "tp", down)
+    low = lax.ppermute(behind[:half], "tp", up)
+    high = lax.ppermute(ahead[half:], "tp", down)
+    return store, ahead, behind, low, high
 
 
 def attend_kernel(scale, q_ref, gate_ref, mem_ref, kv_ref, grads_ref, tokens_ref):
@@ -519,16 +517,16 @@
                 src, dst = w_ref.at[self.half], w_out.at[slot, self.half]
                 self.near.append(copies.start(src, dst, place.along_x(step)))
 
-    def forward(self):
-        for copy in self.near:
+    def forward(self, n):
+        for copy in self.near[2 * n : 2 * n + 2]:
             copy.wait_recv()
-        for w_out in self.outs:
-            src = w_out.at[2 * self.place.k, self.half]
-            dst = w_out.at[1, self.half]
-            device = self.place.along_x(2 * self.place.k - 1)
-            self.middle.append(self.copies.start(src, dst, device))
-            for slot in (0, 2):
-                self.give(w_out.at[slot, self.half])
+        w_out = self.outs[n]
+        src = w_out.at[2 * self.place.k, self.half]
+        dst = w_out.at[1, self.half]
+        device = self.place.along_x(2 * self.place.k - 1)
+        self.middle.append(self.copies.start(src, dst, device))
+        for slot in (0, 2):
+            self.give(w_out.at[slot, self.half])
 
     def give(self, part):
         self.gifts.append(self.copies.start(part, part, self.place.twin))
@@ -591,8 +589,8 @@
                 )
         if i == 1:
             share = WeightShare(place, w_copies, w_refs, w_outs)
-        if i == 2 * stages // 3:
-            share.forward()
+        if i in (6, 10, 14, 18):
+            share.forward((i - 6) // 4)
     share.finish()
 
     @pl.loop(0, out_ref.shape[0])
@@ -947,6 +945,7 @@
             pltpu.SMEM((slots + 1,), jnp.int32),
             pltpu.SemaphoreType.DMA((2,)),
         ],
+        cost_estimate=pl.CostEstimate(flops=6 * 10**9, bytes_accessed=10**5, transcendentals=0),
         name="routes",
     )(size, info)
 
@@ -962,7 +961,8 @@
     out_ref[:, cols] = total.astype(out_ref.dtype)
 
 
-def tail_kernel(sums_ref, all_ref, tokens_ref, tokens_in, *refs):
+def tail_kernel(sums_ref, tokens_ref, tokens_in, *refs):
+    pieces, refs = refs[:5], refs[5:]
     weights, refs = refs[:8], refs[8:]
     d_tokens_ref, d_store_ref, d_wkey_ref = refs[:3]
     wbuf_t, wbuf_s, own_t, in_t, own_s, in_s, refs = *refs[3:9], refs[9:]
@@ -981,8 +981,13 @@
         loads.append(copy)
 
     load(sums_ref, keys)
-    for n in range(tp):
-        load(all_ref.at[n], all_buf.at[n])
+    own_piece, ahead, behind, low, high = pieces
+    part = low.shape[0]
+    load(own_piece, all_buf.at[0])
+    load(ahead, all_buf.at[1])
+    load(behind, all_buf.at[tp - 1])
+    load(low, all_buf.at[2, pl.ds(0, part)])
+    load(high, all_buf.at[2, pl.ds(part, part)])
     greet(place.twin, place.along_z(1), place.along_z(-1), *peers)
     share = sums_ref.shape[0] // tp
     for rel, peer in enumerate(peers, 1):
@@ -1000,14 +1005,16 @@
         load(wb_far, wbuf.at[pl.ds(2 + tp - 1, tp - 1)])
     count, pass_len, pair = sums_ref.shape
     rows, cols = count * pass_len, pair // 2
-    depth = all_ref.shape[3]
+    depth = own_piece.shape[2]
     width = terms.shape[3]
     loads[0].wait()
     keys_turned[...] = keys[:, :, :cols].reshape(rows, cols).T
-    for n in range(tp):
-        loads[1 + n].wait()
+    for copy in loads[1:6]:
+        copy.wait()
+    for rel in range(tp):
+        n = lax.rem(place.x + rel, tp)
         term = jnp.dot(
-            keys_turned[...], all_buf[n].reshape(rows, depth), preferred_element_type=F32
+            keys_turned[...], all_buf[rel].reshape(rows, depth), preferred_element_type=F32
         )
         for c in range(depth // width):
             for h in range(2):
@@ -1015,7 +1022,7 @@
                     h * (cols // 2) : (h + 1) * (cols // 2), c * width : (c + 1) * width
                 ]
     gift = gifts.start(terms.at[1 - place.k], twin_terms, place.twin)
-    for copy in loads[1 + tp :]:
+    for copy in loads[6:]:
         copy.wait()
 
     def operands(own, far_rows, wbuf):
@@ -1087,7 +1094,7 @@
         group.wait_sends()
 
 
-def tail(ident, sums, all_rows, tokens, tokens_in, weights):
+def tail(ident, sums, tokens, tokens_in, pieces, weights):
     tp, ring = lax.axis_size("tp"), lax.axis_size("st_0")
     model, head_cols = weights[0].shape
     count, pass_len, pair = sums.shape
@@ -1101,7 +1108,7 @@
             jax.ShapeDtypeStruct((share * pass_len, model), low),
             jax.ShapeDtypeStruct((width // 2, head_cols), F32),
         ],
-        in_specs=[ANY_SPEC] * (4 + len(weights)),
+        in_specs=[ANY_SPEC] * (3 + len(pieces) + len(weights)),
         out_specs=[VMEM_SPEC] * 3,
         scratch_shapes=[
             pltpu.VMEM((2 * tp, model, head_cols), low),
@@ -1112,14 +1119,14 @@
             pltpu.VMEM((tp - 1, share, pass_len, pair), low),
             pltpu.VMEM(sums.shape, low),
             pltpu.VMEM((head_cols, count * pass_len), low),
-            pltpu.VMEM(all_rows.shape, low),
+            pltpu.VMEM((tp, *pieces[0].shape), low),
             pltpu.VMEM((2, ring, head_cols // 2, width), F32),
             pltpu.VMEM((ring, head_cols // 2, width), F32),
             pltpu.VMEM((ring, head_cols // 2, width), low),
             pltpu.VMEM((ring, head_cols // 2, width), low),
             pltpu.VMEM((2, width // 2, head_cols // 2), F32),
             pltpu.VMEM((width // 2, head_cols // 2), F32),
-            pltpu.SemaphoreType.DMA((4 + tp + len(weights),)),
+            pltpu.SemaphoreType.DMA((4 + len(pieces) + len(weights),)),
         ]
         + copy_sems(tp - 1)
         + copy_sems(2)
@@ -1128,7 +1135,7 @@
             collective_id=ident, has_side_effects=True, vmem_limit_bytes=VMEM_LIMIT
         ),
         name="tail",
-    )(sums, all_rows, tokens, tokens_in, *weights)
+    )(sums, tokens, tokens_in, *pieces, *weights)
 
 
 def first_slot(plan, d, step):
@@ -1183,10 +1190,12 @@
     requests = pass_ids.size
     plan = Plan(ring, passages)
     ids = jnp.zeros((8, 128), jnp.int32).at[0, :requests].set(pass_ids.reshape(-1))
-    ids, all_rows, kv = front(5, ids, store, w_key, w_value)
+    pieces = gather_store(store)
+    ids = gather_ids(5, ids)
     ids = ids[:, :, 0, :requests].reshape(2 * ring, requests)
     fits, cast_table, fold_table = stream_routes(ring, passages, ids)
     fits = fits[0] > 0
+    kv = keys_values(pieces, w_key, w_value)
 
     def cast_short(ids, table, kv, weights):
         return stream_cast(0, table, kv, weights)
@@ -1213,9 +1222,9 @@
     d_tokens, d_store, d_wkey = tail(
         4,
         sums,
-        all_rows,
         token_grads,
         tokens_in,
+        pieces,
         (w_query, w_gate, wq_far, wg_far, w_key, w_value, wk_far, wv_far),
     )
     return d_tokens, d_store.reshape(passages // tp_count, pass_len, model_width), d_wkey

time: 320 us -> 313 us (0.978)
  Pallas kernels: 307 us -> 294 us
  starting transfers between devices: 0 us -> 6.63 us
    pallas_call x1 -> x2, Pallas kernels: 65.1 us -> 45.1 us  [the longest x1 38.9 us: gather_ids(): pl.pallas_call(ids_kernel, out_shape=jax.ShapeDtypeStruct((ring, 2, *ids....]
    ppermute x0 -> x4, starting transfers between devices: none -> 6.63 us  [the longest x1 2.67 us: gather_store(): high = lax.ppermute(ahead[half:], 'tp', down)]
    pallas_call x1, Pallas kernels: 95.1 us -> 98.8 us  [stream_cast(): pl.pallas_call(functools.partial(stream_cast_kernel, len(weights)), out_s...]
  transfers between devices with their start and end apart: 0 -> 4, of which waited for: 0 -> 0; matrix products, arithmetic and copies ran while one was open for 0% -> 2% of each run, Pallas kernels for 0% -> 16%
where the time goes in v6:
time: 313 us
  Pallas kernels  294 us (94%)
  local copies, waits for them, and re-layouts  9.31 us (3%)
  starting transfers between devices  6.63 us (2%)
    pallas_call x1, Pallas kernels, stream_cast(): pl.pallas_call(functools.partial(stream_cast_kernel, len(weights)), out_s...  98.8 us
    pallas_call x1, Pallas kernels, stream_fold(): pl.pallas_call(stream_fold_kernel, out_shape=[jax.ShapeDtypeStruct((count...  92.5 us
    pallas_call x1, Pallas kernels, gather_ids(): pl.pallas_call(ids_kernel, out_shape=jax.ShapeDtypeStruct((ring, 2, *ids....  38.9 us
    pallas_call x1, Pallas kernels, tail(): pl.pallas_call(tail_kernel, out_shape=[jax.ShapeDtypeStruct((tokens.shape...  36.9 us
    pallas_call x1, Pallas kernels, stream_routes(): pl.pallas_call(functools.partial(routes_kernel, count, requests), out_sha...  12.2 us
    pallas_call x1, Pallas kernels, attend(): pl.pallas_call(functools.partial(attend_kernel, HD ** (-0.5)), grid=(grid...  8.03 us
  transfers between devices with their start and end apart: 4, of which 0 were waited for; matrix products, arithmetic and copies ran while one was open for 2% of the time, Pallas kernels for 16%

profile of v6, /device:TPU:33, one launch (start us, length us, event | category | flops | bytes accessed | tf_op | source)
XLA Modules:
  0.0 313.2 jit_solution(9554674934647073454)
XLA Ops:
  0.6 2.3 collective-permute-start.1
  2.9 1.7 collective-permute-start
  4.6 0.8 copy.16
  5.6 38.9 %gather_ids.1 = s32[16,2,8,128]{3,2,1,0:T(8,128)S(1)} custom-call(s32[8,128]{1,0:T(8,128)S(1)} %scatter.4.ids_ref), custom_call_target="tpu_custom_call" | custom-call | flops 8999999488 | bytes 1000000 | tf_op jit(solution)/shard_map/gather_ids/pallas_call | solution.py:136
  44.7 0.7 select_reduce_fusion.15
  45.9 0.4 convert_reduce_fusion.6
  46.4 0.8 convert_reduce_fusion.4
  47.5 0.6 pad.9.size_ref
  48.4 0.2 select_reduce_fusion.16
  48.6 0.7 concatenate.11.info_ref
  49.3 0.9 slice.28
  50.3 1.0 slice.29
  51.2 2.7 collective-permute-start.3
  53.9 12.2 %routes.1 = (s32[1]{0:T(128)}, s32[140]{0:T(256)S(1)}, s32[672]{0:T(1024)S(1)}) custom-call(s32[8,128]{1,0:T(8,128)} %pad.9.size_ref, s32[448]{0:T(512)} %concatenate.11.info_ref), custom_call_target="tpu_custom_call" | custom-call | flops 6000000000 | bytes 100000 | tf_op jit(solution)/shard_map/routes/pallas_call | solution.py:932
  66.7 6.1 %keys_values.1 = bf16[16,64,512]{2,1,0:T(8,128)(2,1)} custom-call(bf16[16,64,512]{2,1,0:T(8,128)(2,1)} %refs_0_.1, bf16[16,64,512]{2,1,0:T(8,128)(2,1)} %copy-done.2, bf16[16,64,512]{2,1,0:T(8,128)(2,1)} %copy-done.1, bf16[8,64,512]{2,1,0:T(8,128)(2,1)} %collective-permute-done.2.low_ref.refs_3_, ...), custom_call_target="tpu_custom_call" | custom-call | tf_op jit(solution)/shard_map/keys_values/pallas_call | solution.py:177
  72.9 98.8 %conditional.2 = ((bf16[32,64,512]{2,1,0:T(8,128)(2,1)}, bf16[3,2048,256]{2,1,0:T(8,128)(2,1)}, bf16[3,2048,256]{2,1,0:T(8,128)(2,1)}, bf16[3,2048,256]{2,1,0:T(8,128)(2,1)}, bf16[3,2048,256]{2,1,0:T(8,128)(2,1)})) conditional(s32[]{:T(128)} %bitcast.15, (s32[16,2,1,32]{3,2,1,0:T(1,128)S(1)}, s32[32,32]{1,0:T(8,128)S(1)}, ...), branch_computations={%region_7.16_spmd, %region_16.17_spmd} | conditional | flops 3053777 | bytes 118530 | solution.py:1215
  72.9 98.8 %stream_cast.1 = (bf16[32,64,512]{2,1,0:T(8,128)(2,1)}, bf16[3,2048,256]{2,1,0:T(8,128)(2,1)}, bf16[3,2048,256]{2,1,0:T(8,128)(2,1)}, bf16[3,2048,256]{2,1,0:T(8,128)(2,1)}, bf16[3,2048,256]{2,1,0:T(8,128)(2,1)}) custom-call(s32[140]{0:T(256)S(1)} %get-tuple-element.59.table_ref, bf16[16,64,512]{2,1,0:T(8,128)(2,1)} %get-tuple-element.60.kv_ref, ...), custom_call_target="tpu_custom_call" | custom-call | tf_op jit(solution)/shard_map/cond/branch_1_fun/stream_cast/pallas_call | solution.py:609
  171.7 8.0 %attend.1 = (bf16[32,64,512]{2,1,0:T(8,128)(2,1)}, bf16[1024,512]{1,0:T(8,128)(2,1)}) custom-call(bf16[1024,256]{1,0:T(8,128)(2,1)} %q_ref.1, bf16[1024,256]{1,0:T(8,128)(2,1)} %gate_ref.1, bf16[1024,256]{1,0:T(8,128)(2,1)} %mem_ref.1, bf16[32,64,512]{2,1,0:T(8,128)(2,1)} %get-tuple-element.92.kv_ref), custom_call_target="tpu_custom_call" | custom-call | tf_op jit(solution)/shard_map/attend/pallas_call | solution.py:244
  179.7 92.5 %conditional.3 = ((bf16[16,64,512]{2,1,0:T(8,128)(2,1)}, bf16[3,256,512]{2,1,0:T(8,128)(2,1)S(1)})) conditional(s32[]{:T(128)} %bitcast.15, (s32[32,32]{1,0:T(8,128)S(1)}, s32[16,2,1,32]{3,2,1,0:T(1,128)S(1)}, bf16[32,64,512]{2,1,0:T(8,128)(2,1)}, bf16[1024,512]{1,0:T(8,128)(2,1)}) %tuple.70, (s32[672]{0:T(1024)S(1)}, ...), branch_computations={%region_17.29_spmd, %region_29.30_spmd} | conditional | flops 4145074 | bytes 353532 | solution.py:1219
  179.7 92.5 %stream_fold.1 = (bf16[16,64,512]{2,1,0:T(8,128)(2,1)}, bf16[3,256,512]{2,1,0:T(8,128)(2,1)S(1)}) custom-call(s32[672]{0:T(1024)S(1)} %get-tuple-element.69.table_ref, bf16[32,64,512]{2,1,0:T(8,128)(2,1)} %get-tuple-element.70.grads_ref, bf16[1024,512]{1,0:T(8,128)(2,1)} %get-tuple-element.71.tokens_ref), custom_call_target="tpu_custom_call" | custom-call | tf_op jit(solution)/shard_map/cond/branch_1_fun/stream_fold/pallas_call | solution.py:722
  272.2 36.9 %tail.1 = (bf16[256,2048]{1,0:T(8,128)(2,1)}, bf16[256,2048]{1,0:T(8,128)(2,1)}, f32[64,256]{1,0:T(8,128)}) custom-call(bf16[16,64,512]{2,1,0:T(8,128)(2,1)} %get-tuple-element.96.sums_ref, bf16[1024,512]{1,0:T(8,128)(2,1)} %get-tuple-element.94.tokens_ref, bf16[3,256,512]{2,1,0:T(8,128)(2,1)S(1)} %get-tuple-element.97.tokens_in, ...), custom_call_target="tpu_custom_call" | custom-call | tf_op jit(solution)/shard_map/tail/pallas_call | solution.py:1104
  309.2 2.4 copy.34
  311.6 1.0 copy.35
  312.5 0.6 copy.36
  (50 shorter events, 1.6 us)
Async XLA Ops:
  0.6 48.7 %collective-permute-start.1 = (bf16[16,64,512]{2,1,0:T(8,128)(2,1)}, bf16[16,64,512]{2,1,0:T(8,128)(2,1)S(1)}, u32[]{:S(2)}, u32[]{:S(2)}) collective-permute-start(bf16[16,64,512]{2,1,0:T(8,128)(2,1)} %refs_0_.1), channel_id=1, source_target_pairs={{0,1},{1,2},{2,3},{3,0},{4,5},{5,6},{6,7},{7,4},{8,9},{9,10},{10,1... | collective-permute-start | bytes 3145736 | tf_op jit(solution)/shard_map/ppermute | solution.py:192
  2.9 47.4 %collective-permute-start = (bf16[16,64,512]{2,1,0:T(8,128)(2,1)}, bf16[16,64,512]{2,1,0:T(8,128)(2,1)S(1)}, u32[]{:S(2)}, u32[]{:S(2)}) collective-permute-start(bf16[16,64,512]{2,1,0:T(8,128)(2,1)} %refs_0_.1), channel_id=1, source_target_pairs={{0,3},{1,0},{2,1},{3,2},{4,7},{5,4},{6,5},{7,6},{8,11},{9,8},{10,9... | collective-permute-start | bytes 3145736 | tf_op jit(solution)/shard_map/ppermute | solution.py:193
  49.3 16.8 %copy-start.1 = (bf16[16,64,512]{2,1,0:T(8,128)(2,1)}, bf16[16,64,512]{2,1,0:T(8,128)(2,1)S(1)}, u32[]{:S(2)}) copy-start(bf16[16,64,512]{2,1,0:T(8,128)(2,1)S(1)} %collective-permute-done.1.behind_ref.refs_2_) | copy-start | bytes 3145732
  50.3 16.4 %collective-permute-start.2 = (bf16[8,64,512]{2,1,0:T(8,128)(2,1)}, bf16[8,64,512]{2,1,0:T(8,128)(2,1)}, u32[]{:S(2)}, u32[]{:S(2)}) collective-permute-start(bf16[8,64,512]{2,1,0:T(8,128)(2,1)} %slice.28), channel_id=1, source_target_pairs={{0,1},{1,2},{2,3},{3,0},{4,5},{5,6},{6,7},{7,4},{8,9},{9,10},{10,1... | collective-permute-start | bytes 1572872 | tf_op jit(solution)/shard_map/ppermute | solution.py:194
  50.3 15.9 %copy-start.2 = (bf16[16,64,512]{2,1,0:T(8,128)(2,1)}, bf16[16,64,512]{2,1,0:T(8,128)(2,1)S(1)}, u32[]{:S(2)}) copy-start(bf16[16,64,512]{2,1,0:T(8,128)(2,1)S(1)} %collective-permute-done.ahead_ref.refs_1_) | copy-start | bytes 3145732
  51.2 15.5 %copy-start = (bf16[2048,256]{1,0:T(8,128)(2,1)S(1)}, bf16[2048,256]{1,0:T(8,128)(2,1)}, u32[]{:S(2)}) copy-start(bf16[2048,256]{1,0:T(8,128)(2,1)} %refs_9_.1) | copy-start | bytes 3145732
  51.2 15.5 %collective-permute-start.3 = (bf16[8,64,512]{2,1,0:T(8,128)(2,1)}, bf16[8,64,512]{2,1,0:T(8,128)(2,1)}, u32[]{:S(2)}, u32[]{:S(2)}) collective-permute-start(bf16[8,64,512]{2,1,0:T(8,128)(2,1)} %slice.29), channel_id=1, source_target_pairs={{0,3},{1,0},{2,1},{3,2},{4,7},{5,4},{6,5},{7,6},{8,11},{9,8},{10,9... | collective-permute-start | bytes 1572872 | tf_op jit(solution)/shard_map/ppermute | solution.py:195
  309.2 2.4 copy-start.3
  309.2 3.4 %copy-start.4 = (f32[64,256]{1,0:T(8,128)S(1)}, f32[64,256]{1,0:T(8,128)}, u32[]{:S(2)}) copy-start(f32[64,256]{1,0:T(8,128)} %get-tuple-element.174) | copy-start | bytes 196612

commit v7 on v6

--- a/solution.py
+++ b/solution.py
@@ -107,27 +107,21 @@
     return [pltpu.SemaphoreType.DMA((count,)), pltpu.SemaphoreType.DMA((count,))]
 
 
-def ids_kernel(ids_ref, ids_out, *sems):
-    gifts, ring_copies = (Copies(*sems[2 * i : 2 * i + 2]) for i in range(2))
+def ids_kernel(ids_ref, ids_out, twin_ids, *sems):
+    gifts, sends = (Copies(*sems[2 * i : 2 * i + 2]) for i in range(2))
     place = Place()
-    reach = place.ring // 2
-    greet(place.along_z(1), place.along_z(-1), place.twin)
-    gift = gifts.start(ids_ref, ids_out.at[place.z, place.k], place.twin)
-    ids_out[place.z, place.k] = ids_ref[...]
+    peers = [place.along_z(step) for step in range(1, place.ring)]
+    greet(place.twin, *peers)
+    gift = gifts.start(ids_ref, twin_ids, place.twin)
+    row = lax.broadcasted_iota(jnp.int32, ids_ref.shape, 0)
     gift.wait_recv()
-    hops = {}
-    for t in range(1, reach + 1):
-        for d in range(2):
-            if t > reach - d:
-                continue
-            if t > 1:
-                hops[d, t - 1].wait_recv()
-            source = lax.rem(place.z + (t - 1) * (2 * d - 1) + place.ring, place.ring)
-            part = ids_out.at[source]
-            hops[d, t] = ring_copies.start(part, part, place.along_z(1 - 2 * d))
-    for d in range(2):
-        hops[d, reach - d].wait_recv()
-    for group in (gifts, ring_copies):
+    ids_out[place.z] = jnp.where(row == place.k, ids_ref[...], twin_ids[...])
+    part = ids_out.at[place.z]
+    for peer in peers:
+        sends.start(part, part, peer)
+    for copy in sends.all:
+        copy.wait_recv()
+    for group in (gifts, sends):
         group.wait_sends()
 
 
@@ -135,10 +129,10 @@
     ring = lax.axis_size("st_0")
     return pl.pallas_call(
         ids_kernel,
-        out_shape=jax.ShapeDtypeStruct((ring, 2, *ids.shape), ids.dtype),
+        out_shape=jax.ShapeDtypeStruct((ring, *ids.shape), ids.dtype),
         in_specs=[VMEM_SPEC],
         out_specs=VMEM_SPEC,
-        scratch_shapes=copy_sems(1) + copy_sems(ring - 1),
+        scratch_shapes=[pltpu.VMEM(ids.shape, ids.dtype)] + copy_sems(1) + copy_sems(ring - 1),
         compiler_params=pltpu.CompilerParams(
             collective_id=ident, has_side_effects=True, vmem_limit_bytes=8 * 1024 * 1024
         ),
@@ -823,18 +817,17 @@
     readers = 2 * MOST
     onward_at, final_at = (slots + 1) * readers, (slots + 1) * readers + 2 * LENGTH
 
-    @pl.loop(0, onward_at)
-    def _(i):
-        fold_ref[i] = 2 * requests
-
     @pl.loop(0, slots + 1)
     def _(i):
         used[i] = 0
-
-    @pl.loop(0, 2 * LENGTH)
+        for q in range(readers):
+            fold_ref[i * readers + q] = 2 * requests
+
+    @pl.loop(0, LENGTH)
     def _(i):
-        fold_ref[onward_at + i] = 2 * LENGTH
-        cast_ref[i] = 0
+        for q in range(2):
+            fold_ref[onward_at + 2 * i + q] = 2 * LENGTH
+            cast_ref[2 * i + q] = 0
 
     def info(row, i):
         return info_ref[row * 2 * requests + i]
@@ -1009,21 +1002,21 @@
     width = terms.shape[3]
     loads[0].wait()
     keys_turned[...] = keys[:, :, :cols].reshape(rows, cols).T
-    for copy in loads[1:6]:
-        copy.wait()
+    chips = depth // width
     for rel in range(tp):
+        for copy in [loads[1:2], loads[2:3], loads[4:6], loads[3:4]][rel]:
+            copy.wait()
         n = lax.rem(place.x + rel, tp)
         term = jnp.dot(
             keys_turned[...], all_buf[rel].reshape(rows, depth), preferred_element_type=F32
         )
-        for c in range(depth // width):
+        for c in range(chips):
             for h in range(2):
-                terms[h, n * (depth // width) + c] = term[
+                terms[h, n * chips + c] = term[
                     h * (cols // 2) : (h + 1) * (cols // 2), c * width : (c + 1) * width
                 ]
-    gift = gifts.start(terms.at[1 - place.k], twin_terms, place.twin)
-    for copy in loads[6:]:
-        copy.wait()
+        part = pl.ds(n * chips, chips)
+        gifts.start(terms.at[1 - place.k, part], twin_terms.at[part], place.twin)
 
     def operands(own, far_rows, wbuf):
         n_cols = own.shape[-1] // 2
@@ -1044,7 +1037,8 @@
     for_store = operands(
         own_s.reshape(part_rows, pair), in_s.reshape(tp - 1, part_rows, pair), wbuf_s
     )
-    gift.wait_recv()
+    for gift in gifts.all:
+        gift.wait_recv()
     hops = {}
 
     def mine(dest):
@@ -1064,6 +1058,9 @@
                 total += come[n - 1].astype(F32)
             sent[n] = total.astype(sent.dtype)
             hops[d, s] = ring_copies.start(sent.at[n], come.at[n], place.along_z(turn))
+        if s == 1:
+            for copy in loads[6:]:
+                copy.wait()
         if s == reach // 2:
             for copy in exchange.all:
                 copy.wait_recv()
@@ -1129,7 +1126,7 @@
             pltpu.SemaphoreType.DMA((4 + len(pieces) + len(weights),)),
         ]
         + copy_sems(tp - 1)
-        + copy_sems(2)
+        + copy_sems(tp + 1)
         + copy_sems(ring - 1),
         compiler_params=pltpu.CompilerParams(
             collective_id=ident, has_side_effects=True, vmem_limit_bytes=VMEM_LIMIT
@@ -1189,10 +1186,10 @@
     model_width = w_key.shape[0]
     requests = pass_ids.size
     plan = Plan(ring, passages)
-    ids = jnp.zeros((8, 128), jnp.int32).at[0, :requests].set(pass_ids.reshape(-1))
+    ids = jnp.zeros((8, 128), jnp.int32).at[:2, :requests].set(pass_ids.reshape(1, -1))
     pieces = gather_store(store)
     ids = gather_ids(5, ids)
-    ids = ids[:, :, 0, :requests].reshape(2 * ring, requests)
+    ids = ids[:, :2, :requests].reshape(2 * ring, requests)
     fits, cast_table, fold_table = stream_routes(ring, passages, ids)
     fits = fits[0] > 0
     kv = keys_values(pieces, w_key, w_value)

time: 313 us -> 302 us (0.965)
  Pallas kernels: 294 us -> 280 us
    pallas_call x1, Pallas kernels: 36.9 us -> 31.9 us  [tail(): pl.pallas_call(tail_kernel, out_shape=[jax.ShapeDtypeStruct((tokens.shape...]
    pallas_call x1, Pallas kernels: 38.9 us -> 34.3 us  [gather_ids(): pl.pallas_call(ids_kernel, out_shape=jax.ShapeDtypeStruct((ring, *ids.sha...]
    pallas_call x1, Pallas kernels: 12.2 us -> 9 us  [stream_routes(): pl.pallas_call(functools.partial(routes_kernel, count, requests), out_sha...]
  transfers between devices with their start and end apart: 4 -> 4, of which waited for: 0 -> 1; matrix products, arithmetic and copies ran while one was open for 2% -> 3% of each run, Pallas kernels for 16% -> 14%
where the time goes in v7:
time: 302 us; the launch traced here: 301 us
  Pallas kernels  280 us (93%)
  local copies, waits for them, and re-layouts  9.26 us (3%)
  starting transfers between devices  6.63 us (2%)
    pallas_call x1, Pallas kernels, stream_cast(): pl.pallas_call(functools.partial(stream_cast_kernel, len(weights)), out_s...  97.5 us
    pallas_call x1, Pallas kernels, stream_fold(): pl.pallas_call(stream_fold_kernel, out_shape=[jax.ShapeDtypeStruct((count...  92.9 us
    pallas_call x1, Pallas kernels, gather_ids(): pl.pallas_call(ids_kernel, out_shape=jax.ShapeDtypeStruct((ring, *ids.sha...  34.3 us
    pallas_call x1, Pallas kernels, tail(): pl.pallas_call(tail_kernel, out_shape=[jax.ShapeDtypeStruct((tokens.shape...  31.9 us
    pallas_call x1, Pallas kernels, stream_routes(): pl.pallas_call(functools.partial(routes_kernel, count, requests), out_sha...  9 us
    pallas_call x1, Pallas kernels, attend(): pl.pallas_call(functools.partial(attend_kernel, HD ** (-0.5)), grid=(grid...  8 us
    pallas_call x1, Pallas kernels, keys_values(): pl.pallas_call(keys_values_kernel, grid=(steps,), out_shape=jax.ShapeDtyp...  6.13 us
  transfers between devices with their start and end apart: 4, of which 1 were waited for; matrix products, arithmetic and copies ran while one was open for 3% of the time, Pallas kernels for 14%

profile of v7, /device:TPU:33, one launch (start us, length us, event | category | flops | bytes accessed | tf_op | source)
XLA Modules:
  0.0 301.5 jit_solution(10592938819382424789)
XLA Ops:
  0.6 2.3 collective-permute-start.1
  2.9 1.7 collective-permute-start
  4.6 0.8 copy.16
  5.6 34.3 %gather_ids.1 = s32[16,8,128]{2,1,0:T(8,128)S(1)} custom-call(s32[8,128]{1,0:T(8,128)S(1)} %scatter.4.ids_ref), custom_call_target="tpu_custom_call" | custom-call | flops 8999999488 | bytes 1000000 | tf_op jit(solution)/shard_map/gather_ids/pallas_call | solution.py:130
  40.1 0.7 select_reduce_fusion.15
  41.2 0.4 convert_reduce_fusion.6
  41.8 0.8 convert_reduce_fusion.4
  42.8 0.6 pad.10.size_ref
  44.0 0.7 concatenate.11.info_ref
  44.7 0.9 slice.32
  45.7 1.0 slice.33
  46.7 2.6 collective-permute-start.3
  49.3 9.0 %routes.1 = (s32[1]{0:T(128)}, s32[140]{0:T(256)S(1)}, s32[672]{0:T(1024)S(1)}) custom-call(s32[8,128]{1,0:T(8,128)} %pad.10.size_ref, s32[448]{0:T(512)} %concatenate.11.info_ref), custom_call_target="tpu_custom_call" | custom-call | flops 6000000000 | bytes 100000 | tf_op jit(solution)/shard_map/routes/pallas_call | solution.py:925
  58.9 2.1 collective-permute-done.2.low_ref.refs_3_
  61.0 6.1 %keys_values.1 = bf16[16,64,512]{2,1,0:T(8,128)(2,1)} custom-call(bf16[16,64,512]{2,1,0:T(8,128)(2,1)} %refs_0_.1, bf16[16,64,512]{2,1,0:T(8,128)(2,1)} %copy-done.2, bf16[16,64,512]{2,1,0:T(8,128)(2,1)} %copy-done.1, bf16[8,64,512]{2,1,0:T(8,128)(2,1)} %collective-permute-done.2.low_ref.refs_3_, ...), custom_call_target="tpu_custom_call" | custom-call | tf_op jit(solution)/shard_map/keys_values/pallas_call | solution.py:171
  67.1 97.5 %conditional.2 = ((bf16[32,64,512]{2,1,0:T(8,128)(2,1)}, bf16[3,2048,256]{2,1,0:T(8,128)(2,1)}, bf16[3,2048,256]{2,1,0:T(8,128)(2,1)}, bf16[3,2048,256]{2,1,0:T(8,128)(2,1)}, bf16[3,2048,256]{2,1,0:T(8,128)(2,1)})) conditional(s32[]{:T(128)} %bitcast.15, (s32[16,2,32]{2,1,0:T(2,128)S(1)}, s32[32,32]{1,0:T(8,128)S(1)}, ...), branch_computations={%region_7.16_spmd, %region_16.17_spmd} | conditional | flops 3053777 | bytes 110326 | solution.py:1212
  67.1 97.5 %stream_cast.1 = (bf16[32,64,512]{2,1,0:T(8,128)(2,1)}, bf16[3,2048,256]{2,1,0:T(8,128)(2,1)}, bf16[3,2048,256]{2,1,0:T(8,128)(2,1)}, bf16[3,2048,256]{2,1,0:T(8,128)(2,1)}, bf16[3,2048,256]{2,1,0:T(8,128)(2,1)}) custom-call(s32[140]{0:T(256)S(1)} %get-tuple-element.59.table_ref, bf16[16,64,512]{2,1,0:T(8,128)(2,1)} %get-tuple-element.60.kv_ref, ...), custom_call_target="tpu_custom_call" | custom-call | tf_op jit(solution)/shard_map/cond/branch_1_fun/stream_cast/pallas_call | solution.py:603
  164.7 8.0 %attend.1 = (bf16[32,64,512]{2,1,0:T(8,128)(2,1)}, bf16[1024,512]{1,0:T(8,128)(2,1)}) custom-call(bf16[1024,256]{1,0:T(8,128)(2,1)} %q_ref.1, bf16[1024,256]{1,0:T(8,128)(2,1)} %gate_ref.1, bf16[1024,256]{1,0:T(8,128)(2,1)} %mem_ref.1, bf16[32,64,512]{2,1,0:T(8,128)(2,1)} %get-tuple-element.92.kv_ref), custom_call_target="tpu_custom_call" | custom-call | tf_op jit(solution)/shard_map/attend/pallas_call | solution.py:238
  172.7 92.9 %conditional.3 = ((bf16[16,64,512]{2,1,0:T(8,128)(2,1)}, bf16[3,256,512]{2,1,0:T(8,128)(2,1)S(1)})) conditional(s32[]{:T(128)} %bitcast.15, (s32[32,32]{1,0:T(8,128)S(1)}, s32[16,2,32]{2,1,0:T(2,128)S(1)}, bf16[32,64,512]{2,1,0:T(8,128)(2,1)}, bf16[1024,512]{1,0:T(8,128)(2,1)}) %tuple.69, (s32[672]{0:T(1024)S(1)}, bf16[32,64,512]{2,1,0:T(8,128)(2,1)}, ...), branch_computations={%region_17.29_spmd, %region_29.30_spmd} | conditional | flops 4145074 | bytes 345328 | solution.py:1216
  172.7 92.9 %stream_fold.1 = (bf16[16,64,512]{2,1,0:T(8,128)(2,1)}, bf16[3,256,512]{2,1,0:T(8,128)(2,1)S(1)}) custom-call(s32[672]{0:T(1024)S(1)} %get-tuple-element.69.table_ref, bf16[32,64,512]{2,1,0:T(8,128)(2,1)} %get-tuple-element.70.grads_ref, bf16[1024,512]{1,0:T(8,128)(2,1)} %get-tuple-element.71.tokens_ref), custom_call_target="tpu_custom_call" | custom-call | tf_op jit(solution)/shard_map/cond/branch_1_fun/stream_fold/pallas_call | solution.py:716
  265.5 31.9 %tail.1 = (bf16[256,2048]{1,0:T(8,128)(2,1)}, bf16[256,2048]{1,0:T(8,128)(2,1)}, f32[64,256]{1,0:T(8,128)}) custom-call(bf16[16,64,512]{2,1,0:T(8,128)(2,1)} %get-tuple-element.96.sums_ref, bf16[1024,512]{1,0:T(8,128)(2,1)} %get-tuple-element.94.tokens_ref, bf16[3,256,512]{2,1,0:T(8,128)(2,1)S(1)} %get-tuple-element.97.tokens_in, ...), custom_call_target="tpu_custom_call" | custom-call | tf_op jit(solution)/shard_map/tail/pallas_call | solution.py:1101
  297.5 2.4 copy.34
  299.9 1.0 copy.35
  300.8 0.6 copy.36
  (51 shorter events, 1.8 us)
Async XLA Ops:
  0.6 44.1 %collective-permute-start.1 = (bf16[16,64,512]{2,1,0:T(8,128)(2,1)}, bf16[16,64,512]{2,1,0:T(8,128)(2,1)S(1)}, u32[]{:S(2)}, u32[]{:S(2)}) collective-permute-start(bf16[16,64,512]{2,1,0:T(8,128)(2,1)} %refs_0_.1), channel_id=1, source_target_pairs={{0,1},{1,2},{2,3},{3,0},{4,5},{5,6},{6,7},{7,4},{8,9},{9,10},{10,1... | collective-permute-start | bytes 3145736 | tf_op jit(solution)/shard_map/ppermute | solution.py:186
  2.9 42.8 %collective-permute-start = (bf16[16,64,512]{2,1,0:T(8,128)(2,1)}, bf16[16,64,512]{2,1,0:T(8,128)(2,1)S(1)}, u32[]{:S(2)}, u32[]{:S(2)}) collective-permute-start(bf16[16,64,512]{2,1,0:T(8,128)(2,1)} %refs_0_.1), channel_id=1, source_target_pairs={{0,3},{1,0},{2,1},{3,2},{4,7},{5,4},{6,5},{7,6},{8,11},{9,8},{10,9... | collective-permute-start | bytes 3145736 | tf_op jit(solution)/shard_map/ppermute | solution.py:187
  44.7 13.6 %copy-start.1 = (bf16[16,64,512]{2,1,0:T(8,128)(2,1)}, bf16[16,64,512]{2,1,0:T(8,128)(2,1)S(1)}, u32[]{:S(2)}) copy-start(bf16[16,64,512]{2,1,0:T(8,128)(2,1)S(1)} %collective-permute-done.1.behind_ref.refs_2_) | copy-start | bytes 3145732
  45.6 15.4 %collective-permute-start.2 = (bf16[8,64,512]{2,1,0:T(8,128)(2,1)}, bf16[8,64,512]{2,1,0:T(8,128)(2,1)}, u32[]{:S(2)}, u32[]{:S(2)}) collective-permute-start(bf16[8,64,512]{2,1,0:T(8,128)(2,1)} %slice.32), channel_id=1, source_target_pairs={{0,1},{1,2},{2,3},{3,0},{4,5},{5,6},{6,7},{7,4},{8,9},{9,10},{10,1... | collective-permute-start | bytes 1572872 | tf_op jit(solution)/shard_map/ppermute | solution.py:188
  45.7 12.6 %copy-start.2 = (bf16[16,64,512]{2,1,0:T(8,128)(2,1)}, bf16[16,64,512]{2,1,0:T(8,128)(2,1)S(1)}, u32[]{:S(2)}) copy-start(bf16[16,64,512]{2,1,0:T(8,128)(2,1)S(1)} %collective-permute-done.ahead_ref.refs_1_) | copy-start | bytes 3145732
  46.7 14.4 %copy-start = (bf16[2048,256]{1,0:T(8,128)(2,1)S(1)}, bf16[2048,256]{1,0:T(8,128)(2,1)}, u32[]{:S(2)}) copy-start(bf16[2048,256]{1,0:T(8,128)(2,1)} %refs_9_.1) | copy-start | bytes 3145732
  46.7 14.3 %collective-permute-start.3 = (bf16[8,64,512]{2,1,0:T(8,128)(2,1)}, bf16[8,64,512]{2,1,0:T(8,128)(2,1)}, u32[]{:S(2)}, u32[]{:S(2)}) collective-permute-start(bf16[8,64,512]{2,1,0:T(8,128)(2,1)} %slice.33), channel_id=1, source_target_pairs={{0,3},{1,0},{2,1},{3,2},{4,7},{5,4},{6,5},{7,6},{8,11},{9,8},{10,9... | collective-permute-start | bytes 1572872 | tf_op jit(solution)/shard_map/ppermute | solution.py:189
  297.4 2.4 copy-start.3
  297.5 3.4 %copy-start.4 = (f32[64,256]{1,0:T(8,128)S(1)}, f32[64,256]{1,0:T(8,128)}, u32[]{:S(2)}) copy-start(f32[64,256]{1,0:T(8,128)} %get-tuple-element.172) | copy-start | bytes 196612
